TPU v7x, 32 devices: a whole 2x2x4 slice. The times are simulated.
32 devices in a mesh: sp: 16 (over z, y, x), tp: 2 (over core).
Axes of the slice: x: 2, y: 2, z: 4, core: 2. Of those that a mesh axis runs over, the one named last changes fastest.
Arguments:
- hidden_in: bfloat16 [4096, 2048], P('sp'), may hold values from -16 to 16
- query_one: bfloat16 [2048, 512], P(None, 'tp'), may hold values from -0.13258252 to 0.13258252
- query_two: bfloat16 [2048, 512], P(None, 'tp'), may hold values from -0.13258252 to 0.13258252
- key_one: bfloat16 [2048, 512], P(None, 'tp'), may hold values from -0.13258252 to 0.13258252
- key_two: bfloat16 [2048, 512], P(None, 'tp'), may hold values from -0.13258252 to 0.13258252
- value_proj: bfloat16 [2048, 1024], P(None, 'tp'), may hold values from -0.125 to 0.125
- lambdas: float32 [8], P('tp'), may hold values from 0.3 to 0.8
- norm_gain: float32 [128], replicated, may hold values from 0.1 to 1.9
- out_proj: bfloat16 [1024, 2048], P('tp'), may hold values from -0.1875 to 0.1875
Outputs:
- attended: bfloat16 [4096, 2048], P('sp')
All inputs are finite; a program needn't handle non-finite values.
Results may differ from a plain program's by a relative error of at most 0.015.
Values may be sent and summed in bfloat16 or wider, within the bound.
No kernel may reach another device: no remote copies, remote signals or barrier semaphores. Data moves between devices by JAX's collectives and lax.ppermute only.
A program may use at most 64 MiB of HBM per device.

v0:
```python
import math

import jax
import jax.numpy as jnp
from jax import lax
from jax.sharding import PartitionSpec as P

epsilon = 1e-06
masked_score = -1e30


def shards(
    hidden_in, query_one, query_two, key_one, key_two, value_proj, lambdas, norm_gain, out_proj
):
    heads_dev = lambdas.shape[0]
    head_qk = query_one.shape[1] // heads_dev
    head_v = value_proj.shape[1] // heads_dev
    width_q = heads_dev * head_qk
    score_scale = 1.75 * head_qk ** (-0.5)
    joined = jnp.concatenate((query_one, query_two, key_one, key_two, value_proj), axis=1)
    projected = jnp.dot(hidden_in, joined, preferred_element_type=jnp.float32).astype(jnp.bfloat16)
    tok_rows = projected.shape[0]
    key_values = projected[:, 2 * width_q :]
    my_index = lax.axis_index("sp")
    offset = my_index * tok_rows
    query_sets = (projected[:, : 2 * width_q],)
    position_sets = (offset + jnp.arange(tok_rows, dtype=jnp.int32),)
    groups = []
    for query_rows, positions in zip(query_sets, position_sets):
        group_rows = query_rows.shape[0]
        query_a = query_rows[:, :width_q].reshape(group_rows, heads_dev, head_qk)
        query_b = query_rows[:, width_q:].reshape(group_rows, heads_dev, head_qk)
        groups.append((query_a, query_b, positions, positions[group_rows - 1]))

    def one_map(queries, keys, value_rows, allowed, running_max, running_sum, accum):
        scores = (
            jnp.einsum("qhd,khd->hqk", queries, keys, preferred_element_type=jnp.float32)
            * score_scale
        )
        scores = jnp.where(allowed[None], scores, masked_score)
        new_max = jnp.maximum(running_max, jnp.max(scores, axis=-1))
        rescale = jnp.exp(running_max - new_max)
        weights = jnp.where(allowed[None], jnp.exp(scores - new_max[..., None]), 0.0)
        new_sum = running_sum * rescale + jnp.sum(weights, axis=-1)
        added = jnp.einsum(
            "hqk,khe->hqe",
            weights.astype(jnp.bfloat16),
            value_rows,
            preferred_element_type=jnp.float32,
        )
        return (new_max, new_sum, accum * rescale[..., None] + added)

    def absorb(group_state, group, kblock, kstart):
        query_a, query_b, positions, last_pos = group
        block_rows = kblock.shape[0]
        k_pos = kstart + jnp.arange(block_rows, dtype=jnp.int32)
        allowed = k_pos[None, :] <= positions[:, None]
        keys_a = kblock[:, :width_q].reshape(block_rows, heads_dev, head_qk)
        keys_b = kblock[:, width_q : 2 * width_q].reshape(block_rows, heads_dev, head_qk)
        value_rows = kblock[:, 2 * width_q :].reshape(block_rows, heads_dev, head_v)
        first_map = one_map(query_a, keys_a, value_rows, allowed, *group_state[:3])
        second_map = one_map(query_b, keys_b, value_rows, allowed, *group_state[3:])
        return first_map + second_map

    group = groups[0]
    group_rows = group[0].shape[0]
    start_max = jnp.full((heads_dev, group_rows), masked_score, jnp.float32)
    start_sum = jnp.zeros((heads_dev, group_rows), jnp.float32)
    start_acc = jnp.zeros((heads_dev, group_rows, head_v), jnp.float32)
    initial_list = [(start_max, start_sum, start_acc, start_max, start_sum, start_acc)]
    initial = tuple(initial_list)
    softmax_state = initial
    kv_piece = lax.all_gather(key_values, "sp", axis=0, tiled=True)
    piece_rows = kv_piece.shape[0]
    block_rows = math.gcd(piece_rows, 512)
    block_count = piece_rows // block_rows
    stacked = kv_piece.reshape(block_count, block_rows, kv_piece.shape[1])

    def absorb_step(carried, blocks_in):
        kblock, block_index = blocks_in
        kstart = block_index * block_rows
        renewed = []
        for group, group_state in zip(groups, carried):
            renewed.append(
                lax.cond(
                    kstart <= group[3],
                    lambda inner, group=group: absorb(inner, group, kblock, kstart),
                    lambda inner: inner,
                    group_state,
                )
            )
        return (tuple(renewed), None)

    softmax_state, _ = lax.scan(
        absorb_step, softmax_state, (stacked, jnp.arange(block_count, dtype=jnp.int32))
    )
    normed_sets = []
    for group_state in softmax_state:
        out_a = group_state[2] / group_state[1][..., None]
        out_b = group_state[5] / group_state[4][..., None]
        mixed_out = out_a - lambdas[:, None, None] * out_b
        scale_rows = lax.rsqrt(jnp.mean(mixed_out * mixed_out, axis=-1, keepdims=True) + epsilon)
        normed = (mixed_out * scale_rows * norm_gain).astype(jnp.bfloat16)
        group_rows = normed.shape[1]
        normed_sets.append(jnp.transpose(normed, (1, 0, 2)).reshape(group_rows, heads_dev * head_v))
    normed_all = normed_sets[0]
    partial_value = jnp.dot(normed_all, out_proj, preferred_element_type=jnp.float32)
    result = lax.psum(partial_value.astype(jnp.bfloat16), "tp")
    return result


def solution(mesh):
    placed = (
        P("sp", None),
        P(None, "tp"),
        P(None, "tp"),
        P(None, "tp"),
        P(None, "tp"),
        P(None, "tp"),
        P("tp"),
        P(),
        P("tp", None),
    )
    return jax.shard_map(
        shards, mesh=mesh, in_specs=placed, out_specs=P("sp", None), check_vma=False
    )
```

profile of v0, /device:TPU:0, one launch (start us, length us, event | category | flops | bytes accessed | tf_op | source)
XLA Modules:
  0.0 254.4 jit_solution(17439998530829736582)
XLA Ops:
  6.5 1.5 constant_dynamic-update-slice_fusion.4
  8.0 0.2 copy-done.2
  8.3 0.2 copy-done.3
  8.6 0.9 copy-done.4
  9.6 0.6 copy-done.1
  10.3 1.1 copy-done.7
  11.4 1.8 fusion.24
  13.3 0.8 slice.34
  14.2 0.7 slice.27
  14.9 136.6 %all-gather.2.cloned.1.call-done = bf16[4096,1024]{0,1:T(8,128)(2,1)} async-done(((bf16[256,1024]{0,1:T(8,128)(2,1)}), bf16[4096,1024]{0,1:T(8,128)(2,1)}) %all-gather.2.cloned.1.call-update) | async-done | bytes 8388624 | tf_op jit(solution)/shard_map/all_gather | solution.py:73
  151.5 7.4 %copy.26 = bf16[128,8,8,512]{3,2,0,1:T(8,128)(2,1)} copy(bf16[128,8,8,512]{3,2,1,0:T(8,128)(2,1)} %bitcast.57) | data formatting | bytes 16777216 | tf_op jit(solution)/shard_map/reshape | solution.py:77
  159.0 21.9 %while.21 = (s32[]{:T(128)}, f32[4,256]{1,0:T(4,128)S(1)}, f32[4,256]{1,0:T(4,128)S(1)}, f32[4,256,128]{2,1,0:T(8,128)S(1)}, f32[4,256]{1,0:T(4,128)S(1)}, /*ind...) while((s32[]{:T(128)}, f32[4,256]{1,0:T(4,128)S(1)}, ...), condition=%wide.region_7.8_spmd.clone, body=%wide.region_0.7_spmd.clone.sunk | while | flops 416944896 | bytes 23601552 | solution.py:94
  159.1 0.6 dynamic_slice.13
  161.0 6.1 %conditional.3 = ((f32[4,256]{1,0:T(4,128)S(1)}, f32[4,256]{1,0:T(4,128)S(1)}, f32[4,256,128]{2,1,0:T(8,128)S(1)}, f32[4,256]{1,0:T(4,128)S(1)}, f32[4,256]{1,0:T(4,128)S(1)}, /*index=5*/f32[4,256,128]{2,1,0:T(8,128)S(1)})) conditional(s32[]{:T(128)} %convert_element_type.38, (f32[4,256]{1,0:T(4,128)S(1)}, f32[4,256]{1,0:T(4,128)S(1)}, ...), branch_computations={%region_1.1_spmd, %region_2.6_spmd} | conditional | flops 416944896 | bytes 23600196 | solution.py:85
  161.0 1.3 dynamic-slice_bitcast_fusion
  162.4 0.5 fusion.27
  163.0 0.7 fusion.3
  163.8 1.0 fusion.7
  164.9 1.1 convolution_add_fusion
  165.9 1.1 convolution_add_fusion.1
  167.1 0.6 dynamic_slice.13
  169.1 0.6 dynamic_slice.13
  171.0 0.6 dynamic_slice.13
  173.0 0.6 dynamic_slice.13
  175.0 0.6 dynamic_slice.13
  177.0 0.6 dynamic_slice.13
  179.0 0.6 dynamic_slice.13
  180.9 1.0 copy.18
  182.2 1.2 multiply_reduce_fusion
  183.5 1.7 convolution_convert_fusion
  185.2 60.0 %all-reduce.2.cloned.1.call-done = bf16[256,2048]{1,0:T(8,128)(2,1)} async-done(((bf16[256,2048]{1,0:T(8,128)(2,1)}), bf16[256,2048]{1,0:T(8,128)(2,1)}) %all-reduce.2.cloned.1.call-update) | async-done | bytes 1048592 | tf_op jit(solution)/shard_map/psum | solution.py:108
  245.3 2.3 copy.67
  (56 shorter events, 1.3 us)
Async XLA Ops:
  6.5 177.0 %copy-start = (bf16[512,2048]{1,0:T(8,128)(2,1)S(1)}, bf16[512,2048]{1,0:T(8,128)(2,1)}, u32[]{:S(2)}) copy-start(bf16[512,2048]{1,0:T(8,128)(2,1)} %param.21) | copy-start | bytes 6291460
  6.5 1.7 copy-start.2
  6.5 145.0 %all-gather.2.cloned.1.call-start = ((), (), s32[]{:S(2)}) async-start(), calls=%async_computation | async-start | bytes 8912896 | tf_op jit(solution)/shard_map/all_gather | solution.py:73
  6.5 2.0 copy-start.3
  8.2 1.3 copy-start.4
  8.5 1.7 copy-start.1
  10.2 1.2 copy-start.7
  14.1 231.1 %all-reduce.2.cloned.1.call-start = ((), (), s32[]{:S(2)}) async-start(), calls=%async_computation.1 | async-start | bytes 2097152 | tf_op jit(solution)/shard_map/psum | solution.py:108
  180.9 1.2 copy-start.5
  180.9 2.4 copy-start.6
Sparse Core Ops, SparseCore 0:
  14.3 137.1 all-gather.1
  185.3 59.8 all-reduce.1
where the time goes:
time: 255 us; the launch traced here: 254 us
  waiting for transfers between devices  197 us (77%)
  local copies, waits for them, and re-layouts  23.5 us (9%)
  between operations  13.6 us (5%)
  loops' own time  11.2 us (4%)
  matrix products  6.91 us (3%)
    all_gather x1, waiting for transfers between devices, shards(): kv_piece = lax.all_gather(key_values, 'sp', axis=0, tiled=True)  137 us
    psum x1, waiting for transfers between devices, shards(): result = lax.psum(partial_value.astype(jnp.bfloat16), 'tp')  60 us
    another operation x1, loops' own time, shards(): lax.scan(absorb_step, softmax_state, (stacked, jnp.arange(block_count, dt...  11 us
    reshape x1, local copies, waits for them, and re-layouts, shards(): stacked = kv_piece.reshape(block_count, block_rows, kv_piece.shape[1])  7.41 us
    unnamed x21, local copies, waits for them, and re-layouts  7.03 us
  transfers between devices with their start and end apart: 2, of which 2 were waited for; matrix products, arithmetic and copies ran while one was open for 0% of the time, Pallas kernels for 0%

commit v1 on v0

v1 whole, which is shorter than its diff:
```python
import functools
import math

import jax
import jax.numpy as jnp
from jax import lax
from jax.experimental import pallas as pl
from jax.experimental.pallas import tpu as pltpu
from jax.sharding import PartitionSpec as P

epsilon = 1e-06
masked_score = -1e30
log2_e = 1.4426950408889634
least_sum = 2.0**-90
most_sum = 2.0**100
lanes = 128
both = ("sp", "tp")


def cost(flops, moved, transcendentals=0):
    return pl.CostEstimate(
        flops=int(flops), bytes_accessed=int(moved), transcendentals=int(transcendentals)
    )


def in_vmem():
    return pl.BlockSpec(memory_space=pltpu.VMEM)


def in_smem():
    return pl.BlockSpec(memory_space=pltpu.SMEM)


def anywhere():
    return pl.BlockSpec(memory_space=pl.ANY)


def pair_up(first, second, heads):
    tiles = []
    low = lax.broadcasted_iota(jnp.int32, (first.shape[0], lanes), 1) < lanes // 2
    for pair in range(heads // 2):
        columns = slice(pair * lanes, (pair + 1) * lanes)
        rolled = pltpu.roll(second[:, columns], lanes // 2, 1)
        tiles.append(jnp.where(low, first[:, columns], rolled))
        tiles.append(jnp.where(low, rolled, first[:, columns]))
    return tiles


def key_value_kernel(heads, place, hidden, key_one, key_two, value_proj, *refs):
    outs, stage = refs[:heads], refs[heads]
    rows = hidden.shape[0]
    tokens = hidden[...]
    first = jnp.dot(tokens, key_one[...], preferred_element_type=jnp.float32)
    second = jnp.dot(tokens, key_two[...], preferred_element_type=jnp.float32)
    for head, tile in enumerate(pair_up(first, second, heads)):
        stage[head, :rows, :] = tile.astype(jnp.bfloat16)
    values = jnp.dot(tokens, value_proj[...], preferred_element_type=jnp.float32)
    for head in range(heads):
        turned = values[:, head * lanes : (head + 1) * lanes].T.astype(jnp.bfloat16)
        for part in range(rows // lanes):
            at = rows + part * lanes
            stage[head, at : at + lanes, :] = turned[:, part * lanes : (part + 1) * lanes]
    for turn in range(heads):
        outs[turn][...] = stage[lax.rem(place[0] + turn, heads)]


def query_kernel(heads, scale, place, hidden, query_one, query_two, *refs):
    outs, stage = refs[:heads], refs[heads]
    tokens = hidden[...]
    first = jnp.dot(tokens, query_one[...], preferred_element_type=jnp.float32)
    second = jnp.dot(tokens, query_two[...], preferred_element_type=jnp.float32)
    for head, tile in enumerate(pair_up(first, second, heads)):
        stage[head] = (tile * scale).astype(jnp.bfloat16)
    for turn in range(heads):
        outs[turn][...] = stage[lax.rem(place[0] + turn, heads)]


def attend_kernel(heads, groups, across, place, lam_mine, lam_other, gain, *refs):
    z, y, x, t = place[0], place[1], place[2], place[3]
    parts = groups * across
    query_in = refs[:heads]
    block_in = refs[heads : heads + heads * parts]
    outs = refs[heads + heads * parts : 2 * heads + heads * parts]
    queries, blocks, accum, sums, peak, done, flag, sems = refs[2 * heads + heads * parts :]
    rows = queries.shape[1]
    head_v = lanes

    copies = []
    for turn in range(heads):
        source = lax.rem(z + heads - turn, heads)
        copies.append(
            pltpu.make_async_copy(query_in[turn], queries.at[source], sems.at[len(copies)])
        )
    for group in range(groups):
        for side in range(across):
            for turn in range(heads):
                source = lax.rem(z + heads - turn, heads)
                block = (source * groups + lax.rem(t + group, groups)) * across
                block = block + lax.rem(x + side, across)
                index = (group * across + side) * heads + turn
                copies.append(
                    pltpu.make_async_copy(block_in[index], blocks.at[block], sems.at[len(copies)])
                )
    for copy in copies:
        copy.start()
    for copy in copies:
        copy.wait()

    mine = t * across + x
    odd = lax.rem(z, 2) == 1
    lam = jnp.where(y == t, lam_mine[z], lam_other[z])
    weight_low = jnp.where(odd, -lam, 1.0)
    weight_high = jnp.where(odd, 1.0, -lam)
    lane = lax.broadcasted_iota(jnp.int32, (1, lanes), 1)
    low = jnp.where(lane < lanes // 2, 1.0, 0.0).astype(jnp.bfloat16)
    high = jnp.where(lane < lanes // 2, 0.0, 1.0).astype(jnp.bfloat16)
    width = 2 * rows
    key_row = lax.broadcasted_iota(jnp.int32, (rows, width), 0)
    query_col = lax.broadcasted_iota(jnp.int32, (rows, width), 1)
    ahead = key_row - jnp.where(query_col < rows, query_col, query_col - rows)

    def scores_of(block, two_maps):
        return lax.dot_general(
            blocks[block, :rows, :],
            two_maps,
            (((1,), (1,)), ((), ())),
            preferred_element_type=jnp.float32,
        )

    def values_of(block):
        pieces = [
            blocks[block, rows + p * lanes : rows + (p + 1) * lanes, :]
            for p in range(rows // lanes)
        ]
        return jnp.concatenate(pieces, axis=1)

    def fold(weights):
        return jnp.sum(weights.reshape(rows // 8, 8, width), axis=0)

    def stripe(first, two_maps, masked):
        added = jnp.zeros((head_v, width), jnp.float32)
        total = jnp.zeros((8, width), jnp.float32)
        for part in range(parts):
            block = first + part
            weights = jnp.exp2(scores_of(block, two_maps))
            if masked:
                weights = jnp.where(ahead <= (mine - part) * rows, weights, 0.0)
            total = total + fold(weights)
            added = added + jnp.dot(
                values_of(block),
                weights.astype(jnp.bfloat16),
                preferred_element_type=jnp.float32,
            )
        return added, total

    def finish(index):
        total = jnp.sum(sums[...], axis=0, keepdims=True)
        heads_out = accum[...] * (1.0 / total)
        mixed = heads_out[:, :rows] * weight_low + heads_out[:, rows:] * weight_high
        scale = lax.rsqrt(jnp.mean(mixed * mixed, axis=0, keepdims=True) + epsilon)
        done[index] = ((mixed * scale).T * gain[...]).astype(jnp.bfloat16)
        return total

    def two_maps_of(index):
        chosen = queries[index]
        return jnp.concatenate([chosen * low, chosen * high], axis=0)

    flag[...] = jnp.zeros_like(flag)

    def one_stripe(index, carried):
        two_maps = two_maps_of(index)
        added, total = stripe(index * parts, two_maps, True)
        accum[...] = added
        sums[...] = total

        def earlier(before, inner):
            more, weight = stripe(before * parts, two_maps, False)
            accum[...] += more
            sums[...] += weight
            return inner

        lax.fori_loop(0, index, earlier, 0)
        total = finish(index)
        inside = (total >= least_sum) & (total <= most_sum)
        flag[...] = jnp.maximum(flag[...], jnp.where(inside, 0.0, 1.0))
        return carried

    lax.fori_loop(0, heads, one_stripe, 0)

    @pl.when(jnp.max(flag[...]) > 0.0)
    def _():
        def redo(index, carried):
            two_maps = two_maps_of(index)
            accum[...] = jnp.zeros_like(accum)
            sums[...] = jnp.zeros_like(sums)
            peak[...] = jnp.full(peak.shape, masked_score, jnp.float32)

            def one_block(block, inner):
                allowed = ahead <= (index * parts + mine - block) * rows
                scores = jnp.where(allowed, scores_of(block, two_maps), masked_score)
                highest = jnp.maximum(peak[...], jnp.max(scores, axis=0, keepdims=True))
                rescale = jnp.exp2(peak[...] - highest)
                weights = jnp.where(allowed, jnp.exp2(scores - highest), 0.0)
                sums[...] = sums[...] * rescale + fold(weights)
                accum[...] = accum[...] * rescale + jnp.dot(
                    values_of(block),
                    weights.astype(jnp.bfloat16),
                    preferred_element_type=jnp.float32,
                )
                peak[...] = highest
                return inner

            lax.fori_loop(0, index * parts + mine + 1, one_block, 0)
            finish(index)
            return carried

        lax.fori_loop(0, heads, redo, 0)

    for turn in range(heads):
        outs[turn][...] = done[lax.rem(z + heads - turn, heads)]


def project_out_kernel(heads, place, *refs):
    mine, other = refs[:heads], refs[heads : 2 * heads]
    out_mine, out_other, result, joined = refs[2 * heads :]
    z = place[0]
    for turn in range(heads):
        at = pl.multiple_of(lax.rem(z + turn, heads) * lanes, lanes)
        joined[0, :, pl.ds(at, lanes)] = mine[turn][...]
        joined[1, :, pl.ds(at, lanes)] = other[turn][...]
    total = jnp.dot(joined[0], out_mine[...], preferred_element_type=jnp.float32)
    total = total + jnp.dot(joined[1], out_other[...], preferred_element_type=jnp.float32)
    result[...] = total.astype(jnp.bfloat16)


def exchanged(
    hidden_in, query_one, query_two, key_one, key_two, value_proj, lambdas, norm_gain, out_proj
):
    heads = lambdas.shape[0]
    groups = lax.axis_size("tp")
    across = lax.axis_size("sp") // (heads * groups)
    parts = groups * across
    rows, model = hidden_in.shape
    head_qk = query_one.shape[1] // heads
    scale = 1.75 * head_qk ** (-0.5) * log2_e
    bf16 = jnp.bfloat16

    sp_index = lax.axis_index("sp")
    z = sp_index // parts
    y = (sp_index // across) % groups
    x = sp_index % across
    t = lax.axis_index("tp")
    place = jnp.stack([z, y, x, t]).astype(jnp.int32)

    def line(zz, yy, xx, cc):
        return ((zz * groups + yy) * across + xx) * groups + cc

    def round_of(turn):
        pairs = []
        for zz in range(heads):
            for yy in range(groups):
                for xx in range(across):
                    for cc in range(groups):
                        pairs.append(
                            (line(zz, yy, xx, cc), line((zz + turn) % heads, cc, xx, yy))
                        )
        return pairs

    swap_core = [(i, (i + 1) % groups) for i in range(groups)]
    swap_side = [(i, i - i % across + (i + 1) % across) for i in range(heads * parts)]

    lam_other = lax.ppermute(lambdas, "tp", swap_core)
    out_other = lax.ppermute(out_proj, "tp", swap_core)

    block_rows = 2 * rows
    kv = pl.pallas_call(
        functools.partial(key_value_kernel, heads),
        out_shape=[jax.ShapeDtypeStruct((block_rows, lanes), bf16)] * heads,
        in_specs=[in_smem()] + [in_vmem()] * 4,
        out_specs=[in_vmem()] * heads,
        scratch_shapes=[pltpu.VMEM((heads, block_rows, lanes), bf16)],
        compiler_params=pltpu.CompilerParams(vmem_limit_bytes=24 << 20),
        cost_estimate=cost(2 * rows * model * 4 * heads * head_qk, 6 << 20),
        name="project_keys",
    )(place, hidden_in, key_one, key_two, value_proj)
    queries = pl.pallas_call(
        functools.partial(query_kernel, heads, scale),
        out_shape=[jax.ShapeDtypeStruct((rows, lanes), bf16)] * heads,
        in_specs=[in_smem()] + [in_vmem()] * 3,
        out_specs=[in_vmem()] * heads,
        scratch_shapes=[pltpu.VMEM((heads, rows, lanes), bf16)],
        compiler_params=pltpu.CompilerParams(vmem_limit_bytes=24 << 20),
        cost_estimate=cost(2 * rows * model * 2 * heads * head_qk, 4 << 20),
        name="project_queries",
    )(place, hidden_in, query_one, query_two)

    own = [lax.ppermute(kv[turn], both, round_of(turn)) for turn in range(heads)]
    moved_queries = [lax.ppermute(queries[turn], both, round_of(turn)) for turn in range(heads)]
    beside = [lax.ppermute(block, "sp", swap_side) for block in own]
    own_swapped = [lax.ppermute(block, "tp", swap_core) for block in own]
    beside_swapped = [lax.ppermute(block, "tp", swap_core) for block in beside]
    blocks = own + beside + own_swapped + beside_swapped

    tokens = heads * rows
    normed = pl.pallas_call(
        functools.partial(attend_kernel, heads, groups, across),
        out_shape=[jax.ShapeDtypeStruct((rows, lanes), bf16)] * heads,
        in_specs=[in_smem()] * 3 + [in_vmem()] + [anywhere()] * (heads + heads * parts),
        out_specs=[in_vmem()] * heads,
        scratch_shapes=[
            pltpu.VMEM((heads, rows, lanes), bf16),
            pltpu.VMEM((heads * parts, block_rows, lanes), bf16),
            pltpu.VMEM((lanes, 2 * rows), jnp.float32),
            pltpu.VMEM((8, 2 * rows), jnp.float32),
            pltpu.VMEM((1, 2 * rows), jnp.float32),
            pltpu.VMEM((heads, rows, lanes), bf16),
            pltpu.VMEM((1, 2 * rows), jnp.float32),
            pltpu.SemaphoreType.DMA((heads + heads * parts,)),
        ],
        compiler_params=pltpu.CompilerParams(vmem_limit_bytes=32 << 20),
        cost_estimate=cost(2 * 2 * tokens * tokens * parts * lanes, 3 << 20),
        name="attend",
    )(place, lambdas, lam_other, norm_gain.reshape(1, lanes), *queries_in(moved_queries), *blocks)

    back = []
    for turn in range(heads):
        back.append(lax.ppermute(normed[turn], both, [(b, a) for a, b in round_of(turn)]))
    back_other = [lax.ppermute(piece, "tp", swap_core) for piece in back]
    return pl.pallas_call(
        functools.partial(project_out_kernel, heads),
        out_shape=jax.ShapeDtypeStruct((rows, model), bf16),
        in_specs=[in_smem()] + [in_vmem()] * (2 * heads + 2),
        out_specs=in_vmem(),
        scratch_shapes=[pltpu.VMEM((groups, rows, heads * lanes), bf16)],
        compiler_params=pltpu.CompilerParams(vmem_limit_bytes=24 << 20),
        cost_estimate=cost(2 * rows * model * groups * heads * lanes, 6 << 20),
        name="project_out",
    )(place, *back, *back_other, out_proj, out_other)


def queries_in(arrays):
    return tuple(arrays)


def gathered(
    hidden_in, query_one, query_two, key_one, key_two, value_proj, lambdas, norm_gain, out_proj
):
    heads_dev = lambdas.shape[0]
    head_qk = query_one.shape[1] // heads_dev
    head_v = value_proj.shape[1] // heads_dev
    width_q = heads_dev * head_qk
    score_scale = 1.75 * head_qk ** (-0.5)
    joined = jnp.concatenate((query_one, query_two, key_one, key_two, value_proj), axis=1)
    projected = jnp.dot(hidden_in, joined, preferred_element_type=jnp.float32).astype(jnp.bfloat16)
    tok_rows = projected.shape[0]
    key_values = projected[:, 2 * width_q :]
    my_index = lax.axis_index("sp")
    positions = my_index * tok_rows + jnp.arange(tok_rows, dtype=jnp.int32)
    query_a = projected[:, :width_q].reshape(tok_rows, heads_dev, head_qk)
    query_b = projected[:, width_q : 2 * width_q].reshape(tok_rows, heads_dev, head_qk)
    last_pos = positions[tok_rows - 1]

    def one_map(queries, keys, value_rows, allowed, running_max, running_sum, accum):
        scores = (
            jnp.einsum("qhd,khd->hqk", queries, keys, preferred_element_type=jnp.float32)
            * score_scale
        )
        scores = jnp.where(allowed[None], scores, masked_score)
        new_max = jnp.maximum(running_max, jnp.max(scores, axis=-1))
        rescale = jnp.exp(running_max - new_max)
        weights = jnp.where(allowed[None], jnp.exp(scores - new_max[..., None]), 0.0)
        new_sum = running_sum * rescale + jnp.sum(weights, axis=-1)
        added = jnp.einsum(
            "hqk,khe->hqe",
            weights.astype(jnp.bfloat16),
            value_rows,
            preferred_element_type=jnp.float32,
        )
        return (new_max, new_sum, accum * rescale[..., None] + added)

    def absorb(state, kblock, kstart):
        block_rows = kblock.shape[0]
        k_pos = kstart + jnp.arange(block_rows, dtype=jnp.int32)
        allowed = k_pos[None, :] <= positions[:, None]
        keys_a = kblock[:, :width_q].reshape(block_rows, heads_dev, head_qk)
        keys_b = kblock[:, width_q : 2 * width_q].reshape(block_rows, heads_dev, head_qk)
        value_rows = kblock[:, 2 * width_q :].reshape(block_rows, heads_dev, head_v)
        first_map = one_map(query_a, keys_a, value_rows, allowed, *state[:3])
        second_map = one_map(query_b, keys_b, value_rows, allowed, *state[3:])
        return first_map + second_map

    start_max = jnp.full((heads_dev, tok_rows), masked_score, jnp.float32)
    start_sum = jnp.zeros((heads_dev, tok_rows), jnp.float32)
    start_acc = jnp.zeros((heads_dev, tok_rows, head_v), jnp.float32)
    state = (start_max, start_sum, start_acc, start_max, start_sum, start_acc)
    kv_piece = lax.all_gather(key_values, "sp", axis=0, tiled=True)
    piece_rows = kv_piece.shape[0]
    block_rows = math.gcd(piece_rows, 512)
    block_count = piece_rows // block_rows
    stacked = kv_piece.reshape(block_count, block_rows, kv_piece.shape[1])

    def absorb_step(carried, blocks_in):
        kblock, block_index = blocks_in
        kstart = block_index * block_rows
        renewed = lax.cond(
            kstart <= last_pos,
            lambda inner: absorb(inner, kblock, kstart),
            lambda inner: inner,
            carried,
        )
        return (renewed, None)

    state, _ = lax.scan(absorb_step, state, (stacked, jnp.arange(block_count, dtype=jnp.int32)))
    out_a = state[2] / state[1][..., None]
    out_b = state[5] / state[4][..., None]
    mixed_out = out_a - lambdas[:, None, None] * out_b
    scale_rows = lax.rsqrt(jnp.mean(mixed_out * mixed_out, axis=-1, keepdims=True) + epsilon)
    normed = (mixed_out * scale_rows * norm_gain).astype(jnp.bfloat16)
    normed_all = jnp.transpose(normed, (1, 0, 2)).reshape(tok_rows, heads_dev * head_v)
    partial_value = jnp.dot(normed_all, out_proj, preferred_element_type=jnp.float32)
    return lax.psum(partial_value.astype(jnp.bfloat16), "tp")


def shards(*args):
    hidden_in, query_one, value_proj, lambdas = args[0], args[1], args[5], args[6]
    heads = lambdas.shape[0]
    groups, length = lax.axis_size("tp"), lax.axis_size("sp")
    fits = (
        groups == 2
        and heads % 2 == 0
        and length == 2 * groups * heads
        and query_one.shape[1] == heads * (lanes // 2)
        and value_proj.shape[1] == heads * lanes
        and hidden_in.shape[0] % lanes == 0
        and hidden_in.shape[0] <= 512
    )
    return exchanged(*args) if fits else gathered(*args)


def solution(mesh):
    placed = (
        P("sp", None),
        P(None, "tp"),
        P(None, "tp"),
        P(None, "tp"),
        P(None, "tp"),
        P(None, "tp"),
        P("tp"),
        P(),
        P("tp", None),
    )
    return jax.shard_map(
        shards, mesh=mesh, in_specs=placed, out_specs=P("sp", None), check_vma=False
    )
```

time: 255 us -> 97.4 us (0.38)
  waiting for transfers between devices: 197 us -> 8.22 us
  starting transfers between devices: 0.04 us -> 45.8 us
  Pallas kernels: 0 us -> 36.7 us
  local copies, waits for them, and re-layouts: 23.5 us -> 4.92 us
  between operations: 13.6 us -> 0.11 us
  loops' own time: 11.2 us -> 0 us
  matrix products: 6.91 us -> 0 us
    all_gather x1 -> x0, waiting for transfers between devices: 137 us -> none  [shards(): kv_piece = lax.all_gather(key_values, 'sp', axis=0, tiled=True)]
    psum x1 -> x0, waiting for transfers between devices: 60 us -> none  [shards(): result = lax.psum(partial_value.astype(jnp.bfloat16), 'tp')]
    ppermute x0 -> x30, starting transfers between devices: none -> 45.8 us  [the longest x4 12.4 us: exchanged(): back_other = [lax.ppermute(piece, 'tp', swap_core) for piece in back]]
    pallas_call x0 -> x4, Pallas kernels: none -> 36.7 us  [the longest x1 30.5 us: exchanged(): pl.pallas_call(functools.partial(attend_kernel, heads, groups, across), o...]
    another operation x9 -> x0, loops' own time: 11.2 us -> none  [the longest x1 11 us: shards(): lax.scan(absorb_step, softmax_state, (stacked, jnp.arange(block_count, dt...]
    ppermute x0 -> x30, waiting for transfers between devices: none -> 8.22 us  [the longest x4 5.94 us: exchanged(): beside = [lax.ppermute(block, 'sp', swap_side) for block in own]]
    reshape x1 -> x0, local copies, waits for them, and re-layouts: 7.41 us -> none  [shards(): stacked = kv_piece.reshape(block_count, block_rows, kv_piece.shape[1])]
    dot_general x6 -> x0, matrix products: 6.91 us -> none  [the longest x2 2.14 us: one_map(): jnp.einsum('hqk,khe->hqe', weights.astype(jnp.bfloat16), value_rows, pref...]
  transfers between devices with their start and end apart: 2 -> 30, of which waited for: 2 -> 5; matrix products, arithmetic and copies ran while one was open for 0% -> 0% of each run, Pallas kernels for 0% -> 35%
where the time goes in v1:
time: 97.4 us; the launch traced here: 95.8 us
  starting transfers between devices  45.8 us (47%)
  Pallas kernels  36.7 us (38%)
  waiting for transfers between devices  8.22 us (8%)
  local copies, waits for them, and re-layouts  4.92 us (5%)
    pallas_call x1, Pallas kernels, exchanged(): pl.pallas_call(functools.partial(attend_kernel, heads, groups, across), o...  30.5 us
    ppermute x4, starting transfers between devices, exchanged(): back_other = [lax.ppermute(piece, 'tp', swap_core) for piece in back]  12.4 us
    ppermute x4, starting transfers between devices, exchanged(): own_swapped = [lax.ppermute(block, 'tp', swap_core) for block in own]  10.7 us
    ppermute x4, starting transfers between devices, exchanged(): lax.ppermute(queries[turn], both, round_of(turn))  7.71 us
    ppermute x4, waiting for transfers between devices, exchanged(): beside = [lax.ppermute(block, 'sp', swap_side) for block in own]  5.94 us
    ppermute x4, starting transfers between devices, exchanged(): beside = [lax.ppermute(block, 'sp', swap_side) for block in own]  5.22 us
    unnamed x18, local copies, waits for them, and re-layouts  4.92 us
    ppermute x4, starting transfers between devices, exchanged(): lax.ppermute(kv[turn], both, round_of(turn))  4.6 us
  transfers between devices with their start and end apart: 30, of which 5 were waited for; matrix products, arithmetic and copies ran while one was open for 0% of the time, Pallas kernels for 35%

profile of v1, /device:TPU:0, one launch (start us, length us, event | category | flops | bytes accessed | tf_op | source)
XLA Modules:
  0.0 95.8 jit_solution(936952934733862559)
XLA Ops:
  0.6 1.2 %copy-done = bf16[256,2048]{1,0:T(8,128)(2,1)S(1)} copy-done((bf16[256,2048]{1,0:T(8,128)(2,1)S(1)}, bf16[256,2048]{1,0:T(8,128)(2,1)}, u32[]{:S(2)}) %copy-start) | copy-done | bytes 1048600
  1.8 1.2 %copy-done.3 = bf16[2048,256]{1,0:T(8,128)(2,1)S(1)} copy-done((bf16[2048,256]{1,0:T(8,128)(2,1)S(1)}, bf16[2048,256]{1,0:T(8,128)(2,1)}, u32[]{:S(2)}) %copy-start.3) | copy-done | bytes 1048600
  3.0 1.2 %copy-done.4 = bf16[2048,256]{1,0:T(8,128)(2,1)S(1)} copy-done((bf16[2048,256]{1,0:T(8,128)(2,1)S(1)}, bf16[2048,256]{1,0:T(8,128)(2,1)}, u32[]{:S(2)}) %copy-start.4) | copy-done | bytes 1048600
  4.3 1.4 %project_queries.1 = (bf16[256,128]{1,0:T(8,128)(2,1)S(1)}, bf16[256,128]{1,0:T(8,128)(2,1)S(1)}, bf16[256,128]{1,0:T(8,128)(2,1)S(1)}, bf16[256,128]{1,0:T(8,128)(2,1)S(1)}) custom-call(s32[4]{0:T(128)S(1)} %pad_add_fusion.place, bf16[256,2048]{1,0:T(8,128)(2,1)S(1)} %copy-done, bf16[2048,256]{1,0:T(8,128)(2,1)S(1)} %copy-done.3, ...), custom_call_target="tpu_custom_call" | custom-call | flops 536870912 | bytes 4194304 | tf_op jit(solution)/shard_map/project_queries/pallas_call | solution.py:286
  5.6 0.7 collective-permute-start.1
  6.3 3.1 %collective-permute-start.2 = (bf16[256,128]{1,0:T(8,128)(2,1)S(1)}, bf16[256,128]{1,0:T(8,128)(2,1)S(1)}, u32[]{:S(2)}, u32[]{:S(2)}) collective-permute-start(bf16[256,128]{1,0:T(8,128)(2,1)S(1)} %get-tuple-element.18), channel_id=1, source_target_pairs={{0,8},{1,12},{2,10},{3,14},{4,9},{5,13},{6,11},{7,15},{8,16},{9,20... | collective-permute-start | bytes 196616 | tf_op jit(solution)/shard_map/ppermute | solution.py:298
  9.4 2.6 %collective-permute-start.3 = (bf16[256,128]{1,0:T(8,128)(2,1)S(1)}, bf16[256,128]{1,0:T(8,128)(2,1)S(1)}, u32[]{:S(2)}, u32[]{:S(2)}) collective-permute-start(bf16[256,128]{1,0:T(8,128)(2,1)S(1)} %get-tuple-element.19), channel_id=1, source_target_pairs={{0,16},{1,20},{2,18},{3,22},{4,17},{5,21},{6,19},{7,23},{8,24},{9,... | collective-permute-start | bytes 196616 | tf_op jit(solution)/shard_map/ppermute | solution.py:298
  12.0 1.3 %collective-permute-start.4 = (bf16[256,128]{1,0:T(8,128)(2,1)S(1)}, bf16[256,128]{1,0:T(8,128)(2,1)S(1)}, u32[]{:S(2)}, u32[]{:S(2)}) collective-permute-start(bf16[256,128]{1,0:T(8,128)(2,1)S(1)} %get-tuple-element.20), channel_id=1, source_target_pairs={{0,24},{1,28},{2,26},{3,30},{4,25},{5,29},{6,27},{7,31},{8,0},{9,4... | collective-permute-start | bytes 196616 | tf_op jit(solution)/shard_map/ppermute | solution.py:298
  13.4 1.2 %copy-done.6 = bf16[2048,256]{1,0:T(8,128)(2,1)S(1)} copy-done((bf16[2048,256]{1,0:T(8,128)(2,1)S(1)}, bf16[2048,256]{1,0:T(8,128)(2,1)}, u32[]{:S(2)}) %copy-start.6) | copy-done | bytes 1048600
  14.6 2.0 %project_keys.1 = (bf16[512,128]{1,0:T(8,128)(2,1)S(1)}, bf16[512,128]{1,0:T(8,128)(2,1)S(1)}, bf16[512,128]{1,0:T(8,128)(2,1)S(1)}, bf16[512,128]{1,0:T(8,128)(2,1)S(1)}) custom-call(s32[4]{0:T(128)S(1)} %pad_add_fusion.place, bf16[256,2048]{1,0:T(8,128)(2,1)S(1)} %copy-done, bf16[2048,256]{1,0:T(8,128)(2,1)S(1)} %copy-done.5, ...), custom_call_target="tpu_custom_call" | custom-call | flops 1073741824 | bytes 6291456 | tf_op jit(solution)/shard_map/project_keys/pallas_call | solution.py:276
  16.6 0.7 collective-permute-start.5
  17.3 0.7 collective-permute-start.6
  18.4 2.8 %collective-permute-start.8 = (bf16[512,128]{1,0:T(8,128)(2,1)S(1)}, bf16[512,128]{1,0:T(8,128)(2,1)S(1)}, u32[]{:S(2)}, u32[]{:S(2)}) collective-permute-start(bf16[512,128]{1,0:T(8,128)(2,1)S(1)} %get-tuple-element.24), channel_id=1, source_target_pairs={{0,24},{1,28},{2,26},{3,30},{4,25},{5,29},{6,27},{7,31},{8,0},{9,4... | collective-permute-start | bytes 393224 | tf_op jit(solution)/shard_map/ppermute | solution.py:297
  21.2 6.5 %collective-permute-start.13 = (bf16[512,128]{1,0:T(8,128)(2,1)S(1)}, bf16[512,128]{1,0:T(8,128)(2,1)S(1)}, u32[]{:S(2)}, u32[]{:S(2)}) collective-permute-start(bf16[512,128]{1,0:T(8,128)(2,1)S(1)} %collective-permute-done.5.refs_4_), channel_id=1, source_target_pairs={{0,1},{1,0},{2,3},{3,2},{4,5},{5,4},{6,7},{7,6},{8,9},{9,8},{10,11... | collective-permute-start | bytes 393224 | tf_op jit(solution)/shard_map/ppermute | solution.py:300
  27.8 1.5 %collective-permute-start.9 = (bf16[512,128]{1,0:T(8,128)(2,1)S(1)}, bf16[512,128]{1,0:T(8,128)(2,1)S(1)}, u32[]{:S(2)}, u32[]{:S(2)}) collective-permute-start(bf16[512,128]{1,0:T(8,128)(2,1)S(1)} %collective-permute-done.5.refs_4_), channel_id=1, source_target_pairs={{0,2},{2,0},{4,6},{6,4},{8,10},{10,8},{12,14},{14,12},{16,18},{18,... | collective-permute-start | bytes 393224 | tf_op jit(solution)/shard_map/ppermute | solution.py:299
  29.3 3.2 %collective-permute-start.14 = (bf16[512,128]{1,0:T(8,128)(2,1)S(1)}, bf16[512,128]{1,0:T(8,128)(2,1)S(1)}, u32[]{:S(2)}, u32[]{:S(2)}) collective-permute-start(bf16[512,128]{1,0:T(8,128)(2,1)S(1)} %collective-permute-done.6.refs_5_), channel_id=1, source_target_pairs={{0,1},{1,0},{2,3},{3,2},{4,5},{5,4},{6,7},{7,6},{8,9},{9,8},{10,11... | collective-permute-start | bytes 393224 | tf_op jit(solution)/shard_map/ppermute | solution.py:300
  32.5 1.5 %collective-permute-start.10 = (bf16[512,128]{1,0:T(8,128)(2,1)S(1)}, bf16[512,128]{1,0:T(8,128)(2,1)S(1)}, u32[]{:S(2)}, u32[]{:S(2)}) collective-permute-start(bf16[512,128]{1,0:T(8,128)(2,1)S(1)} %collective-permute-done.6.refs_5_), channel_id=1, source_target_pairs={{0,2},{2,0},{4,6},{6,4},{8,10},{10,8},{12,14},{14,12},{16,18},{18,... | collective-permute-start | bytes 393224 | tf_op jit(solution)/shard_map/ppermute | solution.py:299
  34.6 1.0 %collective-permute-start.16 = (bf16[512,128]{1,0:T(8,128)(2,1)S(1)}, bf16[512,128]{1,0:T(8,128)(2,1)S(1)}, u32[]{:S(2)}, u32[]{:S(2)}) collective-permute-start(bf16[512,128]{1,0:T(8,128)(2,1)S(1)} %collective-permute-done.8.refs_7_), channel_id=1, source_target_pairs={{0,1},{1,0},{2,3},{3,2},{4,5},{5,4},{6,7},{7,6},{8,9},{9,8},{10,11... | collective-permute-start | bytes 393224 | tf_op jit(solution)/shard_map/ppermute | solution.py:300
  35.6 3.1 %collective-permute-done.10.refs_9_ = bf16[512,128]{1,0:T(8,128)(2,1)S(1)} collective-permute-done((bf16[512,128]{1,0:T(8,128)(2,1)S(1)}, bf16[512,128]{1,0:T(8,128)(2,1)S(1)}, u32[]{:S(2)}, u32[]{:S(2)}) %collective-permute-start.10) | collective-permute-done | bytes 131104 | tf_op jit(solution)/shard_map/ppermute | solution.py:299
  38.7 1.6 %collective-permute-start.12 = (bf16[512,128]{1,0:T(8,128)(2,1)S(1)}, bf16[512,128]{1,0:T(8,128)(2,1)S(1)}, u32[]{:S(2)}, u32[]{:S(2)}) collective-permute-start(bf16[512,128]{1,0:T(8,128)(2,1)S(1)} %collective-permute-done.8.refs_7_), channel_id=1, source_target_pairs={{0,2},{2,0},{4,6},{6,4},{8,10},{10,8},{12,14},{14,12},{16,18},{18,... | collective-permute-start | bytes 393224 | tf_op jit(solution)/shard_map/ppermute | solution.py:299
  40.3 1.2 %collective-permute-done.11.refs_10_ = bf16[512,128]{1,0:T(8,128)(2,1)S(1)} collective-permute-done((bf16[512,128]{1,0:T(8,128)(2,1)S(1)}, bf16[512,128]{1,0:T(8,128)(2,1)S(1)}, u32[]{:S(2)}, u32[]{:S(2)}) %collective-permute-start.11) | collective-permute-done | bytes 131104 | tf_op jit(solution)/shard_map/ppermute | solution.py:299
  42.0 1.6 %collective-permute-done.12.refs_11_ = bf16[512,128]{1,0:T(8,128)(2,1)S(1)} collective-permute-done((bf16[512,128]{1,0:T(8,128)(2,1)S(1)}, bf16[512,128]{1,0:T(8,128)(2,1)S(1)}, u32[]{:S(2)}, u32[]{:S(2)}) %collective-permute-start.12) | collective-permute-done | bytes 131104 | tf_op jit(solution)/shard_map/ppermute | solution.py:299
  43.7 1.3 %collective-permute-done.20.refs_19_ = bf16[512,128]{1,0:T(8,128)(2,1)S(1)} collective-permute-done((bf16[512,128]{1,0:T(8,128)(2,1)S(1)}, bf16[512,128]{1,0:T(8,128)(2,1)S(1)}, u32[]{:S(2)}, u32[]{:S(2)}) %collective-permute-start.20) | collective-permute-done | bytes 131104 | tf_op jit(solution)/shard_map/ppermute | solution.py:301
  45.0 30.5 %attend.1 = (bf16[256,128]{1,0:T(8,128)(2,1)S(1)}, bf16[256,128]{1,0:T(8,128)(2,1)S(1)}, bf16[256,128]{1,0:T(8,128)(2,1)S(1)}, bf16[256,128]{1,0:T(8,128)(2,1)S(1)}) custom-call(s32[4]{0:T(128)S(1)} %pad_add_fusion.place, f32[4]{0:T(128)S(1)} %copy-done.7, f32[4]{0:T(128)S(1)} %collective-permute-done.lam_other, f32[1,128]{1,0:T(1,128)S(1)} %bitcast.5, ...), custom_call_target="tpu_custom_call" | custom-call | flops 2147483648 | bytes 3145728 | tf_op jit(solution)/shard_map/attend/pallas_call | solution.py:305
  75.5 0.7 collective-permute-start.21
  76.2 2.8 %collective-permute-start.22 = (bf16[256,128]{1,0:T(8,128)(2,1)S(1)}, bf16[256,128]{1,0:T(8,128)(2,1)S(1)}, u32[]{:S(2)}, u32[]{:S(2)}) collective-permute-start(bf16[256,128]{1,0:T(8,128)(2,1)S(1)} %get-tuple-element.26), channel_id=1, source_target_pairs={{8,0},{12,1},{10,2},{14,3},{9,4},{13,5},{11,6},{15,7},{16,8},{20,9... | collective-permute-start | bytes 196616 | tf_op jit(solution)/shard_map/ppermute | solution.py:327
  79.6 6.2 %collective-permute-start.25 = (bf16[256,128]{1,0:T(8,128)(2,1)S(1)}, bf16[256,128]{1,0:T(8,128)(2,1)S(1)}, u32[]{:S(2)}, u32[]{:S(2)}) collective-permute-start(bf16[256,128]{1,0:T(8,128)(2,1)S(1)} %collective-permute-done.21.refs_0_), channel_id=1, source_target_pairs={{0,1},{1,0},{2,3},{3,2},{4,5},{5,4},{6,7},{7,6},{8,9},{9,8},{10,11... | collective-permute-start | bytes 196616 | tf_op jit(solution)/shard_map/ppermute | solution.py:328
  85.8 1.1 %collective-permute-start.26 = (bf16[256,128]{1,0:T(8,128)(2,1)S(1)}, bf16[256,128]{1,0:T(8,128)(2,1)S(1)}, u32[]{:S(2)}, u32[]{:S(2)}) collective-permute-start(bf16[256,128]{1,0:T(8,128)(2,1)S(1)} %collective-permute-done.22.refs_1_), channel_id=1, source_target_pairs={{0,1},{1,0},{2,3},{3,2},{4,5},{5,4},{6,7},{7,6},{8,9},{9,8},{10,11... | collective-permute-start | bytes 196616 | tf_op jit(solution)/shard_map/ppermute | solution.py:328
  87.0 4.2 %collective-permute-start.27 = (bf16[256,128]{1,0:T(8,128)(2,1)S(1)}, bf16[256,128]{1,0:T(8,128)(2,1)S(1)}, u32[]{:S(2)}, u32[]{:S(2)}) collective-permute-start(bf16[256,128]{1,0:T(8,128)(2,1)S(1)} %collective-permute-done.23.refs_2_), channel_id=1, source_target_pairs={{0,1},{1,0},{2,3},{3,2},{4,5},{5,4},{6,7},{7,6},{8,9},{9,8},{10,11... | collective-permute-start | bytes 196616 | tf_op jit(solution)/shard_map/ppermute | solution.py:328
  91.1 0.9 collective-permute-start.28
  92.1 0.9 collective-permute-done.28.refs_7_
  92.9 2.9 %project_out.1 = bf16[256,2048]{1,0:T(8,128)(2,1)} custom-call(s32[4]{0:T(128)S(1)} %pad_add_fusion.place, bf16[256,128]{1,0:T(8,128)(2,1)S(1)} %collective-permute-done.21.refs_0_, bf16[256,128]{1,0:T(8,128)(2,1)S(1)} %collective-permute-done.22.refs_1_, bf16[256,128]{1,0:T(8,128)(2,1)S(1)} %collective-permute-done.23.refs_2_, ...), custom_call_target="tpu_custom_call" | custom-call | flops 1073741824 | bytes 6291456 | tf_op jit(solution)/shard_map/project_out/pallas_call | solution.py:329
  (51 shorter events, 2.8 us)
Async XLA Ops:
  0.0 92.9 %collective-permute-start.29 = (bf16[512,2048]{1,0:T(8,128)(2,1)}, bf16[512,2048]{1,0:T(8,128)(2,1)S(1)}, u32[]{:S(2)}, u32[]{:S(2)}) collective-permute-start(bf16[512,2048]{1,0:T(8,128)(2,1)} %refs_8_.1), channel_id=1, source_target_pairs={{0,1},{1,0},{2,3},{3,2},{4,5},{5,4},{6,7},{7,6},{8,9},{9,8},{10,11... | collective-permute-start | bytes 6291464 | tf_op jit(solution)/shard_map/ppermute | solution.py:273
  0.5 11.5 %collective-permute-start = (f32[4]{0:T(128)}, f32[4]{0:T(128)S(1)}, u32[]{:S(2)}, u32[]{:S(2)}) collective-permute-start(f32[4]{0:T(128)} %lam_mine.1), channel_id=1, source_target_pairs={{0,1},{1,0},{2,3},{3,2},{4,5},{5,4},{6,7},{7,6},{8,9},{9,8},{10,11... | collective-permute-start | bytes 56 | tf_op jit(solution)/shard_map/ppermute | solution.py:272
  5.6 10.9 %collective-permute-start.1 = (bf16[256,128]{1,0:T(8,128)(2,1)S(1)}, bf16[256,128]{1,0:T(8,128)(2,1)S(1)}, u32[]{:S(2)}, u32[]{:S(2)}) collective-permute-start(bf16[256,128]{1,0:T(8,128)(2,1)S(1)} %get-tuple-element.17), channel_id=1, source_target_pairs={{0,0},{1,4},{2,2},{3,6},{4,1},{5,5},{6,3},{7,7},{8,8},{9,12},{10,1... | collective-permute-start | bytes 196616 | tf_op jit(solution)/shard_map/ppermute | solution.py:298
  6.3 11.0 %collective-permute-start.2 = (bf16[256,128]{1,0:T(8,128)(2,1)S(1)}, bf16[256,128]{1,0:T(8,128)(2,1)S(1)}, u32[]{:S(2)}, u32[]{:S(2)}) collective-permute-start(bf16[256,128]{1,0:T(8,128)(2,1)S(1)} %get-tuple-element.18), channel_id=1, source_target_pairs={{0,8},{1,12},{2,10},{3,14},{4,9},{5,13},{6,11},{7,15},{8,16},{9,20... | collective-permute-start | bytes 196616 | tf_op jit(solution)/shard_map/ppermute | solution.py:298
  9.4 8.6 %collective-permute-start.3 = (bf16[256,128]{1,0:T(8,128)(2,1)S(1)}, bf16[256,128]{1,0:T(8,128)(2,1)S(1)}, u32[]{:S(2)}, u32[]{:S(2)}) collective-permute-start(bf16[256,128]{1,0:T(8,128)(2,1)S(1)} %get-tuple-element.19), channel_id=1, source_target_pairs={{0,16},{1,20},{2,18},{3,22},{4,17},{5,21},{6,19},{7,23},{8,24},{9,... | collective-permute-start | bytes 196616 | tf_op jit(solution)/shard_map/ppermute | solution.py:298
  12.0 6.4 %collective-permute-start.4 = (bf16[256,128]{1,0:T(8,128)(2,1)S(1)}, bf16[256,128]{1,0:T(8,128)(2,1)S(1)}, u32[]{:S(2)}, u32[]{:S(2)}) collective-permute-start(bf16[256,128]{1,0:T(8,128)(2,1)S(1)} %get-tuple-element.20), channel_id=1, source_target_pairs={{0,24},{1,28},{2,26},{3,30},{4,25},{5,29},{6,27},{7,31},{8,0},{9,4... | collective-permute-start | bytes 196616 | tf_op jit(solution)/shard_map/ppermute | solution.py:298
  14.6 30.4 %copy-start.8 = (f32[128]{0:T(128)S(1)}, f32[128]{0:T(128)}, u32[]{:S(2)}) copy-start(f32[128]{0:T(128)} %param.16) | copy-start | bytes 1540
  16.6 4.6 %collective-permute-start.5 = (bf16[512,128]{1,0:T(8,128)(2,1)S(1)}, bf16[512,128]{1,0:T(8,128)(2,1)S(1)}, u32[]{:S(2)}, u32[]{:S(2)}) collective-permute-start(bf16[512,128]{1,0:T(8,128)(2,1)S(1)} %get-tuple-element.21), channel_id=1, source_target_pairs={{0,0},{1,4},{2,2},{3,6},{4,1},{5,5},{6,3},{7,7},{8,8},{9,12},{10,1... | collective-permute-start | bytes 393224 | tf_op jit(solution)/shard_map/ppermute | solution.py:297
  17.3 10.5 %collective-permute-start.6 = (bf16[512,128]{1,0:T(8,128)(2,1)S(1)}, bf16[512,128]{1,0:T(8,128)(2,1)S(1)}, u32[]{:S(2)}, u32[]{:S(2)}) collective-permute-start(bf16[512,128]{1,0:T(8,128)(2,1)S(1)} %get-tuple-element.22), channel_id=1, source_target_pairs={{0,8},{1,12},{2,10},{3,14},{4,9},{5,13},{6,11},{7,15},{8,16},{9,20... | collective-permute-start | bytes 393224 | tf_op jit(solution)/shard_map/ppermute | solution.py:297
  18.0 11.2 %collective-permute-start.7 = (bf16[512,128]{1,0:T(8,128)(2,1)S(1)}, bf16[512,128]{1,0:T(8,128)(2,1)S(1)}, u32[]{:S(2)}, u32[]{:S(2)}) collective-permute-start(bf16[512,128]{1,0:T(8,128)(2,1)S(1)} %get-tuple-element.23), channel_id=1, source_target_pairs={{0,16},{1,20},{2,18},{3,22},{4,17},{5,21},{6,19},{7,23},{8,24},{9,... | collective-permute-start | bytes 393224 | tf_op jit(solution)/shard_map/ppermute | solution.py:297
  18.4 14.1 %collective-permute-start.8 = (bf16[512,128]{1,0:T(8,128)(2,1)S(1)}, bf16[512,128]{1,0:T(8,128)(2,1)S(1)}, u32[]{:S(2)}, u32[]{:S(2)}) collective-permute-start(bf16[512,128]{1,0:T(8,128)(2,1)S(1)} %get-tuple-element.24), channel_id=1, source_target_pairs={{0,24},{1,28},{2,26},{3,30},{4,25},{5,29},{6,27},{7,31},{8,0},{9,4... | collective-permute-start | bytes 393224 | tf_op jit(solution)/shard_map/ppermute | solution.py:297
  21.2 12.8 %collective-permute-start.13 = (bf16[512,128]{1,0:T(8,128)(2,1)S(1)}, bf16[512,128]{1,0:T(8,128)(2,1)S(1)}, u32[]{:S(2)}, u32[]{:S(2)}) collective-permute-start(bf16[512,128]{1,0:T(8,128)(2,1)S(1)} %collective-permute-done.5.refs_4_), channel_id=1, source_target_pairs={{0,1},{1,0},{2,3},{3,2},{4,5},{5,4},{6,7},{7,6},{8,9},{9,8},{10,11... | collective-permute-start | bytes 393224 | tf_op jit(solution)/shard_map/ppermute | solution.py:300
  27.8 6.2 %collective-permute-start.9 = (bf16[512,128]{1,0:T(8,128)(2,1)S(1)}, bf16[512,128]{1,0:T(8,128)(2,1)S(1)}, u32[]{:S(2)}, u32[]{:S(2)}) collective-permute-start(bf16[512,128]{1,0:T(8,128)(2,1)S(1)} %collective-permute-done.5.refs_4_), channel_id=1, source_target_pairs={{0,2},{2,0},{4,6},{6,4},{8,10},{10,8},{12,14},{14,12},{16,18},{18,... | collective-permute-start | bytes 393224 | tf_op jit(solution)/shard_map/ppermute | solution.py:299
  29.3 5.3 %collective-permute-start.14 = (bf16[512,128]{1,0:T(8,128)(2,1)S(1)}, bf16[512,128]{1,0:T(8,128)(2,1)S(1)}, u32[]{:S(2)}, u32[]{:S(2)}) collective-permute-start(bf16[512,128]{1,0:T(8,128)(2,1)S(1)} %collective-permute-done.6.refs_5_), channel_id=1, source_target_pairs={{0,1},{1,0},{2,3},{3,2},{4,5},{5,4},{6,7},{7,6},{8,9},{9,8},{10,11... | collective-permute-start | bytes 393224 | tf_op jit(solution)/shard_map/ppermute | solution.py:300
  32.5 6.2 %collective-permute-start.10 = (bf16[512,128]{1,0:T(8,128)(2,1)S(1)}, bf16[512,128]{1,0:T(8,128)(2,1)S(1)}, u32[]{:S(2)}, u32[]{:S(2)}) collective-permute-start(bf16[512,128]{1,0:T(8,128)(2,1)S(1)} %collective-permute-done.6.refs_5_), channel_id=1, source_target_pairs={{0,2},{2,0},{4,6},{6,4},{8,10},{10,8},{12,14},{14,12},{16,18},{18,... | collective-permute-start | bytes 393224 | tf_op jit(solution)/shard_map/ppermute | solution.py:299
  34.0 6.4 %collective-permute-start.15 = (bf16[512,128]{1,0:T(8,128)(2,1)S(1)}, bf16[512,128]{1,0:T(8,128)(2,1)S(1)}, u32[]{:S(2)}, u32[]{:S(2)}) collective-permute-start(bf16[512,128]{1,0:T(8,128)(2,1)S(1)} %collective-permute-done.7.refs_6_), channel_id=1, source_target_pairs={{0,1},{1,0},{2,3},{3,2},{4,5},{5,4},{6,7},{7,6},{8,9},{9,8},{10,11... | collective-permute-start | bytes 393224 | tf_op jit(solution)/shard_map/ppermute | solution.py:300
  34.0 7.5 %collective-permute-start.11 = (bf16[512,128]{1,0:T(8,128)(2,1)S(1)}, bf16[512,128]{1,0:T(8,128)(2,1)S(1)}, u32[]{:S(2)}, u32[]{:S(2)}) collective-permute-start(bf16[512,128]{1,0:T(8,128)(2,1)S(1)} %collective-permute-done.7.refs_6_), channel_id=1, source_target_pairs={{0,2},{2,0},{4,6},{6,4},{8,10},{10,8},{12,14},{14,12},{16,18},{18,... | collective-permute-start | bytes 393224 | tf_op jit(solution)/shard_map/ppermute | solution.py:299
  34.6 6.9 %collective-permute-start.16 = (bf16[512,128]{1,0:T(8,128)(2,1)S(1)}, bf16[512,128]{1,0:T(8,128)(2,1)S(1)}, u32[]{:S(2)}, u32[]{:S(2)}) collective-permute-start(bf16[512,128]{1,0:T(8,128)(2,1)S(1)} %collective-permute-done.8.refs_7_), channel_id=1, source_target_pairs={{0,1},{1,0},{2,3},{3,2},{4,5},{5,4},{6,7},{7,6},{8,9},{9,8},{10,11... | collective-permute-start | bytes 393224 | tf_op jit(solution)/shard_map/ppermute | solution.py:300
  38.7 5.0 %collective-permute-start.12 = (bf16[512,128]{1,0:T(8,128)(2,1)S(1)}, bf16[512,128]{1,0:T(8,128)(2,1)S(1)}, u32[]{:S(2)}, u32[]{:S(2)}) collective-permute-start(bf16[512,128]{1,0:T(8,128)(2,1)S(1)} %collective-permute-done.8.refs_7_), channel_id=1, source_target_pairs={{0,2},{2,0},{4,6},{6,4},{8,10},{10,8},{12,14},{14,12},{16,18},{18,... | collective-permute-start | bytes 393224 | tf_op jit(solution)/shard_map/ppermute | solution.py:299
  40.3 3.3 %collective-permute-start.17 = (bf16[512,128]{1,0:T(8,128)(2,1)S(1)}, bf16[512,128]{1,0:T(8,128)(2,1)S(1)}, u32[]{:S(2)}, u32[]{:S(2)}) collective-permute-start(bf16[512,128]{1,0:T(8,128)(2,1)S(1)} %collective-permute-done.9.refs_8_), channel_id=1, source_target_pairs={{0,1},{1,0},{2,3},{3,2},{4,5},{5,4},{6,7},{7,6},{8,9},{9,8},{10,11... | collective-permute-start | bytes 393224 | tf_op jit(solution)/shard_map/ppermute | solution.py:301
  41.5 2.2 %collective-permute-start.18 = (bf16[512,128]{1,0:T(8,128)(2,1)S(1)}, bf16[512,128]{1,0:T(8,128)(2,1)S(1)}, u32[]{:S(2)}, u32[]{:S(2)}) collective-permute-start(bf16[512,128]{1,0:T(8,128)(2,1)S(1)} %collective-permute-done.10.refs_9_), channel_id=1, source_target_pairs={{0,1},{1,0},{2,3},{3,2},{4,5},{5,4},{6,7},{7,6},{8,9},{9,8},{10,11... | collective-permute-start | bytes 393224 | tf_op jit(solution)/shard_map/ppermute | solution.py:301
  41.5 2.2 %collective-permute-start.19 = (bf16[512,128]{1,0:T(8,128)(2,1)S(1)}, bf16[512,128]{1,0:T(8,128)(2,1)S(1)}, u32[]{:S(2)}, u32[]{:S(2)}) collective-permute-start(bf16[512,128]{1,0:T(8,128)(2,1)S(1)} %collective-permute-done.11.refs_10_), channel_id=1, source_target_pairs={{0,1},{1,0},{2,3},{3,2},{4,5},{5,4},{6,7},{7,6},{8,9},{9,8},{10,11... | collective-permute-start | bytes 393224 | tf_op jit(solution)/shard_map/ppermute | solution.py:301
  43.7 1.3 %collective-permute-start.20 = (bf16[512,128]{1,0:T(8,128)(2,1)S(1)}, bf16[512,128]{1,0:T(8,128)(2,1)S(1)}, u32[]{:S(2)}, u32[]{:S(2)}) collective-permute-start(bf16[512,128]{1,0:T(8,128)(2,1)S(1)} %collective-permute-done.12.refs_11_), channel_id=1, source_target_pairs={{0,1},{1,0},{2,3},{3,2},{4,5},{5,4},{6,7},{7,6},{8,9},{9,8},{10,11... | collective-permute-start | bytes 393224 | tf_op jit(solution)/shard_map/ppermute | solution.py:301
  45.0 47.9 %copy-start.1 = (bf16[512,2048]{1,0:T(8,128)(2,1)S(1)}, bf16[512,2048]{1,0:T(8,128)(2,1)}, u32[]{:S(2)}) copy-start(bf16[512,2048]{1,0:T(8,128)(2,1)} %refs_8_.1) | copy-start | bytes 6291460
  75.5 4.1 %collective-permute-start.21 = (bf16[256,128]{1,0:T(8,128)(2,1)S(1)}, bf16[256,128]{1,0:T(8,128)(2,1)S(1)}, u32[]{:S(2)}, u32[]{:S(2)}) collective-permute-start(bf16[256,128]{1,0:T(8,128)(2,1)S(1)} %get-tuple-element.25), channel_id=1, source_target_pairs={{0,0},{4,1},{2,2},{6,3},{1,4},{5,5},{3,6},{7,7},{8,8},{12,9},{10,1... | collective-permute-start | bytes 196616 | tf_op jit(solution)/shard_map/ppermute | solution.py:327
  76.2 9.7 %collective-permute-start.22 = (bf16[256,128]{1,0:T(8,128)(2,1)S(1)}, bf16[256,128]{1,0:T(8,128)(2,1)S(1)}, u32[]{:S(2)}, u32[]{:S(2)}) collective-permute-start(bf16[256,128]{1,0:T(8,128)(2,1)S(1)} %get-tuple-element.26), channel_id=1, source_target_pairs={{8,0},{12,1},{10,2},{14,3},{9,4},{13,5},{11,6},{15,7},{16,8},{20,9... | collective-permute-start | bytes 196616 | tf_op jit(solution)/shard_map/ppermute | solution.py:327
  79.0 8.0 %collective-permute-start.23 = (bf16[256,128]{1,0:T(8,128)(2,1)S(1)}, bf16[256,128]{1,0:T(8,128)(2,1)S(1)}, u32[]{:S(2)}, u32[]{:S(2)}) collective-permute-start(bf16[256,128]{1,0:T(8,128)(2,1)S(1)} %get-tuple-element.27), channel_id=1, source_target_pairs={{16,0},{20,1},{18,2},{22,3},{17,4},{21,5},{19,6},{23,7},{24,8},{28... | collective-permute-start | bytes 196616 | tf_op jit(solution)/shard_map/ppermute | solution.py:327
  79.0 12.2 %collective-permute-start.24 = (bf16[256,128]{1,0:T(8,128)(2,1)S(1)}, bf16[256,128]{1,0:T(8,128)(2,1)S(1)}, u32[]{:S(2)}, u32[]{:S(2)}) collective-permute-start(bf16[256,128]{1,0:T(8,128)(2,1)S(1)} %get-tuple-element.28), channel_id=1, source_target_pairs={{24,0},{28,1},{26,2},{30,3},{25,4},{29,5},{27,6},{31,7},{0,8},{4,9... | collective-permute-start | bytes 196616 | tf_op jit(solution)/shard_map/ppermute | solution.py:327
  79.6 12.4 %collective-permute-start.25 = (bf16[256,128]{1,0:T(8,128)(2,1)S(1)}, bf16[256,128]{1,0:T(8,128)(2,1)S(1)}, u32[]{:S(2)}, u32[]{:S(2)}) collective-permute-start(bf16[256,128]{1,0:T(8,128)(2,1)S(1)} %collective-permute-done.21.refs_0_), channel_id=1, source_target_pairs={{0,1},{1,0},{2,3},{3,2},{4,5},{5,4},{6,7},{7,6},{8,9},{9,8},{10,11... | collective-permute-start | bytes 196616 | tf_op jit(solution)/shard_map/ppermute | solution.py:328
  85.8 6.2 %collective-permute-start.26 = (bf16[256,128]{1,0:T(8,128)(2,1)S(1)}, bf16[256,128]{1,0:T(8,128)(2,1)S(1)}, u32[]{:S(2)}, u32[]{:S(2)}) collective-permute-start(bf16[256,128]{1,0:T(8,128)(2,1)S(1)} %collective-permute-done.22.refs_1_), channel_id=1, source_target_pairs={{0,1},{1,0},{2,3},{3,2},{4,5},{5,4},{6,7},{7,6},{8,9},{9,8},{10,11... | collective-permute-start | bytes 196616 | tf_op jit(solution)/shard_map/ppermute | solution.py:328
  87.0 5.1 %collective-permute-start.27 = (bf16[256,128]{1,0:T(8,128)(2,1)S(1)}, bf16[256,128]{1,0:T(8,128)(2,1)S(1)}, u32[]{:S(2)}, u32[]{:S(2)}) collective-permute-start(bf16[256,128]{1,0:T(8,128)(2,1)S(1)} %collective-permute-done.23.refs_2_), channel_id=1, source_target_pairs={{0,1},{1,0},{2,3},{3,2},{4,5},{5,4},{6,7},{7,6},{8,9},{9,8},{10,11... | collective-permute-start | bytes 196616 | tf_op jit(solution)/shard_map/ppermute | solution.py:328
  91.1 1.8 %collective-permute-start.28 = (bf16[256,128]{1,0:T(8,128)(2,1)S(1)}, bf16[256,128]{1,0:T(8,128)(2,1)S(1)}, u32[]{:S(2)}, u32[]{:S(2)}) collective-permute-start(bf16[256,128]{1,0:T(8,128)(2,1)S(1)} %collective-permute-done.24.refs_3_), channel_id=1, source_target_pairs={{0,1},{1,0},{2,3},{3,2},{4,5},{5,4},{6,7},{7,6},{8,9},{9,8},{10,11... | collective-permute-start | bytes 196616 | tf_op jit(solution)/shard_map/ppermute | solution.py:328
  (7 other events, 53.5 us)

commit v2 on v0

v2 whole, which is shorter than its diff:
```python
import functools
import math

import jax
import jax.numpy as jnp
from jax import lax
from jax.experimental import pallas as pl
from jax.experimental.pallas import tpu as pltpu
from jax.sharding import PartitionSpec as P


epsilon = 1e-06
masked_score = -1e30
log2_e = 1.4426950408889634
least_sum = 2.0**-90
most_sum = 2.0**100
lanes = 128


def cost(flops, moved):
    return pl.CostEstimate(flops=int(flops), bytes_accessed=int(moved), transcendentals=0)


def in_vmem():
    return pl.BlockSpec(memory_space=pltpu.VMEM)


def in_smem():
    return pl.BlockSpec(memory_space=pltpu.SMEM)


def in_hbm():
    return pl.BlockSpec(memory_space=pltpu.HBM)


def pair_up(first, second, heads):
    tiles = []
    low = lax.broadcasted_iota(jnp.int32, (first.shape[0], lanes), 1) < lanes // 2
    for pair in range(heads // 2):
        columns = slice(pair * lanes, (pair + 1) * lanes)
        rolled = pltpu.roll(second[:, columns], lanes // 2, 1)
        tiles.append(jnp.where(low, first[:, columns], rolled))
        tiles.append(jnp.where(low, rolled, first[:, columns]))
    return tiles


def fetch(arrays, buffers, sems):
    copies = []
    for index, (array, buffer) in enumerate(zip(arrays, buffers)):
        copies.append(pltpu.make_async_copy(array, buffer, sems.at[index]))
    for copy in copies:
        copy.start()
    return copies


def turned_into(stage, head, at, tile):
    turned = tile.T.astype(jnp.bfloat16)
    for part in range(tile.shape[0] // lanes):
        begin = at + part * lanes
        stage[head, begin : begin + lanes, :] = turned[:, part * lanes : (part + 1) * lanes]


def key_value_kernel(heads, place, *refs):
    arrays, outs = refs[:6], refs[6 : 6 + heads]
    hidden, query_one, query_two = refs[6 + heads : 9 + heads]
    key_one, key_two, value_proj, stage, sems = refs[9 + heads :]
    buffers = (hidden, key_one, key_two, value_proj, query_one, query_two)
    copies = fetch(arrays, buffers, sems)
    rows = hidden.shape[0]
    copies[0].wait()
    copies[1].wait()
    first = jnp.dot(hidden[...], key_one[...], preferred_element_type=jnp.float32)
    copies[2].wait()
    second = jnp.dot(hidden[...], key_two[...], preferred_element_type=jnp.float32)
    for head, tile in enumerate(pair_up(first, second, heads)):
        stage[head, :rows, :] = tile.astype(jnp.bfloat16)
    copies[3].wait()
    values = jnp.dot(hidden[...], value_proj[...], preferred_element_type=jnp.float32)
    for head in range(heads):
        turned_into(stage, head, rows, values[:, head * lanes : (head + 1) * lanes])
    for turn in range(heads):
        outs[turn][...] = stage[place[0] ^ turn]
    copies[4].wait()
    copies[5].wait()


def query_kernel(heads, scale, place, hidden, query_one, query_two, *refs):
    outs, stage = refs[:heads], refs[heads]
    first = jnp.dot(hidden[...], query_one[...], preferred_element_type=jnp.float32)
    second = jnp.dot(hidden[...], query_two[...], preferred_element_type=jnp.float32)
    for head, tile in enumerate(pair_up(first, second, heads)):
        turned_into(stage, head, 0, tile * scale)
    for turn in range(heads):
        outs[turn][...] = stage[place[0] ^ turn]


def attend_kernel(heads, down, across, place, lambdas, gain, *refs):
    z, y, x = place[0], place[1], place[2]
    parts = down * across
    query_in, refs = refs[:heads], refs[heads:]
    block_in, refs = refs[: heads * parts], refs[heads * parts :]
    outs, refs = refs[:heads], refs[heads:]
    queries, keys, values, accum, sums, peak, done, flag = refs
    rows = queries.shape[1]
    width = 2 * rows
    span = parts * rows
    bf16 = jnp.bfloat16

    for turn in range(heads):
        queries[z ^ turn] = query_in[turn][...]
    for below in range(down):
        for aside in range(across):
            for turn in range(heads):
                block = ((z ^ turn) * down + (y ^ below)) * across + (x ^ aside)
                given = block_in[(below * across + aside) * heads + turn]
                at = pl.multiple_of(block * rows, rows)
                keys[pl.ds(at, rows), :] = given[:rows, :]
                for part in range(rows // lanes):
                    begin = rows + part * lanes
                    column = pl.multiple_of(at + part * lanes, lanes)
                    values[:, pl.ds(column, lanes)] = given[begin : begin + lanes, :]

    mine = y * across + x
    odd = lax.rem(z, 2) == 1
    lam = lambdas[z]
    weight_low = jnp.where(odd, -lam, 1.0)
    weight_high = jnp.where(odd, 1.0, -lam)

    def ahead_of(count):
        key_row = lax.broadcasted_iota(jnp.int32, (count, width), 0)
        query_col = lax.broadcasted_iota(jnp.int32, (count, width), 1)
        return key_row - jnp.where(query_col < rows, query_col, query_col - rows)

    def two_maps_of(index):
        pieces = [
            queries[index, part * lanes : (part + 1) * lanes, :] for part in range(rows // lanes)
        ]
        joined = jnp.concatenate(pieces, axis=1)
        nothing = jnp.zeros((lanes // 2, rows), bf16)
        low = jnp.concatenate([joined[: lanes // 2], nothing], axis=0)
        high = jnp.concatenate([nothing, joined[lanes // 2 :]], axis=0)
        return jnp.concatenate([low, high], axis=1)

    def scores_of(at, count, two_maps):
        return jnp.dot(keys[pl.ds(at, count), :], two_maps, preferred_element_type=jnp.float32)

    def weighed(at, count, weights):
        return jnp.dot(
            values[:, pl.ds(at, count)], weights.astype(bf16), preferred_element_type=jnp.float32
        )

    def fold(weights):
        return jnp.sum(weights.reshape(weights.shape[0] // 8, 8, width), axis=0)

    def finish(index, added, total):
        total = jnp.sum(total, axis=0, keepdims=True)
        heads_out = added * (1.0 / total)
        mixed = heads_out[:, :rows] * weight_low + heads_out[:, rows:] * weight_high
        scale = lax.rsqrt(jnp.mean(mixed * mixed, axis=0, keepdims=True) + epsilon)
        done[index] = ((mixed * scale).T * gain[...]).astype(bf16)
        return total

    flag[...] = jnp.zeros_like(flag)
    for index in range(heads):
        two_maps = two_maps_of(index)
        weights = jnp.exp2(scores_of(index * span, span, two_maps))
        weights = jnp.where(ahead_of(span) <= mine * rows, weights, 0.0)
        total = fold(weights)
        added = weighed(index * span, span, weights)
        for before in range(index):
            weights = jnp.exp2(scores_of(before * span, span, two_maps))
            total = total + fold(weights)
            added = added + weighed(before * span, span, weights)
        total = finish(index, added, total)
        inside = (total >= least_sum) & (total <= most_sum)
        flag[...] = jnp.maximum(flag[...], jnp.where(inside, 0.0, 1.0))

    @pl.when(jnp.max(flag[...]) > 0.0)
    def _():
        def redo(index, carried):
            two_maps = two_maps_of(index)
            accum[...] = jnp.zeros_like(accum)
            sums[...] = jnp.zeros_like(sums)
            peak[...] = jnp.full(peak.shape, masked_score, jnp.float32)

            def one_block(block, inner):
                at = pl.multiple_of(block * rows, rows)
                allowed = ahead_of(rows) <= (index * parts + mine - block) * rows
                scores = jnp.where(allowed, scores_of(at, rows, two_maps), masked_score)
                highest = jnp.maximum(peak[...], jnp.max(scores, axis=0, keepdims=True))
                rescale = jnp.exp2(peak[...] - highest)
                weights = jnp.where(allowed, jnp.exp2(scores - highest), 0.0)
                sums[...] = sums[...] * rescale + fold(weights)
                accum[...] = accum[...] * rescale + weighed(at, rows, weights)
                peak[...] = highest
                return inner

            lax.fori_loop(0, index * parts + mine + 1, one_block, 0)
            finish(index, accum[...], sums[...])
            return carried

        lax.fori_loop(0, heads, redo, 0)

    for turn in range(heads):
        outs[turn][...] = done[z ^ turn]


def join_kernel(heads, place, *refs):
    pieces, joined = refs[:heads], refs[heads]
    for turn in range(heads):
        at = pl.multiple_of((place[0] ^ turn) * lanes, lanes)
        joined[:, pl.ds(at, lanes)] = pieces[turn][...]


def project_out_kernel(mine, other, out_mine, out_other, result, staged, sems):
    copies = []
    pieces = sems.shape[0]
    wide = result.shape[1] // pieces
    for piece in range(pieces):
        columns = slice(piece * wide, (piece + 1) * wide)
        total = jnp.dot(mine[...], out_mine[:, columns], preferred_element_type=jnp.float32)
        total = total + jnp.dot(
            other[...], out_other[:, columns], preferred_element_type=jnp.float32
        )
        staged[:, columns] = total.astype(jnp.bfloat16)
        copies.append(
            pltpu.make_async_copy(staged.at[:, columns], result.at[:, columns], sems.at[piece])
        )
        copies[-1].start()
    for copy in copies:
        copy.wait()


def from_hbm(*arrays):
    return [pltpu.with_memory_space_constraint(array, pltpu.HBM) for array in arrays]


def exchanged(
    hidden_in, query_one, query_two, key_one, key_two, value_proj, lambdas, norm_gain, out_proj
):
    heads = lambdas.shape[0]
    groups = lax.axis_size("tp")
    down = across = 2
    parts = down * across
    rows, model = hidden_in.shape
    head_qk = query_one.shape[1] // heads
    width = heads * head_qk
    scale = 1.75 * head_qk ** (-0.5) * log2_e
    bf16 = jnp.bfloat16
    f32 = jnp.float32

    sp_index = lax.axis_index("sp")
    z = sp_index // parts
    y = (sp_index // across) % down
    x = sp_index % across
    place = jnp.stack([z, y, x]).astype(jnp.int32)

    def exchange(array, step):
        pairs = [(index, index ^ step) for index in range(heads * parts)]
        return lax.ppermute(array, "sp", pairs)

    swap_core = [(i, (i + 1) % groups) for i in range(groups)]
    turns = range(heads)

    block_rows = 2 * rows
    block = jax.ShapeDtypeStruct((block_rows, lanes), bf16)
    stripe = jax.ShapeDtypeStruct((rows, lanes), bf16)
    fetched = (hidden_in, query_one, query_two)
    made = pl.pallas_call(
        functools.partial(key_value_kernel, heads),
        out_shape=[block] * heads + [jax.ShapeDtypeStruct(a.shape, bf16) for a in fetched],
        in_specs=[in_smem()] + [in_hbm()] * 6,
        out_specs=[in_vmem()] * (heads + 3),
        scratch_shapes=[
            pltpu.VMEM((model, width), bf16),
            pltpu.VMEM((model, width), bf16),
            pltpu.VMEM((model, heads * lanes), bf16),
            pltpu.VMEM((heads, block_rows, lanes), bf16),
            pltpu.SemaphoreType.DMA((6,)),
        ],
        compiler_params=pltpu.CompilerParams(vmem_limit_bytes=20 << 20),
        cost_estimate=cost(2 * rows * model * 4 * width, 7 << 20),
        name="project_keys",
    )(place, *from_hbm(hidden_in, key_one, key_two, value_proj, query_one, query_two))
    kv, held = made[:heads], made[heads:]
    own = [kv[0]] + [exchange(kv[turn], turn * parts) for turn in turns[1:]]

    queries = pl.pallas_call(
        functools.partial(query_kernel, heads, scale),
        out_shape=[stripe] * heads,
        in_specs=[in_smem()] + [in_vmem()] * 3,
        out_specs=[in_vmem()] * heads,
        scratch_shapes=[pltpu.VMEM((heads, rows, lanes), bf16)],
        compiler_params=pltpu.CompilerParams(vmem_limit_bytes=16 << 20),
        cost_estimate=cost(2 * rows * model * 2 * width, 4 << 20),
        name="project_queries",
    )(place, *held)
    own_queries = [queries[0]]
    for turn in turns[1:]:
        own_queries.append(exchange(queries[turn], turn * parts))

    out_other = lax.ppermute(out_proj, "tp", swap_core)
    aside = [exchange(own[turn], 1) for turn in turns]
    below = [exchange(own[turn], across) for turn in turns]
    corner = [exchange(own[turn], 1 + across) for turn in turns]
    blocks = own + aside + below + corner

    tokens = heads * rows
    normed = pl.pallas_call(
        functools.partial(attend_kernel, heads, down, across),
        out_shape=[jax.ShapeDtypeStruct((rows, lanes), bf16)] * heads,
        in_specs=[in_smem()] * 2 + [in_vmem()] * (1 + heads + heads * parts),
        out_specs=[in_vmem()] * heads,
        scratch_shapes=[
            pltpu.VMEM((heads, rows, lanes), bf16),
            pltpu.VMEM((parts * tokens, lanes), bf16),
            pltpu.VMEM((lanes, parts * tokens), bf16),
            pltpu.VMEM((lanes, 2 * rows), f32),
            pltpu.VMEM((8, 2 * rows), f32),
            pltpu.VMEM((1, 2 * rows), f32),
            pltpu.VMEM((heads, rows, lanes), bf16),
            pltpu.VMEM((1, 2 * rows), f32),
        ],
        compiler_params=pltpu.CompilerParams(vmem_limit_bytes=32 << 20),
        cost_estimate=cost(4 * tokens * tokens * parts * lanes, 3 << 20),
        name="attend",
    )(place, lambdas, norm_gain.reshape(1, lanes), *own_queries, *blocks)

    back = [normed[0]]
    for turn in turns[1:]:
        back.append(exchange(normed[turn], turn * parts))
    joined = pl.pallas_call(
        functools.partial(join_kernel, heads),
        out_shape=jax.ShapeDtypeStruct((rows, heads * lanes), bf16),
        in_specs=[in_smem()] + [in_vmem()] * heads,
        out_specs=in_vmem(),
        compiler_params=pltpu.CompilerParams(vmem_limit_bytes=4 << 20),
        cost_estimate=cost(0, 2 * rows * heads * lanes),
        name="join",
    )(place, *back)
    joined_other = lax.ppermute(joined, "tp", swap_core)
    return pl.pallas_call(
        project_out_kernel,
        out_shape=jax.ShapeDtypeStruct((rows, model), bf16),
        in_specs=[in_vmem()] * 4,
        out_specs=in_hbm(),
        scratch_shapes=[pltpu.VMEM((rows, model), bf16), pltpu.SemaphoreType.DMA((4,))],
        compiler_params=pltpu.CompilerParams(vmem_limit_bytes=16 << 20),
        cost_estimate=cost(2 * rows * model * groups * heads * lanes, 6 << 20),
        name="project_out",
    )(joined, joined_other, out_proj, out_other)


def gathered(
    hidden_in, query_one, query_two, key_one, key_two, value_proj, lambdas, norm_gain, out_proj
):
    heads_dev = lambdas.shape[0]
    head_qk = query_one.shape[1] // heads_dev
    head_v = value_proj.shape[1] // heads_dev
    width_q = heads_dev * head_qk
    score_scale = 1.75 * head_qk ** (-0.5)
    joined = jnp.concatenate((query_one, query_two, key_one, key_two, value_proj), axis=1)
    projected = jnp.dot(hidden_in, joined, preferred_element_type=jnp.float32).astype(jnp.bfloat16)
    tok_rows = projected.shape[0]
    key_values = projected[:, 2 * width_q :]
    my_index = lax.axis_index("sp")
    positions = my_index * tok_rows + jnp.arange(tok_rows, dtype=jnp.int32)
    query_a = projected[:, :width_q].reshape(tok_rows, heads_dev, head_qk)
    query_b = projected[:, width_q : 2 * width_q].reshape(tok_rows, heads_dev, head_qk)
    last_pos = positions[tok_rows - 1]

    def one_map(queries, keys, value_rows, allowed, running_max, running_sum, accum):
        scores = (
            jnp.einsum("qhd,khd->hqk", queries, keys, preferred_element_type=jnp.float32)
            * score_scale
        )
        scores = jnp.where(allowed[None], scores, masked_score)
        new_max = jnp.maximum(running_max, jnp.max(scores, axis=-1))
        rescale = jnp.exp(running_max - new_max)
        weights = jnp.where(allowed[None], jnp.exp(scores - new_max[..., None]), 0.0)
        new_sum = running_sum * rescale + jnp.sum(weights, axis=-1)
        added = jnp.einsum(
            "hqk,khe->hqe",
            weights.astype(jnp.bfloat16),
            value_rows,
            preferred_element_type=jnp.float32,
        )
        return (new_max, new_sum, accum * rescale[..., None] + added)

    def absorb(state, kblock, kstart):
        block_rows = kblock.shape[0]
        k_pos = kstart + jnp.arange(block_rows, dtype=jnp.int32)
        allowed = k_pos[None, :] <= positions[:, None]
        keys_a = kblock[:, :width_q].reshape(block_rows, heads_dev, head_qk)
        keys_b = kblock[:, width_q : 2 * width_q].reshape(block_rows, heads_dev, head_qk)
        value_rows = kblock[:, 2 * width_q :].reshape(block_rows, heads_dev, head_v)
        first_map = one_map(query_a, keys_a, value_rows, allowed, *state[:3])
        second_map = one_map(query_b, keys_b, value_rows, allowed, *state[3:])
        return first_map + second_map

    start_max = jnp.full((heads_dev, tok_rows), masked_score, jnp.float32)
    start_sum = jnp.zeros((heads_dev, tok_rows), jnp.float32)
    start_acc = jnp.zeros((heads_dev, tok_rows, head_v), jnp.float32)
    state = (start_max, start_sum, start_acc, start_max, start_sum, start_acc)
    kv_piece = lax.all_gather(key_values, "sp", axis=0, tiled=True)
    piece_rows = kv_piece.shape[0]
    block_rows = math.gcd(piece_rows, 512)
    block_count = piece_rows // block_rows
    stacked = kv_piece.reshape(block_count, block_rows, kv_piece.shape[1])

    def absorb_step(carried, blocks_in):
        kblock, block_index = blocks_in
        kstart = block_index * block_rows
        renewed = lax.cond(
            kstart <= last_pos,
            lambda inner: absorb(inner, kblock, kstart),
            lambda inner: inner,
            carried,
        )
        return (renewed, None)

    state, _ = lax.scan(absorb_step, state, (stacked, jnp.arange(block_count, dtype=jnp.int32)))
    out_a = state[2] / state[1][..., None]
    out_b = state[5] / state[4][..., None]
    mixed_out = out_a - lambdas[:, None, None] * out_b
    scale_rows = lax.rsqrt(jnp.mean(mixed_out * mixed_out, axis=-1, keepdims=True) + epsilon)
    normed = (mixed_out * scale_rows * norm_gain).astype(jnp.bfloat16)
    normed_all = jnp.transpose(normed, (1, 0, 2)).reshape(tok_rows, heads_dev * head_v)
    partial_value = jnp.dot(normed_all, out_proj, preferred_element_type=jnp.float32)
    return lax.psum(partial_value.astype(jnp.bfloat16), "tp")


def shards(*args):
    hidden_in, query_one, value_proj, lambdas = args[0], args[1], args[5], args[6]
    heads = lambdas.shape[0]
    groups, length = lax.axis_size("tp"), lax.axis_size("sp")
    fits = (
        groups == 2
        and heads == 4
        and length == 4 * heads
        and query_one.shape[1] == heads * (lanes // 2)
        and value_proj.shape[1] == heads * lanes
        and hidden_in.shape[0] % lanes == 0
        and hidden_in.shape[0] <= 512
    )
    if not fits:
        return gathered(*args)
    return exchanged(*args)


def solution(mesh):
    placed = (
        P("sp", None),
        P(None, "tp"),
        P(None, "tp"),
        P(None, "tp"),
        P(None, "tp"),
        P(None, "tp"),
        P("tp"),
        P(),
        P("tp", None),
    )
    return jax.shard_map(
        shards, mesh=mesh, in_specs=placed, out_specs=P("sp", None), check_vma=False
    )
```

time: 255 us -> 102 us (0.40)
  the two profiles are of different devices: /device:TPU:0 before, /device:TPU:7 now
where the time goes in v2:
time: 102 us; the launch traced here: 101 us
  waiting for transfers between devices  36 us (35%)
  Pallas kernels  35.8 us (35%)
  starting transfers between devices  29.5 us (29%)
    ppermute x21, waiting for transfers between devices, exchange(): return lax.ppermute(array, 'sp', pairs)  34.8 us
    pallas_call x1, Pallas kernels, exchanged(): pl.pallas_call(functools.partial(attend_kernel, heads, down, across), out...  27.3 us
    ppermute x21, starting transfers between devices, exchange(): return lax.ppermute(array, 'sp', pairs)  25 us
    pallas_call x1, Pallas kernels, exchanged(): pl.pallas_call(functools.partial(key_value_kernel, heads), out_shape=[blo...  4.46 us
    ppermute x1, starting transfers between devices, exchanged(): joined_other = lax.ppermute(joined, 'tp', swap_core)  3.87 us
  transfers between devices with their start and end apart: 23, of which 12 were waited for; matrix products, arithmetic and copies ran while one was open for 0% of the time, Pallas kernels for 33%

profile of v2, /device:TPU:7, one launch (start us, length us, event | category | flops | bytes accessed | tf_op | source)
XLA Modules:
  0.0 101.4 jit_solution(15749172431955054971)
XLA Ops:
  0.0 0.7 collective-permute-start.22
  0.8 4.5 %project_keys.1 = (bf16[512,128]{1,0:T(8,128)(2,1)S(1)}, bf16[512,128]{1,0:T(8,128)(2,1)S(1)}, bf16[512,128]{1,0:T(8,128)(2,1)S(1)}, bf16[512,128]{1,0:T(8,128)(...) custom-call(s32[3]{0:T(128)S(1)} %pad_add_fusion.place, ...), custom_call_target="tpu_custom_call" | custom-call | flops 1073741824 | bytes 7340032 | tf_op jit(solution)/shard_map/project_keys/pallas_call | solution.py:269
  5.2 1.4 %project_queries.1 = (bf16[256,128]{1,0:T(8,128)(2,1)S(1)}, bf16[256,128]{1,0:T(8,128)(2,1)S(1)}, bf16[256,128]{1,0:T(8,128)(2,1)S(1)}, bf16[256,128]{1,0:T(8,128)(2,1)S(1)}) custom-call(s32[3]{0:T(128)S(1)} %pad_add_fusion.place, bf16[256,2048]{1,0:T(8,128)(2,1)S(1)} %get-tuple-element.20.hidden, bf16[2048,256]{1,0:T(8,128)(2,1)S(1)} %get-tuple-element.21.query_one, ...), custom_call_target="tpu_custom_call" | custom-call | flops 536870912 | bytes 4194304 | tf_op jit(solution)/shard_map/project_queries/pallas_call | solution.py:288
  6.7 1.4 %collective-permute-start = (bf16[256,128]{1,0:T(8,128)(2,1)S(1)}, bf16[256,128]{1,0:T(8,128)(2,1)S(1)}, u32[]{:S(2)}, u32[]{:S(2)}) collective-permute-start(bf16[256,128]{1,0:T(8,128)(2,1)S(1)} %get-tuple-element.24), channel_id=1, source_target_pairs={{0,8},{2,10},{4,12},{6,14},{8,0},{10,2},{12,4},{14,6},{16,24},{18,... | collective-permute-start | bytes 196616 | tf_op jit(solution)/shard_map/ppermute | solution.py:260
  8.1 2.3 %collective-permute-start.1 = (bf16[256,128]{1,0:T(8,128)(2,1)S(1)}, bf16[256,128]{1,0:T(8,128)(2,1)S(1)}, u32[]{:S(2)}, u32[]{:S(2)}) collective-permute-start(bf16[256,128]{1,0:T(8,128)(2,1)S(1)} %get-tuple-element.25), channel_id=1, source_target_pairs={{0,16},{2,18},{4,20},{6,22},{8,24},{10,26},{12,28},{14,30},{16,0},... | collective-permute-start | bytes 196616 | tf_op jit(solution)/shard_map/ppermute | solution.py:260
  10.6 3.3 %collective-permute-start.5 = (bf16[512,128]{1,0:T(8,128)(2,1)S(1)}, bf16[512,128]{1,0:T(8,128)(2,1)S(1)}, u32[]{:S(2)}, u32[]{:S(2)}) collective-permute-start(bf16[512,128]{1,0:T(8,128)(2,1)S(1)} %get-tuple-element.30), channel_id=1, source_target_pairs={{0,24},{2,26},{4,28},{6,30},{8,16},{10,18},{12,20},{14,22},{16,8},... | collective-permute-start | bytes 393224 | tf_op jit(solution)/shard_map/ppermute | solution.py:260
  13.9 0.4 collective-permute-start.2
  14.4 9.3 %collective-permute-done.2.refs_3_ = bf16[256,128]{1,0:T(8,128)(2,1)S(1)} collective-permute-done((bf16[256,128]{1,0:T(8,128)(2,1)S(1)}, bf16[256,128]{1,0:T(8,128)(2,1)S(1)}, u32[]{:S(2)}, u32[]{:S(2)}) %collective-permute-start.2) | collective-permute-done | bytes 65568 | tf_op jit(solution)/shard_map/ppermute | solution.py:260
  24.0 1.2 %collective-permute-start.14 = (bf16[512,128]{1,0:T(8,128)(2,1)S(1)}, bf16[512,128]{1,0:T(8,128)(2,1)S(1)}, u32[]{:S(2)}, u32[]{:S(2)}) collective-permute-start(bf16[512,128]{1,0:T(8,128)(2,1)S(1)} %get-tuple-element.27.refs_4_), channel_id=1, source_target_pairs={{0,6},{2,4},{4,2},{6,0},{8,14},{10,12},{12,10},{14,8},{16,22},{18,... | collective-permute-start | bytes 393224 | tf_op jit(solution)/shard_map/ppermute | solution.py:260
  25.2 1.2 %collective-permute-start.6 = (bf16[512,128]{1,0:T(8,128)(2,1)S(1)}, bf16[512,128]{1,0:T(8,128)(2,1)S(1)}, u32[]{:S(2)}, u32[]{:S(2)}) collective-permute-start(bf16[512,128]{1,0:T(8,128)(2,1)S(1)} %get-tuple-element.27.refs_4_), channel_id=1, source_target_pairs={{0,2},{2,0},{4,6},{6,4},{8,10},{10,8},{12,14},{14,12},{16,18},{18,... | collective-permute-start | bytes 393224 | tf_op jit(solution)/shard_map/ppermute | solution.py:260
  26.6 2.9 %collective-permute-done.10.refs_12_ = bf16[512,128]{1,0:T(8,128)(2,1)S(1)} collective-permute-done((bf16[512,128]{1,0:T(8,128)(2,1)S(1)}, bf16[512,128]{1,0:T(8,128)(2,1)S(1)}, u32[]{:S(2)}, u32[]{:S(2)}) %collective-permute-start.10) | collective-permute-done | bytes 131104 | tf_op jit(solution)/shard_map/ppermute | solution.py:260
  29.6 1.5 %collective-permute-start.13 = (bf16[512,128]{1,0:T(8,128)(2,1)S(1)}, bf16[512,128]{1,0:T(8,128)(2,1)S(1)}, u32[]{:S(2)}, u32[]{:S(2)}) collective-permute-start(bf16[512,128]{1,0:T(8,128)(2,1)S(1)} %collective-permute-done.5.refs_7_), channel_id=1, source_target_pairs={{0,4},{2,6},{4,0},{6,2},{8,12},{10,14},{12,8},{14,10},{16,20},{18,... | collective-permute-start | bytes 393224 | tf_op jit(solution)/shard_map/ppermute | solution.py:260
  31.0 0.6 collective-permute-done.6.refs_8_
  31.8 1.8 %collective-permute-done.11.refs_13_ = bf16[512,128]{1,0:T(8,128)(2,1)S(1)} collective-permute-done((bf16[512,128]{1,0:T(8,128)(2,1)S(1)}, bf16[512,128]{1,0:T(8,128)(2,1)S(1)}, u32[]{:S(2)}, u32[]{:S(2)}) %collective-permute-start.11) | collective-permute-done | bytes 131104 | tf_op jit(solution)/shard_map/ppermute | solution.py:260
  33.6 0.9 collective-permute-start.16
  34.5 4.7 %collective-permute-done.12.refs_14_ = bf16[512,128]{1,0:T(8,128)(2,1)S(1)} collective-permute-done((bf16[512,128]{1,0:T(8,128)(2,1)S(1)}, bf16[512,128]{1,0:T(8,128)(2,1)S(1)}, u32[]{:S(2)}, u32[]{:S(2)}) %collective-permute-start.12) | collective-permute-done | bytes 131104 | tf_op jit(solution)/shard_map/ppermute | solution.py:260
  39.2 2.3 %collective-permute-start.17 = (bf16[512,128]{1,0:T(8,128)(2,1)S(1)}, bf16[512,128]{1,0:T(8,128)(2,1)S(1)}, u32[]{:S(2)}, u32[]{:S(2)}) collective-permute-start(bf16[512,128]{1,0:T(8,128)(2,1)S(1)} %collective-permute-done.5.refs_7_), channel_id=1, source_target_pairs={{0,6},{2,4},{4,2},{6,0},{8,14},{10,12},{12,10},{14,8},{16,22},{18,... | collective-permute-start | bytes 393224 | tf_op jit(solution)/shard_map/ppermute | solution.py:260
  41.5 4.7 %collective-permute-done.13.refs_15_ = bf16[512,128]{1,0:T(8,128)(2,1)S(1)} collective-permute-done((bf16[512,128]{1,0:T(8,128)(2,1)S(1)}, bf16[512,128]{1,0:T(8,128)(2,1)S(1)}, u32[]{:S(2)}, u32[]{:S(2)}) %collective-permute-start.13) | collective-permute-done | bytes 131104 | tf_op jit(solution)/shard_map/ppermute | solution.py:260
  46.5 1.2 %collective-permute-start.8 = (bf16[512,128]{1,0:T(8,128)(2,1)S(1)}, bf16[512,128]{1,0:T(8,128)(2,1)S(1)}, u32[]{:S(2)}, u32[]{:S(2)}) collective-permute-start(bf16[512,128]{1,0:T(8,128)(2,1)S(1)} %collective-permute-done.4.refs_6_), channel_id=1, source_target_pairs={{0,2},{2,0},{4,6},{6,4},{8,10},{10,8},{12,14},{14,12},{16,18},{18,... | collective-permute-start | bytes 393224 | tf_op jit(solution)/shard_map/ppermute | solution.py:260
  48.0 2.1 %collective-permute-done.7.refs_9_ = bf16[512,128]{1,0:T(8,128)(2,1)S(1)} collective-permute-done((bf16[512,128]{1,0:T(8,128)(2,1)S(1)}, bf16[512,128]{1,0:T(8,128)(2,1)S(1)}, u32[]{:S(2)}, u32[]{:S(2)}) %collective-permute-start.7) | collective-permute-done | bytes 131104 | tf_op jit(solution)/shard_map/ppermute | solution.py:260
  50.1 2.6 %collective-permute-done.8.refs_10_ = bf16[512,128]{1,0:T(8,128)(2,1)S(1)} collective-permute-done((bf16[512,128]{1,0:T(8,128)(2,1)S(1)}, bf16[512,128]{1,0:T(8,128)(2,1)S(1)}, u32[]{:S(2)}, u32[]{:S(2)}) %collective-permute-start.8) | collective-permute-done | bytes 131104 | tf_op jit(solution)/shard_map/ppermute | solution.py:260
  52.6 2.8 %collective-permute-done.9.refs_11_ = bf16[512,128]{1,0:T(8,128)(2,1)S(1)} collective-permute-done((bf16[512,128]{1,0:T(8,128)(2,1)S(1)}, bf16[512,128]{1,0:T(8,128)(2,1)S(1)}, u32[]{:S(2)}, u32[]{:S(2)}) %collective-permute-start.9) | collective-permute-done | bytes 131104 | tf_op jit(solution)/shard_map/ppermute | solution.py:260
  55.4 27.3 %attend.1 = (bf16[256,128]{1,0:T(8,128)(2,1)S(1)}, bf16[256,128]{1,0:T(8,128)(2,1)S(1)}, bf16[256,128]{1,0:T(8,128)(2,1)S(1)}, bf16[256,128]{1,0:T(8,128)(2,1)S(1)}) custom-call(s32[3]{0:T(128)S(1)} %pad_add_fusion.place, f32[4]{0:T(128)S(1)} %copy-done.1, f32[1,128]{1,0:T(1,128)S(1)} %bitcast.4, bf16[256,128]{1,0:T(8,128)(2,1)S(1)} %get-tuple-element.23.refs_0_, ...), custom_call_target="tpu_custom_call" | custom-call | flops 2147483648 | bytes 3145728 | tf_op jit(solution)/shard_map/attend/pallas_call | solution.py:309
  82.7 5.7 %collective-permute-start.18 = (bf16[256,128]{1,0:T(8,128)(2,1)S(1)}, bf16[256,128]{1,0:T(8,128)(2,1)S(1)}, u32[]{:S(2)}, u32[]{:S(2)}) collective-permute-start(bf16[256,128]{1,0:T(8,128)(2,1)S(1)} %get-tuple-element.32), channel_id=1, source_target_pairs={{0,8},{2,10},{4,12},{6,14},{8,0},{10,2},{12,4},{14,6},{16,24},{18,... | collective-permute-start | bytes 196616 | tf_op jit(solution)/shard_map/ppermute | solution.py:260
  88.4 0.4 collective-permute-start.19
  88.8 1.8 %collective-permute-start.20 = (bf16[256,128]{1,0:T(8,128)(2,1)S(1)}, bf16[256,128]{1,0:T(8,128)(2,1)S(1)}, u32[]{:S(2)}, u32[]{:S(2)}) collective-permute-start(bf16[256,128]{1,0:T(8,128)(2,1)S(1)} %get-tuple-element.34), channel_id=1, source_target_pairs={{0,24},{2,26},{4,28},{6,30},{8,16},{10,18},{12,20},{14,22},{16,8},... | collective-permute-start | bytes 196616 | tf_op jit(solution)/shard_map/ppermute | solution.py:260
  90.6 2.4 %collective-permute-done.19.refs_2_ = bf16[256,128]{1,0:T(8,128)(2,1)S(1)} collective-permute-done((bf16[256,128]{1,0:T(8,128)(2,1)S(1)}, bf16[256,128]{1,0:T(8,128)(2,1)S(1)}, u32[]{:S(2)}, u32[]{:S(2)}) %collective-permute-start.19) | collective-permute-done | bytes 65568 | tf_op jit(solution)/shard_map/ppermute | solution.py:260
  93.0 0.8 collective-permute-done.20.refs_3_
  93.8 0.6 join.1.mine
  94.4 3.9 %collective-permute-start.21 = (bf16[256,512]{1,0:T(8,128)(2,1)S(1)}, bf16[256,512]{1,0:T(8,128)(2,1)S(1)}, u32[]{:S(2)}, u32[]{:S(2)}) collective-permute-start(bf16[256,512]{1,0:T(8,128)(2,1)S(1)} %join.1.mine), channel_id=1, source_target_pairs={{0,1},{1,0},{2,3},{3,2},{4,5},{5,4},{6,7},{7,6},{8,9},{9,8},{10,11... | collective-permute-start | bytes 786440 | tf_op jit(solution)/shard_map/ppermute | solution.py:341
  98.3 1.2 %collective-permute-done.21.other = bf16[256,512]{1,0:T(8,128)(2,1)S(1)} collective-permute-done((bf16[256,512]{1,0:T(8,128)(2,1)S(1)}, bf16[256,512]{1,0:T(8,128)(2,1)S(1)}, u32[]{:S(2)}, u32[]{:S(2)}) %collective-permute-start.21) | collective-permute-done | bytes 262176 | tf_op jit(solution)/shard_map/ppermute | solution.py:341
  99.4 2.0 %project_out.1 = bf16[256,2048]{1,0:T(8,128)(2,1)} custom-call(bf16[256,512]{1,0:T(8,128)(2,1)S(1)} %join.1.mine, bf16[256,512]{1,0:T(8,128)(2,1)S(1)} %collective-permute-done.21.other, bf16[512,2048]{1,0:T(8,128)(2,1)S(1)} %copy-done, bf16[512,2048]{1,0:T(8,128)(2,1)S(1)} %collective-permute-done.22.out_other), custom_call_target="tpu_custom_call" | custom-call | flops 1073741824 | bytes 6291456 | tf_op jit(solution)/shard_map/project_out/pallas_call | solution.py:342
  (26 shorter events, 1.6 us)
Async XLA Ops:
  0.0 99.4 %collective-permute-start.22 = (bf16[512,2048]{1,0:T(8,128)(2,1)}, bf16[512,2048]{1,0:T(8,128)(2,1)S(1)}, u32[]{:S(2)}, u32[]{:S(2)}) collective-permute-start(bf16[512,2048]{1,0:T(8,128)(2,1)} %out_mine.1), channel_id=1, source_target_pairs={{0,1},{1,0},{2,3},{3,2},{4,5},{5,4},{6,7},{7,6},{8,9},{9,8},{10,11... | collective-permute-start | bytes 6291464 | tf_op jit(solution)/shard_map/ppermute | solution.py:302
  5.2 50.2 %copy-start.1 = (f32[4]{0:T(128)S(1)}, f32[4]{0:T(128)}, u32[]{:S(2)}) copy-start(f32[4]{0:T(128)} %lambdas.1) | copy-start | bytes 52
  5.2 50.2 %copy-start.2 = (f32[128]{0:T(128)S(1)}, f32[128]{0:T(128)}, u32[]{:S(2)}) copy-start(f32[128]{0:T(128)} %param.16) | copy-start | bytes 1540
  6.7 3.9 %collective-permute-start = (bf16[256,128]{1,0:T(8,128)(2,1)S(1)}, bf16[256,128]{1,0:T(8,128)(2,1)S(1)}, u32[]{:S(2)}, u32[]{:S(2)}) collective-permute-start(bf16[256,128]{1,0:T(8,128)(2,1)S(1)} %get-tuple-element.24), channel_id=1, source_target_pairs={{0,8},{2,10},{4,12},{6,14},{8,0},{10,2},{12,4},{14,6},{16,24},{18,... | collective-permute-start | bytes 196616 | tf_op jit(solution)/shard_map/ppermute | solution.py:260
  8.1 5.9 %collective-permute-start.1 = (bf16[256,128]{1,0:T(8,128)(2,1)S(1)}, bf16[256,128]{1,0:T(8,128)(2,1)S(1)}, u32[]{:S(2)}, u32[]{:S(2)}) collective-permute-start(bf16[256,128]{1,0:T(8,128)(2,1)S(1)} %get-tuple-element.25), channel_id=1, source_target_pairs={{0,16},{2,18},{4,20},{6,22},{8,24},{10,26},{12,28},{14,30},{16,0},... | collective-permute-start | bytes 196616 | tf_op jit(solution)/shard_map/ppermute | solution.py:260
  10.4 13.6 %collective-permute-start.3 = (bf16[512,128]{1,0:T(8,128)(2,1)S(1)}, bf16[512,128]{1,0:T(8,128)(2,1)S(1)}, u32[]{:S(2)}, u32[]{:S(2)}) collective-permute-start(bf16[512,128]{1,0:T(8,128)(2,1)S(1)} %get-tuple-element.28), channel_id=1, source_target_pairs={{0,8},{2,10},{4,12},{6,14},{8,0},{10,2},{12,4},{14,6},{16,24},{18,... | collective-permute-start | bytes 393224 | tf_op jit(solution)/shard_map/ppermute | solution.py:260
  10.5 14.6 %collective-permute-start.4 = (bf16[512,128]{1,0:T(8,128)(2,1)S(1)}, bf16[512,128]{1,0:T(8,128)(2,1)S(1)}, u32[]{:S(2)}, u32[]{:S(2)}) collective-permute-start(bf16[512,128]{1,0:T(8,128)(2,1)S(1)} %get-tuple-element.29), channel_id=1, source_target_pairs={{0,16},{2,18},{4,20},{6,22},{8,24},{10,26},{12,28},{14,30},{16,0},... | collective-permute-start | bytes 393224 | tf_op jit(solution)/shard_map/ppermute | solution.py:260
  10.6 15.8 %collective-permute-start.5 = (bf16[512,128]{1,0:T(8,128)(2,1)S(1)}, bf16[512,128]{1,0:T(8,128)(2,1)S(1)}, u32[]{:S(2)}, u32[]{:S(2)}) collective-permute-start(bf16[512,128]{1,0:T(8,128)(2,1)S(1)} %get-tuple-element.30), channel_id=1, source_target_pairs={{0,24},{2,26},{4,28},{6,30},{8,16},{10,18},{12,20},{14,22},{16,8},... | collective-permute-start | bytes 393224 | tf_op jit(solution)/shard_map/ppermute | solution.py:260
  13.9 9.8 %collective-permute-start.2 = (bf16[256,128]{1,0:T(8,128)(2,1)S(1)}, bf16[256,128]{1,0:T(8,128)(2,1)S(1)}, u32[]{:S(2)}, u32[]{:S(2)}) collective-permute-start(bf16[256,128]{1,0:T(8,128)(2,1)S(1)} %get-tuple-element.26), channel_id=1, source_target_pairs={{0,24},{2,26},{4,28},{6,30},{8,16},{10,18},{12,20},{14,22},{16,8},... | collective-permute-start | bytes 196616 | tf_op jit(solution)/shard_map/ppermute | solution.py:260
  23.7 5.8 %collective-permute-start.10 = (bf16[512,128]{1,0:T(8,128)(2,1)S(1)}, bf16[512,128]{1,0:T(8,128)(2,1)S(1)}, u32[]{:S(2)}, u32[]{:S(2)}) collective-permute-start(bf16[512,128]{1,0:T(8,128)(2,1)S(1)} %get-tuple-element.27.refs_4_), channel_id=1, source_target_pairs={{0,4},{2,6},{4,0},{6,2},{8,12},{10,14},{12,8},{14,10},{16,20},{18,... | collective-permute-start | bytes 393224 | tf_op jit(solution)/shard_map/ppermute | solution.py:260
  24.0 5.6 %collective-permute-start.14 = (bf16[512,128]{1,0:T(8,128)(2,1)S(1)}, bf16[512,128]{1,0:T(8,128)(2,1)S(1)}, u32[]{:S(2)}, u32[]{:S(2)}) collective-permute-start(bf16[512,128]{1,0:T(8,128)(2,1)S(1)} %get-tuple-element.27.refs_4_), channel_id=1, source_target_pairs={{0,6},{2,4},{4,2},{6,0},{8,14},{10,12},{12,10},{14,8},{16,22},{18,... | collective-permute-start | bytes 393224 | tf_op jit(solution)/shard_map/ppermute | solution.py:260
  25.2 6.5 %collective-permute-start.6 = (bf16[512,128]{1,0:T(8,128)(2,1)S(1)}, bf16[512,128]{1,0:T(8,128)(2,1)S(1)}, u32[]{:S(2)}, u32[]{:S(2)}) collective-permute-start(bf16[512,128]{1,0:T(8,128)(2,1)S(1)} %get-tuple-element.27.refs_4_), channel_id=1, source_target_pairs={{0,2},{2,0},{4,6},{6,4},{8,10},{10,8},{12,14},{14,12},{16,18},{18,... | collective-permute-start | bytes 393224 | tf_op jit(solution)/shard_map/ppermute | solution.py:260
  26.4 7.2 %collective-permute-start.11 = (bf16[512,128]{1,0:T(8,128)(2,1)S(1)}, bf16[512,128]{1,0:T(8,128)(2,1)S(1)}, u32[]{:S(2)}, u32[]{:S(2)}) collective-permute-start(bf16[512,128]{1,0:T(8,128)(2,1)S(1)} %collective-permute-done.3.refs_5_), channel_id=1, source_target_pairs={{0,4},{2,6},{4,0},{6,2},{8,12},{10,14},{12,8},{14,10},{16,20},{18,... | collective-permute-start | bytes 393224 | tf_op jit(solution)/shard_map/ppermute | solution.py:260
  29.6 9.7 %collective-permute-start.12 = (bf16[512,128]{1,0:T(8,128)(2,1)S(1)}, bf16[512,128]{1,0:T(8,128)(2,1)S(1)}, u32[]{:S(2)}, u32[]{:S(2)}) collective-permute-start(bf16[512,128]{1,0:T(8,128)(2,1)S(1)} %collective-permute-done.4.refs_6_), channel_id=1, source_target_pairs={{0,4},{2,6},{4,0},{6,2},{8,12},{10,14},{12,8},{14,10},{16,20},{18,... | collective-permute-start | bytes 393224 | tf_op jit(solution)/shard_map/ppermute | solution.py:260
  29.6 16.7 %collective-permute-start.13 = (bf16[512,128]{1,0:T(8,128)(2,1)S(1)}, bf16[512,128]{1,0:T(8,128)(2,1)S(1)}, u32[]{:S(2)}, u32[]{:S(2)}) collective-permute-start(bf16[512,128]{1,0:T(8,128)(2,1)S(1)} %collective-permute-done.5.refs_7_), channel_id=1, source_target_pairs={{0,4},{2,6},{4,0},{6,2},{8,12},{10,14},{12,8},{14,10},{16,20},{18,... | collective-permute-start | bytes 393224 | tf_op jit(solution)/shard_map/ppermute | solution.py:260
  31.7 14.9 %collective-permute-start.15 = (bf16[512,128]{1,0:T(8,128)(2,1)S(1)}, bf16[512,128]{1,0:T(8,128)(2,1)S(1)}, u32[]{:S(2)}, u32[]{:S(2)}) collective-permute-start(bf16[512,128]{1,0:T(8,128)(2,1)S(1)} %collective-permute-done.3.refs_5_), channel_id=1, source_target_pairs={{0,6},{2,4},{4,2},{6,0},{8,14},{10,12},{12,10},{14,8},{16,22},{18,... | collective-permute-start | bytes 393224 | tf_op jit(solution)/shard_map/ppermute | solution.py:260
  33.6 14.1 %collective-permute-start.16 = (bf16[512,128]{1,0:T(8,128)(2,1)S(1)}, bf16[512,128]{1,0:T(8,128)(2,1)S(1)}, u32[]{:S(2)}, u32[]{:S(2)}) collective-permute-start(bf16[512,128]{1,0:T(8,128)(2,1)S(1)} %collective-permute-done.4.refs_6_), channel_id=1, source_target_pairs={{0,6},{2,4},{4,2},{6,0},{8,14},{10,12},{12,10},{14,8},{16,22},{18,... | collective-permute-start | bytes 393224 | tf_op jit(solution)/shard_map/ppermute | solution.py:260
  39.2 8.8 %collective-permute-start.17 = (bf16[512,128]{1,0:T(8,128)(2,1)S(1)}, bf16[512,128]{1,0:T(8,128)(2,1)S(1)}, u32[]{:S(2)}, u32[]{:S(2)}) collective-permute-start(bf16[512,128]{1,0:T(8,128)(2,1)S(1)} %collective-permute-done.5.refs_7_), channel_id=1, source_target_pairs={{0,6},{2,4},{4,2},{6,0},{8,14},{10,12},{12,10},{14,8},{16,22},{18,... | collective-permute-start | bytes 393224 | tf_op jit(solution)/shard_map/ppermute | solution.py:260
  46.2 3.8 %collective-permute-start.7 = (bf16[512,128]{1,0:T(8,128)(2,1)S(1)}, bf16[512,128]{1,0:T(8,128)(2,1)S(1)}, u32[]{:S(2)}, u32[]{:S(2)}) collective-permute-start(bf16[512,128]{1,0:T(8,128)(2,1)S(1)} %collective-permute-done.3.refs_5_), channel_id=1, source_target_pairs={{0,2},{2,0},{4,6},{6,4},{8,10},{10,8},{12,14},{14,12},{16,18},{18,... | collective-permute-start | bytes 393224 | tf_op jit(solution)/shard_map/ppermute | solution.py:260
  46.5 6.1 %collective-permute-start.8 = (bf16[512,128]{1,0:T(8,128)(2,1)S(1)}, bf16[512,128]{1,0:T(8,128)(2,1)S(1)}, u32[]{:S(2)}, u32[]{:S(2)}) collective-permute-start(bf16[512,128]{1,0:T(8,128)(2,1)S(1)} %collective-permute-done.4.refs_6_), channel_id=1, source_target_pairs={{0,2},{2,0},{4,6},{6,4},{8,10},{10,8},{12,14},{14,12},{16,18},{18,... | collective-permute-start | bytes 393224 | tf_op jit(solution)/shard_map/ppermute | solution.py:260
  47.7 7.7 %collective-permute-start.9 = (bf16[512,128]{1,0:T(8,128)(2,1)S(1)}, bf16[512,128]{1,0:T(8,128)(2,1)S(1)}, u32[]{:S(2)}, u32[]{:S(2)}) collective-permute-start(bf16[512,128]{1,0:T(8,128)(2,1)S(1)} %collective-permute-done.5.refs_7_), channel_id=1, source_target_pairs={{0,2},{2,0},{4,6},{6,4},{8,10},{10,8},{12,14},{14,12},{16,18},{18,... | collective-permute-start | bytes 393224 | tf_op jit(solution)/shard_map/ppermute | solution.py:260
  55.4 44.0 %copy-start = (bf16[512,2048]{1,0:T(8,128)(2,1)S(1)}, bf16[512,2048]{1,0:T(8,128)(2,1)}, u32[]{:S(2)}) copy-start(bf16[512,2048]{1,0:T(8,128)(2,1)} %out_mine.1) | copy-start | bytes 6291460
  82.7 7.8 %collective-permute-start.18 = (bf16[256,128]{1,0:T(8,128)(2,1)S(1)}, bf16[256,128]{1,0:T(8,128)(2,1)S(1)}, u32[]{:S(2)}, u32[]{:S(2)}) collective-permute-start(bf16[256,128]{1,0:T(8,128)(2,1)S(1)} %get-tuple-element.32), channel_id=1, source_target_pairs={{0,8},{2,10},{4,12},{6,14},{8,0},{10,2},{12,4},{14,6},{16,24},{18,... | collective-permute-start | bytes 196616 | tf_op jit(solution)/shard_map/ppermute | solution.py:260
  88.4 4.6 %collective-permute-start.19 = (bf16[256,128]{1,0:T(8,128)(2,1)S(1)}, bf16[256,128]{1,0:T(8,128)(2,1)S(1)}, u32[]{:S(2)}, u32[]{:S(2)}) collective-permute-start(bf16[256,128]{1,0:T(8,128)(2,1)S(1)} %get-tuple-element.33), channel_id=1, source_target_pairs={{0,16},{2,18},{4,20},{6,22},{8,24},{10,26},{12,28},{14,30},{16,0},... | collective-permute-start | bytes 196616 | tf_op jit(solution)/shard_map/ppermute | solution.py:260
  88.8 5.0 %collective-permute-start.20 = (bf16[256,128]{1,0:T(8,128)(2,1)S(1)}, bf16[256,128]{1,0:T(8,128)(2,1)S(1)}, u32[]{:S(2)}, u32[]{:S(2)}) collective-permute-start(bf16[256,128]{1,0:T(8,128)(2,1)S(1)} %get-tuple-element.34), channel_id=1, source_target_pairs={{0,24},{2,26},{4,28},{6,30},{8,16},{10,18},{12,20},{14,22},{16,8},... | collective-permute-start | bytes 196616 | tf_op jit(solution)/shard_map/ppermute | solution.py:260
  94.4 5.0 %collective-permute-start.21 = (bf16[256,512]{1,0:T(8,128)(2,1)S(1)}, bf16[256,512]{1,0:T(8,128)(2,1)S(1)}, u32[]{:S(2)}, u32[]{:S(2)}) collective-permute-start(bf16[256,512]{1,0:T(8,128)(2,1)S(1)} %join.1.mine), channel_id=1, source_target_pairs={{0,1},{1,0},{2,3},{3,2},{4,5},{5,4},{6,7},{7,6},{8,9},{9,8},{10,11... | collective-permute-start | bytes 786440 | tf_op jit(solution)/shard_map/ppermute | solution.py:341

commit v3 on v2

--- a/solution.py
+++ b/solution.py
@@ -94,31 +94,110 @@
         outs[turn][...] = stage[place[0] ^ turn]
 
 
-def attend_kernel(heads, down, across, place, lambdas, gain, *refs):
+def two_maps_of(turned):
+    rows = turned.shape[0]
+    pieces = [turned[part * lanes : (part + 1) * lanes] for part in range(rows // lanes)]
+    joined = jnp.concatenate(pieces, axis=1)
+    nothing = jnp.zeros((lanes // 2, rows), jnp.bfloat16)
+    low = jnp.concatenate([joined[: lanes // 2], nothing], axis=0)
+    high = jnp.concatenate([nothing, joined[lanes // 2 :]], axis=0)
+    return jnp.concatenate([low, high], axis=1)
+
+
+def ahead_of(count, rows):
+    key_row = lax.broadcasted_iota(jnp.int32, (count, 2 * rows), 0)
+    query_col = lax.broadcasted_iota(jnp.int32, (count, 2 * rows), 1)
+    return key_row - jnp.where(query_col < rows, query_col, query_col - rows)
+
+
+def scores_of(keys, at, count, two_maps):
+    return jnp.dot(keys[pl.ds(at, count), :], two_maps, preferred_element_type=jnp.float32)
+
+
+def weighed(values, at, weights):
+    return jnp.dot(
+        values[:, pl.ds(at, weights.shape[0])],
+        weights.astype(jnp.bfloat16),
+        preferred_element_type=jnp.float32,
+    )
+
+
+def fold(weights):
+    return jnp.sum(weights.reshape(weights.shape[0] // 8, 8, weights.shape[1]), axis=0)
+
+
+def span_of(keys, values, at, span, two_maps, limit=None):
+    weights = jnp.exp2(scores_of(keys, at, span, two_maps))
+    if limit is not None:
+        weights = jnp.where(ahead_of(span, two_maps.shape[1] // 2) <= limit, weights, 0.0)
+    return weighed(values, at, weights), fold(weights)
+
+
+def place_block(given, keys, values, at, rows):
+    keys[pl.ds(at, rows), :] = given[:rows, :]
+    for part in range(rows // lanes):
+        begin = rows + part * lanes
+        column = pl.multiple_of(at + part * lanes, lanes)
+        values[:, pl.ds(column, lanes)] = given[begin : begin + lanes, :]
+
+
+def early_kernel(heads, down, across, place, *refs):
     z, y, x = place[0], place[1], place[2]
     parts = down * across
+    last = heads // 2
+    early = [turn for turn in range(heads) if turn != last]
     query_in, refs = refs[:heads], refs[heads:]
-    block_in, refs = refs[: heads * parts], refs[heads * parts :]
-    outs, refs = refs[:heads], refs[heads:]
-    queries, keys, values, accum, sums, peak, done, flag = refs
+    block_in, refs = refs[: len(early) * parts], refs[len(early) * parts :]
+    queries, keys, values, accum, sums = refs
     rows = queries.shape[1]
-    width = 2 * rows
     span = parts * rows
-    bf16 = jnp.bfloat16
 
     for turn in range(heads):
         queries[z ^ turn] = query_in[turn][...]
     for below in range(down):
         for aside in range(across):
-            for turn in range(heads):
+            for number, turn in enumerate(early):
                 block = ((z ^ turn) * down + (y ^ below)) * across + (x ^ aside)
-                given = block_in[(below * across + aside) * heads + turn]
-                at = pl.multiple_of(block * rows, rows)
-                keys[pl.ds(at, rows), :] = given[:rows, :]
-                for part in range(rows // lanes):
-                    begin = rows + part * lanes
-                    column = pl.multiple_of(at + part * lanes, lanes)
-                    values[:, pl.ds(column, lanes)] = given[begin : begin + lanes, :]
+                given = block_in[(below * across + aside) * len(early) + number]
+                place_block(given, keys, values, pl.multiple_of(block * rows, rows), rows)
+
+    mine = y * across + x
+    for case in range(heads):
+
+        @pl.when(z == case)
+        def _(case=case):
+            for index in range(heads):
+                two_maps = two_maps_of(queries[index])
+                added = jnp.zeros(accum.shape[1:], jnp.float32)
+                total = jnp.zeros(sums.shape[1:], jnp.float32)
+                for at in range(index, -1, -1):
+                    if at == case ^ last:
+                        continue
+                    limit = mine * rows if at == index else None
+                    more, weight = span_of(keys, values, at * span, span, two_maps, limit)
+                    added = added + more
+                    total = total + weight
+                accum[index] = added
+                sums[index] = total
+
+
+def late_kernel(heads, down, across, place, lambdas, gain, *refs):
+    z, y, x = place[0], place[1], place[2]
+    parts = down * across
+    last = heads // 2
+    block_in, refs = refs[:parts], refs[parts:]
+    queries, keys, values, accum, sums = refs[:5]
+    outs, refs = refs[5 : 5 + heads], refs[5 + heads :]
+    late_keys, late_values, all_keys, all_values, done, flag, added_ref, sums_ref, peak = refs
+    rows = queries.shape[1]
+    span = parts * rows
+
+    for below in range(down):
+        for aside in range(across):
+            block = (y ^ below) * across + (x ^ aside)
+            given = block_in[below * across + aside]
+            at = pl.multiple_of(block * rows, rows)
+            place_block(given, late_keys, late_values, at, rows)
 
     mine = y * across + x
     odd = lax.rem(z, 2) == 1
@@ -126,77 +205,59 @@
     weight_low = jnp.where(odd, -lam, 1.0)
     weight_high = jnp.where(odd, 1.0, -lam)
 
-    def ahead_of(count):
-        key_row = lax.broadcasted_iota(jnp.int32, (count, width), 0)
-        query_col = lax.broadcasted_iota(jnp.int32, (count, width), 1)
-        return key_row - jnp.where(query_col < rows, query_col, query_col - rows)
-
-    def two_maps_of(index):
-        pieces = [
-            queries[index, part * lanes : (part + 1) * lanes, :] for part in range(rows // lanes)
-        ]
-        joined = jnp.concatenate(pieces, axis=1)
-        nothing = jnp.zeros((lanes // 2, rows), bf16)
-        low = jnp.concatenate([joined[: lanes // 2], nothing], axis=0)
-        high = jnp.concatenate([nothing, joined[lanes // 2 :]], axis=0)
-        return jnp.concatenate([low, high], axis=1)
-
-    def scores_of(at, count, two_maps):
-        return jnp.dot(keys[pl.ds(at, count), :], two_maps, preferred_element_type=jnp.float32)
-
-    def weighed(at, count, weights):
-        return jnp.dot(
-            values[:, pl.ds(at, count)], weights.astype(bf16), preferred_element_type=jnp.float32
-        )
-
-    def fold(weights):
-        return jnp.sum(weights.reshape(weights.shape[0] // 8, 8, width), axis=0)
-
     def finish(index, added, total):
         total = jnp.sum(total, axis=0, keepdims=True)
         heads_out = added * (1.0 / total)
         mixed = heads_out[:, :rows] * weight_low + heads_out[:, rows:] * weight_high
         scale = lax.rsqrt(jnp.mean(mixed * mixed, axis=0, keepdims=True) + epsilon)
-        done[index] = ((mixed * scale).T * gain[...]).astype(bf16)
+        done[index] = ((mixed * scale).T * gain[...]).astype(jnp.bfloat16)
         return total
 
     flag[...] = jnp.zeros_like(flag)
-    for index in range(heads):
-        two_maps = two_maps_of(index)
-        weights = jnp.exp2(scores_of(index * span, span, two_maps))
-        weights = jnp.where(ahead_of(span) <= mine * rows, weights, 0.0)
-        total = fold(weights)
-        added = weighed(index * span, span, weights)
-        for before in range(index):
-            weights = jnp.exp2(scores_of(before * span, span, two_maps))
-            total = total + fold(weights)
-            added = added + weighed(before * span, span, weights)
-        total = finish(index, added, total)
-        inside = (total >= least_sum) & (total <= most_sum)
-        flag[...] = jnp.maximum(flag[...], jnp.where(inside, 0.0, 1.0))
+    for case in range(heads):
+
+        @pl.when(z == case)
+        def _(case=case):
+            for index in range(heads):
+                added, total = accum[index], sums[index]
+                if index >= case ^ last:
+                    two_maps = two_maps_of(queries[index])
+                    limit = mine * rows if index == case ^ last else None
+                    more, weight = span_of(late_keys, late_values, 0, span, two_maps, limit)
+                    added = added + more
+                    total = total + weight
+                total = finish(index, added, total)
+                inside = (total >= least_sum) & (total <= most_sum)
+                flag[...] = jnp.maximum(flag[...], jnp.where(inside, 0.0, 1.0))
 
     @pl.when(jnp.max(flag[...]) > 0.0)
     def _():
+        all_keys[...] = keys[...]
+        all_values[...] = values[...]
+        begin = pl.multiple_of((z ^ last) * span, span)
+        all_keys[pl.ds(begin, span), :] = late_keys[...]
+        all_values[:, pl.ds(begin, span)] = late_values[...]
+
         def redo(index, carried):
-            two_maps = two_maps_of(index)
-            accum[...] = jnp.zeros_like(accum)
-            sums[...] = jnp.zeros_like(sums)
+            two_maps = two_maps_of(queries[index])
+            added_ref[...] = jnp.zeros_like(added_ref)
+            sums_ref[...] = jnp.zeros_like(sums_ref)
             peak[...] = jnp.full(peak.shape, masked_score, jnp.float32)
 
             def one_block(block, inner):
                 at = pl.multiple_of(block * rows, rows)
-                allowed = ahead_of(rows) <= (index * parts + mine - block) * rows
-                scores = jnp.where(allowed, scores_of(at, rows, two_maps), masked_score)
+                allowed = ahead_of(rows, rows) <= (index * parts + mine - block) * rows
+                scores = jnp.where(allowed, scores_of(all_keys, at, rows, two_maps), masked_score)
                 highest = jnp.maximum(peak[...], jnp.max(scores, axis=0, keepdims=True))
                 rescale = jnp.exp2(peak[...] - highest)
                 weights = jnp.where(allowed, jnp.exp2(scores - highest), 0.0)
-                sums[...] = sums[...] * rescale + fold(weights)
-                accum[...] = accum[...] * rescale + weighed(at, rows, weights)
+                sums_ref[...] = sums_ref[...] * rescale + fold(weights)
+                added_ref[...] = added_ref[...] * rescale + weighed(all_values, at, weights)
                 peak[...] = highest
                 return inner
 
             lax.fori_loop(0, index * parts + mine + 1, one_block, 0)
-            finish(index, accum[...], sums[...])
+            finish(index, added_ref[...], sums_ref[...])
             return carried
 
         lax.fori_loop(0, heads, redo, 0)
@@ -205,22 +266,22 @@
         outs[turn][...] = done[z ^ turn]
 
 
-def join_kernel(heads, place, *refs):
-    pieces, joined = refs[:heads], refs[heads]
+def project_out_kernel(heads, place, *refs):
+    mine, other = refs[:heads], refs[heads : 2 * heads]
+    out_mine, out_other, result, joined, staged, sems = refs[2 * heads :]
+    z = place[0]
     for turn in range(heads):
-        at = pl.multiple_of((place[0] ^ turn) * lanes, lanes)
-        joined[:, pl.ds(at, lanes)] = pieces[turn][...]
-
-
-def project_out_kernel(mine, other, out_mine, out_other, result, staged, sems):
+        at = pl.multiple_of((z ^ turn) * lanes, lanes)
+        joined[0, :, pl.ds(at, lanes)] = mine[turn][...]
+        joined[1, :, pl.ds(at, lanes)] = other[turn][...]
     copies = []
     pieces = sems.shape[0]
     wide = result.shape[1] // pieces
     for piece in range(pieces):
         columns = slice(piece * wide, (piece + 1) * wide)
-        total = jnp.dot(mine[...], out_mine[:, columns], preferred_element_type=jnp.float32)
+        total = jnp.dot(joined[0], out_mine[:, columns], preferred_element_type=jnp.float32)
         total = total + jnp.dot(
-            other[...], out_other[:, columns], preferred_element_type=jnp.float32
+            joined[1], out_other[:, columns], preferred_element_type=jnp.float32
         )
         staged[:, columns] = total.astype(jnp.bfloat16)
         copies.append(
@@ -303,52 +364,71 @@
     aside = [exchange(own[turn], 1) for turn in turns]
     below = [exchange(own[turn], across) for turn in turns]
     corner = [exchange(own[turn], 1 + across) for turn in turns]
-    blocks = own + aside + below + corner
-
+    sides = (own, aside, below, corner)
+    last = heads // 2
     tokens = heads * rows
+    early_blocks = [side[turn] for side in sides for turn in turns if turn != last]
+    state = [
+        jax.ShapeDtypeStruct((heads, rows, lanes), bf16),
+        jax.ShapeDtypeStruct((parts * tokens, lanes), bf16),
+        jax.ShapeDtypeStruct((lanes, parts * tokens), bf16),
+        jax.ShapeDtypeStruct((heads, lanes, 2 * rows), f32),
+        jax.ShapeDtypeStruct((heads, 8, 2 * rows), f32),
+    ]
+    state = pl.pallas_call(
+        functools.partial(early_kernel, heads, down, across),
+        out_shape=state,
+        in_specs=[in_smem()] + [in_vmem()] * (heads + len(early_blocks)),
+        out_specs=[in_vmem()] * 5,
+        compiler_params=pltpu.CompilerParams(vmem_limit_bytes=28 << 20),
+        cost_estimate=cost(3 * tokens * tokens * parts * lanes, 3 << 20),
+        name="attend_early",
+    )(place, *own_queries, *early_blocks)
     normed = pl.pallas_call(
-        functools.partial(attend_kernel, heads, down, across),
-        out_shape=[jax.ShapeDtypeStruct((rows, lanes), bf16)] * heads,
-        in_specs=[in_smem()] * 2 + [in_vmem()] * (1 + heads + heads * parts),
+        functools.partial(late_kernel, heads, down, across),
+        out_shape=[stripe] * heads,
+        in_specs=[in_smem()] * 2 + [in_vmem()] * (1 + parts + 5),
         out_specs=[in_vmem()] * heads,
         scratch_shapes=[
-            pltpu.VMEM((heads, rows, lanes), bf16),
+            pltpu.VMEM((parts * rows, lanes), bf16),
+            pltpu.VMEM((lanes, parts * rows), bf16),
             pltpu.VMEM((parts * tokens, lanes), bf16),
             pltpu.VMEM((lanes, parts * tokens), bf16),
+            pltpu.VMEM((heads, rows, lanes), bf16),
+            pltpu.VMEM((1, 2 * rows), f32),
             pltpu.VMEM((lanes, 2 * rows), f32),
             pltpu.VMEM((8, 2 * rows), f32),
             pltpu.VMEM((1, 2 * rows), f32),
-            pltpu.VMEM((heads, rows, lanes), bf16),
-            pltpu.VMEM((1, 2 * rows), f32),
         ],
-        compiler_params=pltpu.CompilerParams(vmem_limit_bytes=32 << 20),
-        cost_estimate=cost(4 * tokens * tokens * parts * lanes, 3 << 20),
-        name="attend",
-    )(place, lambdas, norm_gain.reshape(1, lanes), *own_queries, *blocks)
+        compiler_params=pltpu.CompilerParams(vmem_limit_bytes=28 << 20),
+        cost_estimate=cost(tokens * tokens * parts * lanes, 3 << 20),
+        name="attend_late",
+    )(
+        place,
+        lambdas,
+        norm_gain.reshape(1, lanes),
+        *[side[last] for side in sides],
+        *state,
+    )
 
     back = [normed[0]]
     for turn in turns[1:]:
         back.append(exchange(normed[turn], turn * parts))
-    joined = pl.pallas_call(
-        functools.partial(join_kernel, heads),
-        out_shape=jax.ShapeDtypeStruct((rows, heads * lanes), bf16),
-        in_specs=[in_smem()] + [in_vmem()] * heads,
-        out_specs=in_vmem(),
-        compiler_params=pltpu.CompilerParams(vmem_limit_bytes=4 << 20),
-        cost_estimate=cost(0, 2 * rows * heads * lanes),
-        name="join",
-    )(place, *back)
-    joined_other = lax.ppermute(joined, "tp", swap_core)
+    back_other = [lax.ppermute(back[turn], "tp", swap_core) for turn in turns]
     return pl.pallas_call(
-        project_out_kernel,
+        functools.partial(project_out_kernel, heads),
         out_shape=jax.ShapeDtypeStruct((rows, model), bf16),
-        in_specs=[in_vmem()] * 4,
+        in_specs=[in_smem()] + [in_vmem()] * (2 * heads + 2),
         out_specs=in_hbm(),
-        scratch_shapes=[pltpu.VMEM((rows, model), bf16), pltpu.SemaphoreType.DMA((4,))],
+        scratch_shapes=[
+            pltpu.VMEM((groups, rows, heads * lanes), bf16),
+            pltpu.VMEM((rows, model), bf16),
+            pltpu.SemaphoreType.DMA((4,)),
+        ],
         compiler_params=pltpu.CompilerParams(vmem_limit_bytes=16 << 20),
         cost_estimate=cost(2 * rows * model * groups * heads * lanes, 6 << 20),
         name="project_out",
-    )(joined, joined_other, out_proj, out_other)
+    )(place, *back, *back_other, out_proj, out_other)
 
 
 def gathered(

time: 102 us -> 85.4 us (0.84)
  waiting for transfers between devices: 36 us -> 14.1 us
  starting transfers between devices: 29.5 us -> 34.3 us
    ppermute x21, waiting for transfers between devices: 34.8 us -> 13.2 us  [exchange(): return lax.ppermute(array, 'sp', pairs)]
    ppermute x1 -> x4, starting transfers between devices: 3.87 us -> 11.6 us  [exchanged(): back_other = [lax.ppermute(back[turn], 'tp', swap_core) for turn in turns]]
    ppermute x21, starting transfers between devices: 25 us -> 21.9 us  [exchange(): return lax.ppermute(array, 'sp', pairs)]
  transfers between devices with their start and end apart: 23 -> 26, of which waited for: 12 -> 10; matrix products, arithmetic and copies ran while one was open for 0% -> 0% of each run, Pallas kernels for 33% -> 40%
where the time goes in v3:
time: 85.4 us; the launch traced here: 85.3 us
  Pallas kernels  36.6 us (43%)
  starting transfers between devices  34.3 us (40%)
  waiting for transfers between devices  14.1 us (17%)
    pallas_call x1, Pallas kernels, exchanged(): pl.pallas_call(functools.partial(late_kernel, heads, down, across), out_s...  23.1 us
    ppermute x21, starting transfers between devices, exchange(): return lax.ppermute(array, 'sp', pairs)  21.9 us
    ppermute x21, waiting for transfers between devices, exchange(): return lax.ppermute(array, 'sp', pairs)  13.2 us
    ppermute x4, starting transfers between devices, exchanged(): back_other = [lax.ppermute(back[turn], 'tp', swap_core) for turn in turns]  11.6 us
    pallas_call x1, Pallas kernels, exchanged(): pl.pallas_call(functools.partial(early_kernel, heads, down, across), out_...  4.98 us
    pallas_call x1, Pallas kernels, exchanged(): pl.pallas_call(functools.partial(key_value_kernel, heads), out_shape=[blo...  4.46 us
    pallas_call x1, Pallas kernels, exchanged(): pl.pallas_call(functools.partial(project_out_kernel, heads), out_shape=ja...  2.63 us
  transfers between devices with their start and end apart: 26, of which 10 were waited for; matrix products, arithmetic and copies ran while one was open for 0% of the time, Pallas kernels for 40%

profile of v3, /device:TPU:7, one launch (start us, length us, event | category | flops | bytes accessed | tf_op | source)
XLA Modules:
  0.0 85.3 jit_solution(7986154231158310462)
XLA Ops:
  0.0 0.7 collective-permute-start.25
  0.8 4.5 %project_keys.1 = (bf16[512,128]{1,0:T(8,128)(2,1)S(1)}, bf16[512,128]{1,0:T(8,128)(2,1)S(1)}, bf16[512,128]{1,0:T(8,128)(2,1)S(1)}, bf16[512,128]{1,0:T(8,128)(...) custom-call(s32[3]{0:T(128)S(1)} %pad_add_fusion.place, ...), custom_call_target="tpu_custom_call" | custom-call | flops 1073741824 | bytes 7340032 | tf_op jit(solution)/shard_map/project_keys/pallas_call | solution.py:330
  5.2 1.4 %project_queries.1 = (bf16[256,128]{1,0:T(8,128)(2,1)S(1)}, bf16[256,128]{1,0:T(8,128)(2,1)S(1)}, bf16[256,128]{1,0:T(8,128)(2,1)S(1)}, bf16[256,128]{1,0:T(8,128)(2,1)S(1)}) custom-call(s32[3]{0:T(128)S(1)} %pad_add_fusion.place, bf16[256,2048]{1,0:T(8,128)(2,1)S(1)} %get-tuple-element.26.hidden, bf16[2048,256]{1,0:T(8,128)(2,1)S(1)} %get-tuple-element.27.query_one, ...), custom_call_target="tpu_custom_call" | custom-call | flops 536870912 | bytes 4194304 | tf_op jit(solution)/shard_map/project_queries/pallas_call | solution.py:349
  6.7 1.4 %collective-permute-start.4 = (bf16[256,128]{1,0:T(8,128)(2,1)S(1)}, bf16[256,128]{1,0:T(8,128)(2,1)S(1)}, u32[]{:S(2)}, u32[]{:S(2)}) collective-permute-start(bf16[256,128]{1,0:T(8,128)(2,1)S(1)} %get-tuple-element.30), channel_id=1, source_target_pairs={{0,8},{2,10},{4,12},{6,14},{8,0},{10,2},{12,4},{14,6},{16,24},{18,... | collective-permute-start | bytes 196616 | tf_op jit(solution)/shard_map/ppermute | solution.py:321
  8.0 2.3 %collective-permute-start.5 = (bf16[256,128]{1,0:T(8,128)(2,1)S(1)}, bf16[256,128]{1,0:T(8,128)(2,1)S(1)}, u32[]{:S(2)}, u32[]{:S(2)}) collective-permute-start(bf16[256,128]{1,0:T(8,128)(2,1)S(1)} %get-tuple-element.31), channel_id=1, source_target_pairs={{0,16},{2,18},{4,20},{6,22},{8,24},{10,26},{12,28},{14,30},{16,0},... | collective-permute-start | bytes 196616 | tf_op jit(solution)/shard_map/ppermute | solution.py:321
  10.3 0.3 collective-permute-start.7
  10.7 3.0 %collective-permute-start.8 = (bf16[512,128]{1,0:T(8,128)(2,1)S(1)}, bf16[512,128]{1,0:T(8,128)(2,1)S(1)}, u32[]{:S(2)}, u32[]{:S(2)}) collective-permute-start(bf16[512,128]{1,0:T(8,128)(2,1)S(1)} %get-tuple-element.35), channel_id=1, source_target_pairs={{0,24},{2,26},{4,28},{6,30},{8,16},{10,18},{12,20},{14,22},{16,8},... | collective-permute-start | bytes 393224 | tf_op jit(solution)/shard_map/ppermute | solution.py:321
  13.9 1.5 %collective-permute-done.6.refs_3_ = bf16[256,128]{1,0:T(8,128)(2,1)S(1)} collective-permute-done((bf16[256,128]{1,0:T(8,128)(2,1)S(1)}, bf16[256,128]{1,0:T(8,128)(2,1)S(1)}, u32[]{:S(2)}, u32[]{:S(2)}) %collective-permute-start.6) | collective-permute-done | bytes 65568 | tf_op jit(solution)/shard_map/ppermute | solution.py:321
  15.8 1.0 %collective-permute-start.9 = (bf16[512,128]{1,0:T(8,128)(2,1)S(1)}, bf16[512,128]{1,0:T(8,128)(2,1)S(1)}, u32[]{:S(2)}, u32[]{:S(2)}) collective-permute-start(bf16[512,128]{1,0:T(8,128)(2,1)S(1)} %get-tuple-element.33.refs_4_), channel_id=1, source_target_pairs={{0,2},{2,0},{4,6},{6,4},{8,10},{10,8},{12,14},{14,12},{16,18},{18,... | collective-permute-start | bytes 393224 | tf_op jit(solution)/shard_map/ppermute | solution.py:321
  16.8 4.1 %collective-permute-done.8.refs_6_ = bf16[512,128]{1,0:T(8,128)(2,1)S(1)} collective-permute-done((bf16[512,128]{1,0:T(8,128)(2,1)S(1)}, bf16[512,128]{1,0:T(8,128)(2,1)S(1)}, u32[]{:S(2)}, u32[]{:S(2)}) %collective-permute-start.8) | collective-permute-done | bytes 131104 | tf_op jit(solution)/shard_map/ppermute | solution.py:321
  20.9 2.6 %collective-permute-start = (bf16[512,128]{1,0:T(8,128)(2,1)S(1)}, bf16[512,128]{1,0:T(8,128)(2,1)S(1)}, u32[]{:S(2)}, u32[]{:S(2)}) collective-permute-start(bf16[512,128]{1,0:T(8,128)(2,1)S(1)} %get-tuple-element.25), channel_id=1, source_target_pairs={{0,16},{2,18},{4,20},{6,22},{8,24},{10,26},{12,28},{14,30},{16,0},... | collective-permute-start | bytes 393224 | tf_op jit(solution)/shard_map/ppermute | solution.py:321
  23.7 1.2 %collective-permute-start.11 = (bf16[512,128]{1,0:T(8,128)(2,1)S(1)}, bf16[512,128]{1,0:T(8,128)(2,1)S(1)}, u32[]{:S(2)}, u32[]{:S(2)}) collective-permute-start(bf16[512,128]{1,0:T(8,128)(2,1)S(1)} %collective-permute-done.8.refs_6_), channel_id=1, source_target_pairs={{0,2},{2,0},{4,6},{6,4},{8,10},{10,8},{12,14},{14,12},{16,18},{18,... | collective-permute-start | bytes 393224 | tf_op jit(solution)/shard_map/ppermute | solution.py:321
  25.1 0.6 collective-permute-done.refs_0_
  25.8 0.6 collective-permute-start.14
  26.4 1.2 %collective-permute-done.10.refs_8_ = bf16[512,128]{1,0:T(8,128)(2,1)S(1)} collective-permute-done((bf16[512,128]{1,0:T(8,128)(2,1)S(1)}, bf16[512,128]{1,0:T(8,128)(2,1)S(1)}, u32[]{:S(2)}, u32[]{:S(2)}) %collective-permute-start.10) | collective-permute-done | bytes 131104 | tf_op jit(solution)/shard_map/ppermute | solution.py:321
  27.7 2.1 %collective-permute-done.11.refs_9_ = bf16[512,128]{1,0:T(8,128)(2,1)S(1)} collective-permute-done((bf16[512,128]{1,0:T(8,128)(2,1)S(1)}, bf16[512,128]{1,0:T(8,128)(2,1)S(1)}, u32[]{:S(2)}, u32[]{:S(2)}) %collective-permute-start.11) | collective-permute-done | bytes 131104 | tf_op jit(solution)/shard_map/ppermute | solution.py:321
  30.1 1.2 %collective-permute-start.1 = (bf16[512,128]{1,0:T(8,128)(2,1)S(1)}, bf16[512,128]{1,0:T(8,128)(2,1)S(1)}, u32[]{:S(2)}, u32[]{:S(2)}) collective-permute-start(bf16[512,128]{1,0:T(8,128)(2,1)S(1)} %collective-permute-done.refs_0_), channel_id=1, source_target_pairs={{0,2},{2,0},{4,6},{6,4},{8,10},{10,8},{12,14},{14,12},{16,18},{18,... | collective-permute-start | bytes 393224 | tf_op jit(solution)/shard_map/ppermute | solution.py:321
  31.3 1.2 %collective-permute-start.2 = (bf16[512,128]{1,0:T(8,128)(2,1)S(1)}, bf16[512,128]{1,0:T(8,128)(2,1)S(1)}, u32[]{:S(2)}, u32[]{:S(2)}) collective-permute-start(bf16[512,128]{1,0:T(8,128)(2,1)S(1)} %collective-permute-done.refs_0_), channel_id=1, source_target_pairs={{0,4},{2,6},{4,0},{6,2},{8,12},{10,14},{12,8},{14,10},{16,20},{18,... | collective-permute-start | bytes 393224 | tf_op jit(solution)/shard_map/ppermute | solution.py:321
  32.5 0.4 collective-permute-done.16.refs_14_
  32.9 0.9 %collective-permute-start.3 = (bf16[512,128]{1,0:T(8,128)(2,1)S(1)}, bf16[512,128]{1,0:T(8,128)(2,1)S(1)}, u32[]{:S(2)}, u32[]{:S(2)}) collective-permute-start(bf16[512,128]{1,0:T(8,128)(2,1)S(1)} %collective-permute-done.refs_0_), channel_id=1, source_target_pairs={{0,6},{2,4},{4,2},{6,0},{8,14},{10,12},{12,10},{14,8},{16,22},{18,... | collective-permute-start | bytes 393224 | tf_op jit(solution)/shard_map/ppermute | solution.py:321
  33.9 0.7 collective-permute-done.17.refs_15_
  34.6 5.0 %attend_early.1 = (bf16[4,256,128]{2,1,0:T(8,128)(2,1)S(1)}, bf16[4096,128]{1,0:T(8,128)(2,1)S(1)}, bf16[128,4096]{1,0:T(8,128)(2,1)S(1)}, f32[4,128,512]{2,1,0:T(8,128)S(1)}, f32[4,8,512]{2,1,0:T(8,128)S(1)}) custom-call(s32[3]{0:T(128)S(1)} %pad_add_fusion.place, bf16[256,128]{1,0:T(8,128)(2,1)S(1)} %get-tuple-element.29.refs_0_, ...), custom_call_target="tpu_custom_call" | custom-call | flops 1610612736 | bytes 3145728 | tf_op jit(solution)/shard_map/attend_early/pallas_call | solution.py:378
  39.6 2.3 %collective-permute-done.2.refs_2_ = bf16[512,128]{1,0:T(8,128)(2,1)S(1)} collective-permute-done((bf16[512,128]{1,0:T(8,128)(2,1)S(1)}, bf16[512,128]{1,0:T(8,128)(2,1)S(1)}, u32[]{:S(2)}, u32[]{:S(2)}) %collective-permute-start.2) | collective-permute-done | bytes 131104 | tf_op jit(solution)/shard_map/ppermute | solution.py:321
  41.9 23.1 %attend_late.1 = (bf16[256,128]{1,0:T(8,128)(2,1)S(1)}, bf16[256,128]{1,0:T(8,128)(2,1)S(1)}, bf16[256,128]{1,0:T(8,128)(2,1)S(1)}, bf16[256,128]{1,0:T(8,128)(2,1)S(1)}) custom-call(s32[3]{0:T(128)S(1)} %pad_add_fusion.place, f32[4]{0:T(128)S(1)} %copy-done.1, f32[1,128]{1,0:T(1,128)S(1)} %bitcast.4, bf16[512,128]{1,0:T(8,128)(2,1)S(1)} %collective-permute-done.refs_0_, ...), custom_call_target="tpu_custom_call" | custom-call | flops 536870912 | bytes 3145728 | tf_op jit(solution)/shard_map/attend_late/pallas_call | solution.py:387
  65.1 2.7 %collective-permute-start.18 = (bf16[256,128]{1,0:T(8,128)(2,1)S(1)}, bf16[256,128]{1,0:T(8,128)(2,1)S(1)}, u32[]{:S(2)}, u32[]{:S(2)}) collective-permute-start(bf16[256,128]{1,0:T(8,128)(2,1)S(1)} %get-tuple-element.42), channel_id=1, source_target_pairs={{0,8},{2,10},{4,12},{6,14},{8,0},{10,2},{12,4},{14,6},{16,24},{18,... | collective-permute-start | bytes 196616 | tf_op jit(solution)/shard_map/ppermute | solution.py:321
  67.8 0.8 collective-permute-start.19
  68.6 1.4 %collective-permute-start.20 = (bf16[256,128]{1,0:T(8,128)(2,1)S(1)}, bf16[256,128]{1,0:T(8,128)(2,1)S(1)}, u32[]{:S(2)}, u32[]{:S(2)}) collective-permute-start(bf16[256,128]{1,0:T(8,128)(2,1)S(1)} %get-tuple-element.44), channel_id=1, source_target_pairs={{0,24},{2,26},{4,28},{6,30},{8,16},{10,18},{12,20},{14,22},{16,8},... | collective-permute-start | bytes 196616 | tf_op jit(solution)/shard_map/ppermute | solution.py:321
  70.0 7.0 %collective-permute-start.21 = (bf16[256,128]{1,0:T(8,128)(2,1)S(1)}, bf16[256,128]{1,0:T(8,128)(2,1)S(1)}, u32[]{:S(2)}, u32[]{:S(2)}) collective-permute-start(bf16[256,128]{1,0:T(8,128)(2,1)S(1)} %get-tuple-element.41.refs_0_), channel_id=1, source_target_pairs={{0,1},{1,0},{2,3},{3,2},{4,5},{5,4},{6,7},{7,6},{8,9},{9,8},{10,11... | collective-permute-start | bytes 196616 | tf_op jit(solution)/shard_map/ppermute | solution.py:417
  77.0 0.8 collective-permute-start.23
  77.8 3.8 %collective-permute-start.24 = (bf16[256,128]{1,0:T(8,128)(2,1)S(1)}, bf16[256,128]{1,0:T(8,128)(2,1)S(1)}, u32[]{:S(2)}, u32[]{:S(2)}) collective-permute-start(bf16[256,128]{1,0:T(8,128)(2,1)S(1)} %collective-permute-done.20.refs_3_), channel_id=1, source_target_pairs={{0,1},{1,0},{2,3},{3,2},{4,5},{5,4},{6,7},{7,6},{8,9},{9,8},{10,11... | collective-permute-start | bytes 196616 | tf_op jit(solution)/shard_map/ppermute | solution.py:417
  81.6 0.9 %collective-permute-done.24.refs_7_ = bf16[256,128]{1,0:T(8,128)(2,1)S(1)} collective-permute-done((bf16[256,128]{1,0:T(8,128)(2,1)S(1)}, bf16[256,128]{1,0:T(8,128)(2,1)S(1)}, u32[]{:S(2)}, u32[]{:S(2)}) %collective-permute-start.24) | collective-permute-done | bytes 65568 | tf_op jit(solution)/shard_map/ppermute | solution.py:417
  82.5 2.6 %project_out.1 = bf16[256,2048]{1,0:T(8,128)(2,1)} custom-call(s32[3]{0:T(128)S(1)} %pad_add_fusion.place, bf16[256,128]{1,0:T(8,128)(2,1)S(1)} %get-tuple-element.41.refs_0_, bf16[256,128]{1,0:T(8,128)(2,1)S(1)} %collective-permute-done.18.refs_1_, bf16[256,128]{1,0:T(8,128)(2,1)S(1)} %collective-permute-done.19.refs_2_, ...), custom_call_target="tpu_custom_call" | custom-call | flops 1073741824 | bytes 6291456 | tf_op jit(solution)/shard_map/project_out/pallas_call | solution.py:418
  (32 shorter events, 1.7 us)
Async XLA Ops:
  0.0 82.5 %collective-permute-start.25 = (bf16[512,2048]{1,0:T(8,128)(2,1)}, bf16[512,2048]{1,0:T(8,128)(2,1)S(1)}, u32[]{:S(2)}, u32[]{:S(2)}) collective-permute-start(bf16[512,2048]{1,0:T(8,128)(2,1)} %refs_8_.1), channel_id=1, source_target_pairs={{0,1},{1,0},{2,3},{3,2},{4,5},{5,4},{6,7},{7,6},{8,9},{9,8},{10,11... | collective-permute-start | bytes 6291464 | tf_op jit(solution)/shard_map/ppermute | solution.py:363
  6.7 4.0 %collective-permute-start.4 = (bf16[256,128]{1,0:T(8,128)(2,1)S(1)}, bf16[256,128]{1,0:T(8,128)(2,1)S(1)}, u32[]{:S(2)}, u32[]{:S(2)}) collective-permute-start(bf16[256,128]{1,0:T(8,128)(2,1)S(1)} %get-tuple-element.30), channel_id=1, source_target_pairs={{0,8},{2,10},{4,12},{6,14},{8,0},{10,2},{12,4},{14,6},{16,24},{18,... | collective-permute-start | bytes 196616 | tf_op jit(solution)/shard_map/ppermute | solution.py:321
  8.0 5.7 %collective-permute-start.5 = (bf16[256,128]{1,0:T(8,128)(2,1)S(1)}, bf16[256,128]{1,0:T(8,128)(2,1)S(1)}, u32[]{:S(2)}, u32[]{:S(2)}) collective-permute-start(bf16[256,128]{1,0:T(8,128)(2,1)S(1)} %get-tuple-element.31), channel_id=1, source_target_pairs={{0,16},{2,18},{4,20},{6,22},{8,24},{10,26},{12,28},{14,30},{16,0},... | collective-permute-start | bytes 196616 | tf_op jit(solution)/shard_map/ppermute | solution.py:321
  10.3 5.0 %collective-permute-start.6 = (bf16[256,128]{1,0:T(8,128)(2,1)S(1)}, bf16[256,128]{1,0:T(8,128)(2,1)S(1)}, u32[]{:S(2)}, u32[]{:S(2)}) collective-permute-start(bf16[256,128]{1,0:T(8,128)(2,1)S(1)} %get-tuple-element.32), channel_id=1, source_target_pairs={{0,24},{2,26},{4,28},{6,30},{8,16},{10,18},{12,20},{14,22},{16,8},... | collective-permute-start | bytes 196616 | tf_op jit(solution)/shard_map/ppermute | solution.py:321
  10.3 5.5 %collective-permute-start.7 = (bf16[512,128]{1,0:T(8,128)(2,1)S(1)}, bf16[512,128]{1,0:T(8,128)(2,1)S(1)}, u32[]{:S(2)}, u32[]{:S(2)}) collective-permute-start(bf16[512,128]{1,0:T(8,128)(2,1)S(1)} %get-tuple-element.34), channel_id=1, source_target_pairs={{0,8},{2,10},{4,12},{6,14},{8,0},{10,2},{12,4},{14,6},{16,24},{18,... | collective-permute-start | bytes 393224 | tf_op jit(solution)/shard_map/ppermute | solution.py:321
  10.7 10.2 %collective-permute-start.8 = (bf16[512,128]{1,0:T(8,128)(2,1)S(1)}, bf16[512,128]{1,0:T(8,128)(2,1)S(1)}, u32[]{:S(2)}, u32[]{:S(2)}) collective-permute-start(bf16[512,128]{1,0:T(8,128)(2,1)S(1)} %get-tuple-element.35), channel_id=1, source_target_pairs={{0,24},{2,26},{4,28},{6,30},{8,16},{10,18},{12,20},{14,22},{16,8},... | collective-permute-start | bytes 393224 | tf_op jit(solution)/shard_map/ppermute | solution.py:321
  13.7 9.7 %collective-permute-start.12 = (bf16[512,128]{1,0:T(8,128)(2,1)S(1)}, bf16[512,128]{1,0:T(8,128)(2,1)S(1)}, u32[]{:S(2)}, u32[]{:S(2)}) collective-permute-start(bf16[512,128]{1,0:T(8,128)(2,1)S(1)} %get-tuple-element.33.refs_4_), channel_id=1, source_target_pairs={{0,4},{2,6},{4,0},{6,2},{8,12},{10,14},{12,8},{14,10},{16,20},{18,... | collective-permute-start | bytes 393224 | tf_op jit(solution)/shard_map/ppermute | solution.py:321
  15.4 8.3 %collective-permute-start.15 = (bf16[512,128]{1,0:T(8,128)(2,1)S(1)}, bf16[512,128]{1,0:T(8,128)(2,1)S(1)}, u32[]{:S(2)}, u32[]{:S(2)}) collective-permute-start(bf16[512,128]{1,0:T(8,128)(2,1)S(1)} %get-tuple-element.33.refs_4_), channel_id=1, source_target_pairs={{0,6},{2,4},{4,2},{6,0},{8,14},{10,12},{12,10},{14,8},{16,22},{18,... | collective-permute-start | bytes 393224 | tf_op jit(solution)/shard_map/ppermute | solution.py:321
  15.8 9.1 %collective-permute-start.9 = (bf16[512,128]{1,0:T(8,128)(2,1)S(1)}, bf16[512,128]{1,0:T(8,128)(2,1)S(1)}, u32[]{:S(2)}, u32[]{:S(2)}) collective-permute-start(bf16[512,128]{1,0:T(8,128)(2,1)S(1)} %get-tuple-element.33.refs_4_), channel_id=1, source_target_pairs={{0,2},{2,0},{4,6},{6,4},{8,10},{10,8},{12,14},{14,12},{16,18},{18,... | collective-permute-start | bytes 393224 | tf_op jit(solution)/shard_map/ppermute | solution.py:321
  20.9 4.9 %collective-permute-start = (bf16[512,128]{1,0:T(8,128)(2,1)S(1)}, bf16[512,128]{1,0:T(8,128)(2,1)S(1)}, u32[]{:S(2)}, u32[]{:S(2)}) collective-permute-start(bf16[512,128]{1,0:T(8,128)(2,1)S(1)} %get-tuple-element.25), channel_id=1, source_target_pairs={{0,16},{2,18},{4,20},{6,22},{8,24},{10,26},{12,28},{14,30},{16,0},... | collective-permute-start | bytes 393224 | tf_op jit(solution)/shard_map/ppermute | solution.py:321
  23.4 4.1 %collective-permute-start.10 = (bf16[512,128]{1,0:T(8,128)(2,1)S(1)}, bf16[512,128]{1,0:T(8,128)(2,1)S(1)}, u32[]{:S(2)}, u32[]{:S(2)}) collective-permute-start(bf16[512,128]{1,0:T(8,128)(2,1)S(1)} %collective-permute-done.7.refs_5_), channel_id=1, source_target_pairs={{0,2},{2,0},{4,6},{6,4},{8,10},{10,8},{12,14},{14,12},{16,18},{18,... | collective-permute-start | bytes 393224 | tf_op jit(solution)/shard_map/ppermute | solution.py:321
  23.7 6.2 %collective-permute-start.11 = (bf16[512,128]{1,0:T(8,128)(2,1)S(1)}, bf16[512,128]{1,0:T(8,128)(2,1)S(1)}, u32[]{:S(2)}, u32[]{:S(2)}) collective-permute-start(bf16[512,128]{1,0:T(8,128)(2,1)S(1)} %collective-permute-done.8.refs_6_), channel_id=1, source_target_pairs={{0,2},{2,0},{4,6},{6,4},{8,10},{10,8},{12,14},{14,12},{16,18},{18,... | collective-permute-start | bytes 393224 | tf_op jit(solution)/shard_map/ppermute | solution.py:321
  24.9 5.2 %collective-permute-start.13 = (bf16[512,128]{1,0:T(8,128)(2,1)S(1)}, bf16[512,128]{1,0:T(8,128)(2,1)S(1)}, u32[]{:S(2)}, u32[]{:S(2)}) collective-permute-start(bf16[512,128]{1,0:T(8,128)(2,1)S(1)} %collective-permute-done.7.refs_5_), channel_id=1, source_target_pairs={{0,4},{2,6},{4,0},{6,2},{8,12},{10,14},{12,8},{14,10},{16,20},{18,... | collective-permute-start | bytes 393224 | tf_op jit(solution)/shard_map/ppermute | solution.py:321
  25.8 5.5 %collective-permute-start.14 = (bf16[512,128]{1,0:T(8,128)(2,1)S(1)}, bf16[512,128]{1,0:T(8,128)(2,1)S(1)}, u32[]{:S(2)}, u32[]{:S(2)}) collective-permute-start(bf16[512,128]{1,0:T(8,128)(2,1)S(1)} %collective-permute-done.8.refs_6_), channel_id=1, source_target_pairs={{0,4},{2,6},{4,0},{6,2},{8,12},{10,14},{12,8},{14,10},{16,20},{18,... | collective-permute-start | bytes 393224 | tf_op jit(solution)/shard_map/ppermute | solution.py:321
  27.5 5.4 %collective-permute-start.16 = (bf16[512,128]{1,0:T(8,128)(2,1)S(1)}, bf16[512,128]{1,0:T(8,128)(2,1)S(1)}, u32[]{:S(2)}, u32[]{:S(2)}) collective-permute-start(bf16[512,128]{1,0:T(8,128)(2,1)S(1)} %collective-permute-done.7.refs_5_), channel_id=1, source_target_pairs={{0,6},{2,4},{4,2},{6,0},{8,14},{10,12},{12,10},{14,8},{16,22},{18,... | collective-permute-start | bytes 393224 | tf_op jit(solution)/shard_map/ppermute | solution.py:321
  29.9 4.7 %collective-permute-start.17 = (bf16[512,128]{1,0:T(8,128)(2,1)S(1)}, bf16[512,128]{1,0:T(8,128)(2,1)S(1)}, u32[]{:S(2)}, u32[]{:S(2)}) collective-permute-start(bf16[512,128]{1,0:T(8,128)(2,1)S(1)} %collective-permute-done.8.refs_6_), channel_id=1, source_target_pairs={{0,6},{2,4},{4,2},{6,0},{8,14},{10,12},{12,10},{14,8},{16,22},{18,... | collective-permute-start | bytes 393224 | tf_op jit(solution)/shard_map/ppermute | solution.py:321
  30.1 9.5 %collective-permute-start.1 = (bf16[512,128]{1,0:T(8,128)(2,1)S(1)}, bf16[512,128]{1,0:T(8,128)(2,1)S(1)}, u32[]{:S(2)}, u32[]{:S(2)}) collective-permute-start(bf16[512,128]{1,0:T(8,128)(2,1)S(1)} %collective-permute-done.refs_0_), channel_id=1, source_target_pairs={{0,2},{2,0},{4,6},{6,4},{8,10},{10,8},{12,14},{14,12},{16,18},{18,... | collective-permute-start | bytes 393224 | tf_op jit(solution)/shard_map/ppermute | solution.py:321
  31.3 10.6 %collective-permute-start.2 = (bf16[512,128]{1,0:T(8,128)(2,1)S(1)}, bf16[512,128]{1,0:T(8,128)(2,1)S(1)}, u32[]{:S(2)}, u32[]{:S(2)}) collective-permute-start(bf16[512,128]{1,0:T(8,128)(2,1)S(1)} %collective-permute-done.refs_0_), channel_id=1, source_target_pairs={{0,4},{2,6},{4,0},{6,2},{8,12},{10,14},{12,8},{14,10},{16,20},{18,... | collective-permute-start | bytes 393224 | tf_op jit(solution)/shard_map/ppermute | solution.py:321
  32.9 9.0 %collective-permute-start.3 = (bf16[512,128]{1,0:T(8,128)(2,1)S(1)}, bf16[512,128]{1,0:T(8,128)(2,1)S(1)}, u32[]{:S(2)}, u32[]{:S(2)}) collective-permute-start(bf16[512,128]{1,0:T(8,128)(2,1)S(1)} %collective-permute-done.refs_0_), channel_id=1, source_target_pairs={{0,6},{2,4},{4,2},{6,0},{8,14},{10,12},{12,10},{14,8},{16,22},{18,... | collective-permute-start | bytes 393224 | tf_op jit(solution)/shard_map/ppermute | solution.py:321
  34.6 7.3 %copy-start.1 = (f32[4]{0:T(128)S(1)}, f32[4]{0:T(128)}, u32[]{:S(2)}) copy-start(f32[4]{0:T(128)} %lambdas.1) | copy-start | bytes 52
  34.6 7.3 %copy-start.2 = (f32[128]{0:T(128)S(1)}, f32[128]{0:T(128)}, u32[]{:S(2)}) copy-start(f32[128]{0:T(128)} %param.16) | copy-start | bytes 1540
  39.6 42.9 %copy-start = (bf16[512,2048]{1,0:T(8,128)(2,1)S(1)}, bf16[512,2048]{1,0:T(8,128)(2,1)}, u32[]{:S(2)}) copy-start(bf16[512,2048]{1,0:T(8,128)(2,1)} %refs_8_.1) | copy-start | bytes 6291460
  65.1 11.9 %collective-permute-start.18 = (bf16[256,128]{1,0:T(8,128)(2,1)S(1)}, bf16[256,128]{1,0:T(8,128)(2,1)S(1)}, u32[]{:S(2)}, u32[]{:S(2)}) collective-permute-start(bf16[256,128]{1,0:T(8,128)(2,1)S(1)} %get-tuple-element.42), channel_id=1, source_target_pairs={{0,8},{2,10},{4,12},{6,14},{8,0},{10,2},{12,4},{14,6},{16,24},{18,... | collective-permute-start | bytes 196616 | tf_op jit(solution)/shard_map/ppermute | solution.py:321
  67.8 9.2 %collective-permute-start.19 = (bf16[256,128]{1,0:T(8,128)(2,1)S(1)}, bf16[256,128]{1,0:T(8,128)(2,1)S(1)}, u32[]{:S(2)}, u32[]{:S(2)}) collective-permute-start(bf16[256,128]{1,0:T(8,128)(2,1)S(1)} %get-tuple-element.43), channel_id=1, source_target_pairs={{0,16},{2,18},{4,20},{6,22},{8,24},{10,26},{12,28},{14,30},{16,0},... | collective-permute-start | bytes 196616 | tf_op jit(solution)/shard_map/ppermute | solution.py:321
  68.6 9.2 %collective-permute-start.20 = (bf16[256,128]{1,0:T(8,128)(2,1)S(1)}, bf16[256,128]{1,0:T(8,128)(2,1)S(1)}, u32[]{:S(2)}, u32[]{:S(2)}) collective-permute-start(bf16[256,128]{1,0:T(8,128)(2,1)S(1)} %get-tuple-element.44), channel_id=1, source_target_pairs={{0,24},{2,26},{4,28},{6,30},{8,16},{10,18},{12,20},{14,22},{16,8},... | collective-permute-start | bytes 196616 | tf_op jit(solution)/shard_map/ppermute | solution.py:321
  70.0 11.6 %collective-permute-start.21 = (bf16[256,128]{1,0:T(8,128)(2,1)S(1)}, bf16[256,128]{1,0:T(8,128)(2,1)S(1)}, u32[]{:S(2)}, u32[]{:S(2)}) collective-permute-start(bf16[256,128]{1,0:T(8,128)(2,1)S(1)} %get-tuple-element.41.refs_0_), channel_id=1, source_target_pairs={{0,1},{1,0},{2,3},{3,2},{4,5},{5,4},{6,7},{7,6},{8,9},{9,8},{10,11... | collective-permute-start | bytes 196616 | tf_op jit(solution)/shard_map/ppermute | solution.py:417
  77.0 4.6 %collective-permute-start.22 = (bf16[256,128]{1,0:T(8,128)(2,1)S(1)}, bf16[256,128]{1,0:T(8,128)(2,1)S(1)}, u32[]{:S(2)}, u32[]{:S(2)}) collective-permute-start(bf16[256,128]{1,0:T(8,128)(2,1)S(1)} %collective-permute-done.18.refs_1_), channel_id=1, source_target_pairs={{0,1},{1,0},{2,3},{3,2},{4,5},{5,4},{6,7},{7,6},{8,9},{9,8},{10,11... | collective-permute-start | bytes 196616 | tf_op jit(solution)/shard_map/ppermute | solution.py:417
  77.0 4.6 %collective-permute-start.23 = (bf16[256,128]{1,0:T(8,128)(2,1)S(1)}, bf16[256,128]{1,0:T(8,128)(2,1)S(1)}, u32[]{:S(2)}, u32[]{:S(2)}) collective-permute-start(bf16[256,128]{1,0:T(8,128)(2,1)S(1)} %collective-permute-done.19.refs_2_), channel_id=1, source_target_pairs={{0,1},{1,0},{2,3},{3,2},{4,5},{5,4},{6,7},{7,6},{8,9},{9,8},{10,11... | collective-permute-start | bytes 196616 | tf_op jit(solution)/shard_map/ppermute | solution.py:417
  77.8 4.7 %collective-permute-start.24 = (bf16[256,128]{1,0:T(8,128)(2,1)S(1)}, bf16[256,128]{1,0:T(8,128)(2,1)S(1)}, u32[]{:S(2)}, u32[]{:S(2)}) collective-permute-start(bf16[256,128]{1,0:T(8,128)(2,1)S(1)} %collective-permute-done.20.refs_3_), channel_id=1, source_target_pairs={{0,1},{1,0},{2,3},{3,2},{4,5},{5,4},{6,7},{7,6},{8,9},{9,8},{10,11... | collective-permute-start | bytes 196616 | tf_op jit(solution)/shard_map/ppermute | solution.py:417

commit v4 on v3

--- a/solution.py
+++ b/solution.py
@@ -15,6 +15,8 @@
 least_sum = 2.0**-90
 most_sum = 2.0**100
 lanes = 128
+key_pieces = 4
+start_queries = 0
 
 
 def cost(flops, moved):
@@ -44,13 +46,11 @@
     return tiles
 
 
-def fetch(arrays, buffers, sems):
-    copies = []
-    for index, (array, buffer) in enumerate(zip(arrays, buffers)):
-        copies.append(pltpu.make_async_copy(array, buffer, sems.at[index]))
-    for copy in copies:
-        copy.start()
-    return copies
+def fetch_later(arrays, buffers, sems, row):
+    return [
+        pltpu.make_async_copy(array, buffer, sems.at[row, number])
+        for number, (array, buffer) in enumerate(zip(arrays, buffers))
+    ]
 
 
 def turned_into(stage, head, at, tile):
@@ -64,32 +64,47 @@
     arrays, outs = refs[:6], refs[6 : 6 + heads]
     hidden, query_one, query_two = refs[6 + heads : 9 + heads]
     key_one, key_two, value_proj, stage, sems = refs[9 + heads :]
-    buffers = (hidden, key_one, key_two, value_proj, query_one, query_two)
-    copies = fetch(arrays, buffers, sems)
-    rows = hidden.shape[0]
-    copies[0].wait()
-    copies[1].wait()
-    first = jnp.dot(hidden[...], key_one[...], preferred_element_type=jnp.float32)
-    copies[2].wait()
-    second = jnp.dot(hidden[...], key_two[...], preferred_element_type=jnp.float32)
+    rows, model = hidden.shape
+    pieces = sems.shape[0] - 1
+    deep = model // pieces
+    copies = []
+    for piece in range(pieces):
+        cut = slice(piece * deep, (piece + 1) * deep)
+        pairs = [(arrays[0].at[:, cut], hidden.at[:, cut])]
+        for array, buffer in zip(arrays[1:4], (key_one, key_two, value_proj)):
+            pairs.append((array.at[cut, :], buffer.at[cut, :]))
+        for number, (source, target) in enumerate(pairs):
+            copies.append(pltpu.make_async_copy(source, target, sems.at[piece, number]))
+            copies[-1].start()
+    later = fetch_later(arrays[4:], (query_one, query_two), sems, pieces)
+    sums = [0.0, 0.0, 0.0]
+    for piece in range(pieces):
+        for copy in copies[4 * piece : 4 * piece + 4]:
+            copy.wait()
+        if piece == start_queries:
+            for copy in later:
+                copy.start()
+        cut = slice(piece * deep, (piece + 1) * deep)
+        tokens = hidden[:, cut]
+        for number, buffer in enumerate((key_one, key_two, value_proj)):
+            sums[number] += jnp.dot(tokens, buffer[cut, :], preferred_element_type=jnp.float32)
+    first, second, values = sums
     for head, tile in enumerate(pair_up(first, second, heads)):
         stage[head, :rows, :] = tile.astype(jnp.bfloat16)
-    copies[3].wait()
-    values = jnp.dot(hidden[...], value_proj[...], preferred_element_type=jnp.float32)
     for head in range(heads):
         turned_into(stage, head, rows, values[:, head * lanes : (head + 1) * lanes])
     for turn in range(heads):
         outs[turn][...] = stage[place[0] ^ turn]
-    copies[4].wait()
-    copies[5].wait()
-
-
-def query_kernel(heads, scale, place, hidden, query_one, query_two, *refs):
+    for copy in later:
+        copy.wait()
+
+
+def query_kernel(heads, place, hidden, query_one, query_two, *refs):
     outs, stage = refs[:heads], refs[heads]
     first = jnp.dot(hidden[...], query_one[...], preferred_element_type=jnp.float32)
     second = jnp.dot(hidden[...], query_two[...], preferred_element_type=jnp.float32)
     for head, tile in enumerate(pair_up(first, second, heads)):
-        turned_into(stage, head, 0, tile * scale)
+        turned_into(stage, head, 0, tile)
     for turn in range(heads):
         outs[turn][...] = stage[place[0] ^ turn]
 
@@ -126,8 +141,8 @@
     return jnp.sum(weights.reshape(weights.shape[0] // 8, 8, weights.shape[1]), axis=0)
 
 
-def span_of(keys, values, at, span, two_maps, limit=None):
-    weights = jnp.exp2(scores_of(keys, at, span, two_maps))
+def span_of(scale, keys, values, at, span, two_maps, limit=None):
+    weights = jnp.exp2(scores_of(keys, at, span, two_maps) * scale)
     if limit is not None:
         weights = jnp.where(ahead_of(span, two_maps.shape[1] // 2) <= limit, weights, 0.0)
     return weighed(values, at, weights), fold(weights)
@@ -141,7 +156,7 @@
         values[:, pl.ds(column, lanes)] = given[begin : begin + lanes, :]
 
 
-def early_kernel(heads, down, across, place, *refs):
+def early_kernel(scale, heads, down, across, place, *refs):
     z, y, x = place[0], place[1], place[2]
     parts = down * across
     last = heads // 2
@@ -174,14 +189,14 @@
                     if at == case ^ last:
                         continue
                     limit = mine * rows if at == index else None
-                    more, weight = span_of(keys, values, at * span, span, two_maps, limit)
+                    more, weight = span_of(scale, keys, values, at * span, span, two_maps, limit)
                     added = added + more
                     total = total + weight
                 accum[index] = added
                 sums[index] = total
 
 
-def late_kernel(heads, down, across, place, lambdas, gain, *refs):
+def late_kernel(scale, heads, down, across, place, lambdas, gain, *refs):
     z, y, x = place[0], place[1], place[2]
     parts = down * across
     last = heads // 2
@@ -223,7 +238,9 @@
                 if index >= case ^ last:
                     two_maps = two_maps_of(queries[index])
                     limit = mine * rows if index == case ^ last else None
-                    more, weight = span_of(late_keys, late_values, 0, span, two_maps, limit)
+                    more, weight = span_of(
+                        scale, late_keys, late_values, 0, span, two_maps, limit
+                    )
                     added = added + more
                     total = total + weight
                 total = finish(index, added, total)
@@ -247,7 +264,8 @@
             def one_block(block, inner):
                 at = pl.multiple_of(block * rows, rows)
                 allowed = ahead_of(rows, rows) <= (index * parts + mine - block) * rows
-                scores = jnp.where(allowed, scores_of(all_keys, at, rows, two_maps), masked_score)
+                scores = scores_of(all_keys, at, rows, two_maps) * scale
+                scores = jnp.where(allowed, scores, masked_score)
                 highest = jnp.maximum(peak[...], jnp.max(scores, axis=0, keepdims=True))
                 rescale = jnp.exp2(peak[...] - highest)
                 weights = jnp.where(allowed, jnp.exp2(scores - highest), 0.0)
@@ -337,7 +355,7 @@
             pltpu.VMEM((model, width), bf16),
             pltpu.VMEM((model, heads * lanes), bf16),
             pltpu.VMEM((heads, block_rows, lanes), bf16),
-            pltpu.SemaphoreType.DMA((6,)),
+            pltpu.SemaphoreType.DMA((key_pieces + 1, 4)),
         ],
         compiler_params=pltpu.CompilerParams(vmem_limit_bytes=20 << 20),
         cost_estimate=cost(2 * rows * model * 4 * width, 7 << 20),
@@ -347,7 +365,7 @@
     own = [kv[0]] + [exchange(kv[turn], turn * parts) for turn in turns[1:]]
 
     queries = pl.pallas_call(
-        functools.partial(query_kernel, heads, scale),
+        functools.partial(query_kernel, heads),
         out_shape=[stripe] * heads,
         in_specs=[in_smem()] + [in_vmem()] * 3,
         out_specs=[in_vmem()] * heads,
@@ -376,7 +394,7 @@
         jax.ShapeDtypeStruct((heads, 8, 2 * rows), f32),
     ]
     state = pl.pallas_call(
-        functools.partial(early_kernel, heads, down, across),
+        functools.partial(early_kernel, scale, heads, down, across),
         out_shape=state,
         in_specs=[in_smem()] + [in_vmem()] * (heads + len(early_blocks)),
         out_specs=[in_vmem()] * 5,
@@ -385,7 +403,7 @@
         name="attend_early",
     )(place, *own_queries, *early_blocks)
     normed = pl.pallas_call(
-        functools.partial(late_kernel, heads, down, across),
+        functools.partial(late_kernel, scale, heads, down, across),
         out_shape=[stripe] * heads,
         in_specs=[in_smem()] * 2 + [in_vmem()] * (1 + parts + 5),
         out_specs=[in_vmem()] * heads,

time: 85.4 us -> 85.3 us (level)
  no operation moved by 1% of the time
where the time goes in v4:
time: 85.3 us; the launch traced here: 85.2 us
  Pallas kernels  36.7 us (43%)
  starting transfers between devices  34.3 us (40%)
  waiting for transfers between devices  13.8 us (16%)
    pallas_call x1, Pallas kernels, exchanged(): pl.pallas_call(functools.partial(late_kernel, scale, heads, down, across)...  23.4 us
    ppermute x21, starting transfers between devices, exchange(): return lax.ppermute(array, 'sp', pairs)  22 us
    ppermute x21, waiting for transfers between devices, exchange(): return lax.ppermute(array, 'sp', pairs)  12.9 us
    ppermute x4, starting transfers between devices, exchanged(): back_other = [lax.ppermute(back[turn], 'tp', swap_core) for turn in turns]  11.7 us
    pallas_call x1, Pallas kernels, exchanged(): pl.pallas_call(functools.partial(early_kernel, scale, heads, down, across...  5.18 us
    pallas_call x1, Pallas kernels, exchanged(): pl.pallas_call(functools.partial(key_value_kernel, heads), out_shape=[blo...  4.06 us
    pallas_call x1, Pallas kernels, exchanged(): pl.pallas_call(functools.partial(project_out_kernel, heads), out_shape=ja...  2.63 us
  transfers between devices with their start and end apart: 26, of which 10 were waited for; matrix products, arithmetic and copies ran while one was open for 0% of the time, Pallas kernels for 40%

profile of v4, /device:TPU:7, one launch (start us, length us, event | category | flops | bytes accessed | tf_op | source)
XLA Modules:
  0.0 85.2 jit_solution(12938815485670834283)
XLA Ops:
  0.0 0.7 collective-permute-start.25
  0.8 4.1 %project_keys.1 = (bf16[512,128]{1,0:T(8,128)(2,1)S(1)}, bf16[512,128]{1,0:T(8,128)(2,1)S(1)}, bf16[512,128]{1,0:T(8,128)(2,1)S(1)}, bf16[512,128]{1,0:T(8,128)(...) custom-call(s32[3]{0:T(128)S(1)} %pad_add_fusion.place, ...), custom_call_target="tpu_custom_call" | custom-call | flops 1073741824 | bytes 7340032 | tf_op jit(solution)/shard_map/project_keys/pallas_call | solution.py:348
  4.8 1.4 %project_queries.1 = (bf16[256,128]{1,0:T(8,128)(2,1)S(1)}, bf16[256,128]{1,0:T(8,128)(2,1)S(1)}, bf16[256,128]{1,0:T(8,128)(2,1)S(1)}, bf16[256,128]{1,0:T(8,128)(2,1)S(1)}) custom-call(s32[3]{0:T(128)S(1)} %pad_add_fusion.place, bf16[256,2048]{1,0:T(8,128)(2,1)S(1)} %get-tuple-element.26.hidden, bf16[2048,256]{1,0:T(8,128)(2,1)S(1)} %get-tuple-element.27.query_one, ...), custom_call_target="tpu_custom_call" | custom-call | flops 536870912 | bytes 4194304 | tf_op jit(solution)/shard_map/project_queries/pallas_call | solution.py:367
  6.3 1.4 %collective-permute-start.4 = (bf16[256,128]{1,0:T(8,128)(2,1)S(1)}, bf16[256,128]{1,0:T(8,128)(2,1)S(1)}, u32[]{:S(2)}, u32[]{:S(2)}) collective-permute-start(bf16[256,128]{1,0:T(8,128)(2,1)S(1)} %get-tuple-element.30), channel_id=1, source_target_pairs={{0,8},{2,10},{4,12},{6,14},{8,0},{10,2},{12,4},{14,6},{16,24},{18,... | collective-permute-start | bytes 196616 | tf_op jit(solution)/shard_map/ppermute | solution.py:339
  7.6 2.3 %collective-permute-start.5 = (bf16[256,128]{1,0:T(8,128)(2,1)S(1)}, bf16[256,128]{1,0:T(8,128)(2,1)S(1)}, u32[]{:S(2)}, u32[]{:S(2)}) collective-permute-start(bf16[256,128]{1,0:T(8,128)(2,1)S(1)} %get-tuple-element.31), channel_id=1, source_target_pairs={{0,16},{2,18},{4,20},{6,22},{8,24},{10,26},{12,28},{14,30},{16,0},... | collective-permute-start | bytes 196616 | tf_op jit(solution)/shard_map/ppermute | solution.py:339
  9.9 0.3 collective-permute-start.7
  10.3 3.0 %collective-permute-start.8 = (bf16[512,128]{1,0:T(8,128)(2,1)S(1)}, bf16[512,128]{1,0:T(8,128)(2,1)S(1)}, u32[]{:S(2)}, u32[]{:S(2)}) collective-permute-start(bf16[512,128]{1,0:T(8,128)(2,1)S(1)} %get-tuple-element.35), channel_id=1, source_target_pairs={{0,24},{2,26},{4,28},{6,30},{8,16},{10,18},{12,20},{14,22},{16,8},... | collective-permute-start | bytes 393224 | tf_op jit(solution)/shard_map/ppermute | solution.py:339
  13.5 1.4 %collective-permute-done.6.refs_3_ = bf16[256,128]{1,0:T(8,128)(2,1)S(1)} collective-permute-done((bf16[256,128]{1,0:T(8,128)(2,1)S(1)}, bf16[256,128]{1,0:T(8,128)(2,1)S(1)}, u32[]{:S(2)}, u32[]{:S(2)}) %collective-permute-start.6) | collective-permute-done | bytes 65568 | tf_op jit(solution)/shard_map/ppermute | solution.py:339
  15.4 1.0 %collective-permute-start.9 = (bf16[512,128]{1,0:T(8,128)(2,1)S(1)}, bf16[512,128]{1,0:T(8,128)(2,1)S(1)}, u32[]{:S(2)}, u32[]{:S(2)}) collective-permute-start(bf16[512,128]{1,0:T(8,128)(2,1)S(1)} %get-tuple-element.33.refs_4_), channel_id=1, source_target_pairs={{0,2},{2,0},{4,6},{6,4},{8,10},{10,8},{12,14},{14,12},{16,18},{18,... | collective-permute-start | bytes 393224 | tf_op jit(solution)/shard_map/ppermute | solution.py:339
  16.4 4.0 %collective-permute-done.8.refs_6_ = bf16[512,128]{1,0:T(8,128)(2,1)S(1)} collective-permute-done((bf16[512,128]{1,0:T(8,128)(2,1)S(1)}, bf16[512,128]{1,0:T(8,128)(2,1)S(1)}, u32[]{:S(2)}, u32[]{:S(2)}) %collective-permute-start.8) | collective-permute-done | bytes 131104 | tf_op jit(solution)/shard_map/ppermute | solution.py:339
  20.4 2.6 %collective-permute-start = (bf16[512,128]{1,0:T(8,128)(2,1)S(1)}, bf16[512,128]{1,0:T(8,128)(2,1)S(1)}, u32[]{:S(2)}, u32[]{:S(2)}) collective-permute-start(bf16[512,128]{1,0:T(8,128)(2,1)S(1)} %get-tuple-element.25), channel_id=1, source_target_pairs={{0,16},{2,18},{4,20},{6,22},{8,24},{10,26},{12,28},{14,30},{16,0},... | collective-permute-start | bytes 393224 | tf_op jit(solution)/shard_map/ppermute | solution.py:339
  23.3 1.2 %collective-permute-start.11 = (bf16[512,128]{1,0:T(8,128)(2,1)S(1)}, bf16[512,128]{1,0:T(8,128)(2,1)S(1)}, u32[]{:S(2)}, u32[]{:S(2)}) collective-permute-start(bf16[512,128]{1,0:T(8,128)(2,1)S(1)} %collective-permute-done.8.refs_6_), channel_id=1, source_target_pairs={{0,2},{2,0},{4,6},{6,4},{8,10},{10,8},{12,14},{14,12},{16,18},{18,... | collective-permute-start | bytes 393224 | tf_op jit(solution)/shard_map/ppermute | solution.py:339
  24.7 0.7 collective-permute-done.refs_0_
  25.4 0.6 collective-permute-start.14
  26.0 1.2 %collective-permute-done.10.refs_8_ = bf16[512,128]{1,0:T(8,128)(2,1)S(1)} collective-permute-done((bf16[512,128]{1,0:T(8,128)(2,1)S(1)}, bf16[512,128]{1,0:T(8,128)(2,1)S(1)}, u32[]{:S(2)}, u32[]{:S(2)}) %collective-permute-start.10) | collective-permute-done | bytes 131104 | tf_op jit(solution)/shard_map/ppermute | solution.py:339
  27.3 2.1 %collective-permute-done.11.refs_9_ = bf16[512,128]{1,0:T(8,128)(2,1)S(1)} collective-permute-done((bf16[512,128]{1,0:T(8,128)(2,1)S(1)}, bf16[512,128]{1,0:T(8,128)(2,1)S(1)}, u32[]{:S(2)}, u32[]{:S(2)}) %collective-permute-start.11) | collective-permute-done | bytes 131104 | tf_op jit(solution)/shard_map/ppermute | solution.py:339
  29.7 1.2 %collective-permute-start.1 = (bf16[512,128]{1,0:T(8,128)(2,1)S(1)}, bf16[512,128]{1,0:T(8,128)(2,1)S(1)}, u32[]{:S(2)}, u32[]{:S(2)}) collective-permute-start(bf16[512,128]{1,0:T(8,128)(2,1)S(1)} %collective-permute-done.refs_0_), channel_id=1, source_target_pairs={{0,2},{2,0},{4,6},{6,4},{8,10},{10,8},{12,14},{14,12},{16,18},{18,... | collective-permute-start | bytes 393224 | tf_op jit(solution)/shard_map/ppermute | solution.py:339
  30.9 1.2 %collective-permute-start.2 = (bf16[512,128]{1,0:T(8,128)(2,1)S(1)}, bf16[512,128]{1,0:T(8,128)(2,1)S(1)}, u32[]{:S(2)}, u32[]{:S(2)}) collective-permute-start(bf16[512,128]{1,0:T(8,128)(2,1)S(1)} %collective-permute-done.refs_0_), channel_id=1, source_target_pairs={{0,4},{2,6},{4,0},{6,2},{8,12},{10,14},{12,8},{14,10},{16,20},{18,... | collective-permute-start | bytes 393224 | tf_op jit(solution)/shard_map/ppermute | solution.py:339
  32.1 0.4 collective-permute-done.16.refs_14_
  32.5 1.0 %collective-permute-start.3 = (bf16[512,128]{1,0:T(8,128)(2,1)S(1)}, bf16[512,128]{1,0:T(8,128)(2,1)S(1)}, u32[]{:S(2)}, u32[]{:S(2)}) collective-permute-start(bf16[512,128]{1,0:T(8,128)(2,1)S(1)} %collective-permute-done.refs_0_), channel_id=1, source_target_pairs={{0,6},{2,4},{4,2},{6,0},{8,14},{10,12},{12,10},{14,8},{16,22},{18,... | collective-permute-start | bytes 393224 | tf_op jit(solution)/shard_map/ppermute | solution.py:339
  33.5 0.7 collective-permute-done.17.refs_15_
  34.2 5.2 %attend_early.1 = (bf16[4,256,128]{2,1,0:T(8,128)(2,1)S(1)}, bf16[4096,128]{1,0:T(8,128)(2,1)S(1)}, bf16[128,4096]{1,0:T(8,128)(2,1)S(1)}, f32[4,128,512]{2,1,0:T(8,128)S(1)}, f32[4,8,512]{2,1,0:T(8,128)S(1)}) custom-call(s32[3]{0:T(128)S(1)} %pad_add_fusion.place, bf16[256,128]{1,0:T(8,128)(2,1)S(1)} %get-tuple-element.29.refs_0_, ...), custom_call_target="tpu_custom_call" | custom-call | flops 1610612736 | bytes 3145728 | tf_op jit(solution)/shard_map/attend_early/pallas_call | solution.py:396
  39.4 2.1 %collective-permute-done.2.refs_2_ = bf16[512,128]{1,0:T(8,128)(2,1)S(1)} collective-permute-done((bf16[512,128]{1,0:T(8,128)(2,1)S(1)}, bf16[512,128]{1,0:T(8,128)(2,1)S(1)}, u32[]{:S(2)}, u32[]{:S(2)}) %collective-permute-start.2) | collective-permute-done | bytes 131104 | tf_op jit(solution)/shard_map/ppermute | solution.py:339
  41.5 23.4 %attend_late.1 = (bf16[256,128]{1,0:T(8,128)(2,1)S(1)}, bf16[256,128]{1,0:T(8,128)(2,1)S(1)}, bf16[256,128]{1,0:T(8,128)(2,1)S(1)}, bf16[256,128]{1,0:T(8,128)(2,1)S(1)}) custom-call(s32[3]{0:T(128)S(1)} %pad_add_fusion.place, f32[4]{0:T(128)S(1)} %copy-done.1, f32[1,128]{1,0:T(1,128)S(1)} %bitcast.4, bf16[512,128]{1,0:T(8,128)(2,1)S(1)} %collective-permute-done.refs_0_, ...), custom_call_target="tpu_custom_call" | custom-call | flops 536870912 | bytes 3145728 | tf_op jit(solution)/shard_map/attend_late/pallas_call | solution.py:405
  64.9 2.7 %collective-permute-start.18 = (bf16[256,128]{1,0:T(8,128)(2,1)S(1)}, bf16[256,128]{1,0:T(8,128)(2,1)S(1)}, u32[]{:S(2)}, u32[]{:S(2)}) collective-permute-start(bf16[256,128]{1,0:T(8,128)(2,1)S(1)} %get-tuple-element.42), channel_id=1, source_target_pairs={{0,8},{2,10},{4,12},{6,14},{8,0},{10,2},{12,4},{14,6},{16,24},{18,... | collective-permute-start | bytes 196616 | tf_op jit(solution)/shard_map/ppermute | solution.py:339
  67.6 0.8 collective-permute-start.19
  68.4 1.3 %collective-permute-start.20 = (bf16[256,128]{1,0:T(8,128)(2,1)S(1)}, bf16[256,128]{1,0:T(8,128)(2,1)S(1)}, u32[]{:S(2)}, u32[]{:S(2)}) collective-permute-start(bf16[256,128]{1,0:T(8,128)(2,1)S(1)} %get-tuple-element.44), channel_id=1, source_target_pairs={{0,24},{2,26},{4,28},{6,30},{8,16},{10,18},{12,20},{14,22},{16,8},... | collective-permute-start | bytes 196616 | tf_op jit(solution)/shard_map/ppermute | solution.py:339
  69.8 7.2 %collective-permute-start.21 = (bf16[256,128]{1,0:T(8,128)(2,1)S(1)}, bf16[256,128]{1,0:T(8,128)(2,1)S(1)}, u32[]{:S(2)}, u32[]{:S(2)}) collective-permute-start(bf16[256,128]{1,0:T(8,128)(2,1)S(1)} %get-tuple-element.41.refs_0_), channel_id=1, source_target_pairs={{0,1},{1,0},{2,3},{3,2},{4,5},{5,4},{6,7},{7,6},{8,9},{9,8},{10,11... | collective-permute-start | bytes 196616 | tf_op jit(solution)/shard_map/ppermute | solution.py:435
  77.0 0.8 collective-permute-start.23
  77.9 3.6 %collective-permute-start.24 = (bf16[256,128]{1,0:T(8,128)(2,1)S(1)}, bf16[256,128]{1,0:T(8,128)(2,1)S(1)}, u32[]{:S(2)}, u32[]{:S(2)}) collective-permute-start(bf16[256,128]{1,0:T(8,128)(2,1)S(1)} %collective-permute-done.20.refs_3_), channel_id=1, source_target_pairs={{0,1},{1,0},{2,3},{3,2},{4,5},{5,4},{6,7},{7,6},{8,9},{9,8},{10,11... | collective-permute-start | bytes 196616 | tf_op jit(solution)/shard_map/ppermute | solution.py:435
  81.5 0.9 %collective-permute-done.24.refs_7_ = bf16[256,128]{1,0:T(8,128)(2,1)S(1)} collective-permute-done((bf16[256,128]{1,0:T(8,128)(2,1)S(1)}, bf16[256,128]{1,0:T(8,128)(2,1)S(1)}, u32[]{:S(2)}, u32[]{:S(2)}) %collective-permute-start.24) | collective-permute-done | bytes 65568 | tf_op jit(solution)/shard_map/ppermute | solution.py:435
  82.4 2.6 %project_out.1 = bf16[256,2048]{1,0:T(8,128)(2,1)} custom-call(s32[3]{0:T(128)S(1)} %pad_add_fusion.place, bf16[256,128]{1,0:T(8,128)(2,1)S(1)} %get-tuple-element.41.refs_0_, bf16[256,128]{1,0:T(8,128)(2,1)S(1)} %collective-permute-done.18.refs_1_, bf16[256,128]{1,0:T(8,128)(2,1)S(1)} %collective-permute-done.19.refs_2_, ...), custom_call_target="tpu_custom_call" | custom-call | flops 1073741824 | bytes 6291456 | tf_op jit(solution)/shard_map/project_out/pallas_call | solution.py:436
  (32 shorter events, 1.7 us)
Async XLA Ops:
  0.0 82.4 %collective-permute-start.25 = (bf16[512,2048]{1,0:T(8,128)(2,1)}, bf16[512,2048]{1,0:T(8,128)(2,1)S(1)}, u32[]{:S(2)}, u32[]{:S(2)}) collective-permute-start(bf16[512,2048]{1,0:T(8,128)(2,1)} %refs_8_.1), channel_id=1, source_target_pairs={{0,1},{1,0},{2,3},{3,2},{4,5},{5,4},{6,7},{7,6},{8,9},{9,8},{10,11... | collective-permute-start | bytes 6291464 | tf_op jit(solution)/shard_map/ppermute | solution.py:381
  6.3 4.0 %collective-permute-start.4 = (bf16[256,128]{1,0:T(8,128)(2,1)S(1)}, bf16[256,128]{1,0:T(8,128)(2,1)S(1)}, u32[]{:S(2)}, u32[]{:S(2)}) collective-permute-start(bf16[256,128]{1,0:T(8,128)(2,1)S(1)} %get-tuple-element.30), channel_id=1, source_target_pairs={{0,8},{2,10},{4,12},{6,14},{8,0},{10,2},{12,4},{14,6},{16,24},{18,... | collective-permute-start | bytes 196616 | tf_op jit(solution)/shard_map/ppermute | solution.py:339
  7.6 5.7 %collective-permute-start.5 = (bf16[256,128]{1,0:T(8,128)(2,1)S(1)}, bf16[256,128]{1,0:T(8,128)(2,1)S(1)}, u32[]{:S(2)}, u32[]{:S(2)}) collective-permute-start(bf16[256,128]{1,0:T(8,128)(2,1)S(1)} %get-tuple-element.31), channel_id=1, source_target_pairs={{0,16},{2,18},{4,20},{6,22},{8,24},{10,26},{12,28},{14,30},{16,0},... | collective-permute-start | bytes 196616 | tf_op jit(solution)/shard_map/ppermute | solution.py:339
  9.9 5.0 %collective-permute-start.6 = (bf16[256,128]{1,0:T(8,128)(2,1)S(1)}, bf16[256,128]{1,0:T(8,128)(2,1)S(1)}, u32[]{:S(2)}, u32[]{:S(2)}) collective-permute-start(bf16[256,128]{1,0:T(8,128)(2,1)S(1)} %get-tuple-element.32), channel_id=1, source_target_pairs={{0,24},{2,26},{4,28},{6,30},{8,16},{10,18},{12,20},{14,22},{16,8},... | collective-permute-start | bytes 196616 | tf_op jit(solution)/shard_map/ppermute | solution.py:339
  9.9 5.5 %collective-permute-start.7 = (bf16[512,128]{1,0:T(8,128)(2,1)S(1)}, bf16[512,128]{1,0:T(8,128)(2,1)S(1)}, u32[]{:S(2)}, u32[]{:S(2)}) collective-permute-start(bf16[512,128]{1,0:T(8,128)(2,1)S(1)} %get-tuple-element.34), channel_id=1, source_target_pairs={{0,8},{2,10},{4,12},{6,14},{8,0},{10,2},{12,4},{14,6},{16,24},{18,... | collective-permute-start | bytes 393224 | tf_op jit(solution)/shard_map/ppermute | solution.py:339
  10.3 10.2 %collective-permute-start.8 = (bf16[512,128]{1,0:T(8,128)(2,1)S(1)}, bf16[512,128]{1,0:T(8,128)(2,1)S(1)}, u32[]{:S(2)}, u32[]{:S(2)}) collective-permute-start(bf16[512,128]{1,0:T(8,128)(2,1)S(1)} %get-tuple-element.35), channel_id=1, source_target_pairs={{0,24},{2,26},{4,28},{6,30},{8,16},{10,18},{12,20},{14,22},{16,8},... | collective-permute-start | bytes 393224 | tf_op jit(solution)/shard_map/ppermute | solution.py:339
  13.3 9.7 %collective-permute-start.12 = (bf16[512,128]{1,0:T(8,128)(2,1)S(1)}, bf16[512,128]{1,0:T(8,128)(2,1)S(1)}, u32[]{:S(2)}, u32[]{:S(2)}) collective-permute-start(bf16[512,128]{1,0:T(8,128)(2,1)S(1)} %get-tuple-element.33.refs_4_), channel_id=1, source_target_pairs={{0,4},{2,6},{4,0},{6,2},{8,12},{10,14},{12,8},{14,10},{16,20},{18,... | collective-permute-start | bytes 393224 | tf_op jit(solution)/shard_map/ppermute | solution.py:339
  15.0 8.3 %collective-permute-start.15 = (bf16[512,128]{1,0:T(8,128)(2,1)S(1)}, bf16[512,128]{1,0:T(8,128)(2,1)S(1)}, u32[]{:S(2)}, u32[]{:S(2)}) collective-permute-start(bf16[512,128]{1,0:T(8,128)(2,1)S(1)} %get-tuple-element.33.refs_4_), channel_id=1, source_target_pairs={{0,6},{2,4},{4,2},{6,0},{8,14},{10,12},{12,10},{14,8},{16,22},{18,... | collective-permute-start | bytes 393224 | tf_op jit(solution)/shard_map/ppermute | solution.py:339
  15.4 9.1 %collective-permute-start.9 = (bf16[512,128]{1,0:T(8,128)(2,1)S(1)}, bf16[512,128]{1,0:T(8,128)(2,1)S(1)}, u32[]{:S(2)}, u32[]{:S(2)}) collective-permute-start(bf16[512,128]{1,0:T(8,128)(2,1)S(1)} %get-tuple-element.33.refs_4_), channel_id=1, source_target_pairs={{0,2},{2,0},{4,6},{6,4},{8,10},{10,8},{12,14},{14,12},{16,18},{18,... | collective-permute-start | bytes 393224 | tf_op jit(solution)/shard_map/ppermute | solution.py:339
  20.4 4.9 %collective-permute-start = (bf16[512,128]{1,0:T(8,128)(2,1)S(1)}, bf16[512,128]{1,0:T(8,128)(2,1)S(1)}, u32[]{:S(2)}, u32[]{:S(2)}) collective-permute-start(bf16[512,128]{1,0:T(8,128)(2,1)S(1)} %get-tuple-element.25), channel_id=1, source_target_pairs={{0,16},{2,18},{4,20},{6,22},{8,24},{10,26},{12,28},{14,30},{16,0},... | collective-permute-start | bytes 393224 | tf_op jit(solution)/shard_map/ppermute | solution.py:339
  23.0 4.1 %collective-permute-start.10 = (bf16[512,128]{1,0:T(8,128)(2,1)S(1)}, bf16[512,128]{1,0:T(8,128)(2,1)S(1)}, u32[]{:S(2)}, u32[]{:S(2)}) collective-permute-start(bf16[512,128]{1,0:T(8,128)(2,1)S(1)} %collective-permute-done.7.refs_5_), channel_id=1, source_target_pairs={{0,2},{2,0},{4,6},{6,4},{8,10},{10,8},{12,14},{14,12},{16,18},{18,... | collective-permute-start | bytes 393224 | tf_op jit(solution)/shard_map/ppermute | solution.py:339
  23.3 6.2 %collective-permute-start.11 = (bf16[512,128]{1,0:T(8,128)(2,1)S(1)}, bf16[512,128]{1,0:T(8,128)(2,1)S(1)}, u32[]{:S(2)}, u32[]{:S(2)}) collective-permute-start(bf16[512,128]{1,0:T(8,128)(2,1)S(1)} %collective-permute-done.8.refs_6_), channel_id=1, source_target_pairs={{0,2},{2,0},{4,6},{6,4},{8,10},{10,8},{12,14},{14,12},{16,18},{18,... | collective-permute-start | bytes 393224 | tf_op jit(solution)/shard_map/ppermute | solution.py:339
  24.5 5.2 %collective-permute-start.13 = (bf16[512,128]{1,0:T(8,128)(2,1)S(1)}, bf16[512,128]{1,0:T(8,128)(2,1)S(1)}, u32[]{:S(2)}, u32[]{:S(2)}) collective-permute-start(bf16[512,128]{1,0:T(8,128)(2,1)S(1)} %collective-permute-done.7.refs_5_), channel_id=1, source_target_pairs={{0,4},{2,6},{4,0},{6,2},{8,12},{10,14},{12,8},{14,10},{16,20},{18,... | collective-permute-start | bytes 393224 | tf_op jit(solution)/shard_map/ppermute | solution.py:339
  25.4 5.5 %collective-permute-start.14 = (bf16[512,128]{1,0:T(8,128)(2,1)S(1)}, bf16[512,128]{1,0:T(8,128)(2,1)S(1)}, u32[]{:S(2)}, u32[]{:S(2)}) collective-permute-start(bf16[512,128]{1,0:T(8,128)(2,1)S(1)} %collective-permute-done.8.refs_6_), channel_id=1, source_target_pairs={{0,4},{2,6},{4,0},{6,2},{8,12},{10,14},{12,8},{14,10},{16,20},{18,... | collective-permute-start | bytes 393224 | tf_op jit(solution)/shard_map/ppermute | solution.py:339
  27.1 5.4 %collective-permute-start.16 = (bf16[512,128]{1,0:T(8,128)(2,1)S(1)}, bf16[512,128]{1,0:T(8,128)(2,1)S(1)}, u32[]{:S(2)}, u32[]{:S(2)}) collective-permute-start(bf16[512,128]{1,0:T(8,128)(2,1)S(1)} %collective-permute-done.7.refs_5_), channel_id=1, source_target_pairs={{0,6},{2,4},{4,2},{6,0},{8,14},{10,12},{12,10},{14,8},{16,22},{18,... | collective-permute-start | bytes 393224 | tf_op jit(solution)/shard_map/ppermute | solution.py:339
  29.5 4.7 %collective-permute-start.17 = (bf16[512,128]{1,0:T(8,128)(2,1)S(1)}, bf16[512,128]{1,0:T(8,128)(2,1)S(1)}, u32[]{:S(2)}, u32[]{:S(2)}) collective-permute-start(bf16[512,128]{1,0:T(8,128)(2,1)S(1)} %collective-permute-done.8.refs_6_), channel_id=1, source_target_pairs={{0,6},{2,4},{4,2},{6,0},{8,14},{10,12},{12,10},{14,8},{16,22},{18,... | collective-permute-start | bytes 393224 | tf_op jit(solution)/shard_map/ppermute | solution.py:339
  29.7 9.7 %collective-permute-start.1 = (bf16[512,128]{1,0:T(8,128)(2,1)S(1)}, bf16[512,128]{1,0:T(8,128)(2,1)S(1)}, u32[]{:S(2)}, u32[]{:S(2)}) collective-permute-start(bf16[512,128]{1,0:T(8,128)(2,1)S(1)} %collective-permute-done.refs_0_), channel_id=1, source_target_pairs={{0,2},{2,0},{4,6},{6,4},{8,10},{10,8},{12,14},{14,12},{16,18},{18,... | collective-permute-start | bytes 393224 | tf_op jit(solution)/shard_map/ppermute | solution.py:339
  30.9 10.6 %collective-permute-start.2 = (bf16[512,128]{1,0:T(8,128)(2,1)S(1)}, bf16[512,128]{1,0:T(8,128)(2,1)S(1)}, u32[]{:S(2)}, u32[]{:S(2)}) collective-permute-start(bf16[512,128]{1,0:T(8,128)(2,1)S(1)} %collective-permute-done.refs_0_), channel_id=1, source_target_pairs={{0,4},{2,6},{4,0},{6,2},{8,12},{10,14},{12,8},{14,10},{16,20},{18,... | collective-permute-start | bytes 393224 | tf_op jit(solution)/shard_map/ppermute | solution.py:339
  32.5 9.0 %collective-permute-start.3 = (bf16[512,128]{1,0:T(8,128)(2,1)S(1)}, bf16[512,128]{1,0:T(8,128)(2,1)S(1)}, u32[]{:S(2)}, u32[]{:S(2)}) collective-permute-start(bf16[512,128]{1,0:T(8,128)(2,1)S(1)} %collective-permute-done.refs_0_), channel_id=1, source_target_pairs={{0,6},{2,4},{4,2},{6,0},{8,14},{10,12},{12,10},{14,8},{16,22},{18,... | collective-permute-start | bytes 393224 | tf_op jit(solution)/shard_map/ppermute | solution.py:339
  34.2 7.3 %copy-start.1 = (f32[4]{0:T(128)S(1)}, f32[4]{0:T(128)}, u32[]{:S(2)}) copy-start(f32[4]{0:T(128)} %lambdas.1) | copy-start | bytes 52
  34.2 7.3 %copy-start.2 = (f32[128]{0:T(128)S(1)}, f32[128]{0:T(128)}, u32[]{:S(2)}) copy-start(f32[128]{0:T(128)} %param.16) | copy-start | bytes 1540
  39.4 43.0 %copy-start = (bf16[512,2048]{1,0:T(8,128)(2,1)S(1)}, bf16[512,2048]{1,0:T(8,128)(2,1)}, u32[]{:S(2)}) copy-start(bf16[512,2048]{1,0:T(8,128)(2,1)} %refs_8_.1) | copy-start | bytes 6291460
  64.9 12.1 %collective-permute-start.18 = (bf16[256,128]{1,0:T(8,128)(2,1)S(1)}, bf16[256,128]{1,0:T(8,128)(2,1)S(1)}, u32[]{:S(2)}, u32[]{:S(2)}) collective-permute-start(bf16[256,128]{1,0:T(8,128)(2,1)S(1)} %get-tuple-element.42), channel_id=1, source_target_pairs={{0,8},{2,10},{4,12},{6,14},{8,0},{10,2},{12,4},{14,6},{16,24},{18,... | collective-permute-start | bytes 196616 | tf_op jit(solution)/shard_map/ppermute | solution.py:339
  67.6 9.4 %collective-permute-start.19 = (bf16[256,128]{1,0:T(8,128)(2,1)S(1)}, bf16[256,128]{1,0:T(8,128)(2,1)S(1)}, u32[]{:S(2)}, u32[]{:S(2)}) collective-permute-start(bf16[256,128]{1,0:T(8,128)(2,1)S(1)} %get-tuple-element.43), channel_id=1, source_target_pairs={{0,16},{2,18},{4,20},{6,22},{8,24},{10,26},{12,28},{14,30},{16,0},... | collective-permute-start | bytes 196616 | tf_op jit(solution)/shard_map/ppermute | solution.py:339
  68.4 9.4 %collective-permute-start.20 = (bf16[256,128]{1,0:T(8,128)(2,1)S(1)}, bf16[256,128]{1,0:T(8,128)(2,1)S(1)}, u32[]{:S(2)}, u32[]{:S(2)}) collective-permute-start(bf16[256,128]{1,0:T(8,128)(2,1)S(1)} %get-tuple-element.44), channel_id=1, source_target_pairs={{0,24},{2,26},{4,28},{6,30},{8,16},{10,18},{12,20},{14,22},{16,8},... | collective-permute-start | bytes 196616 | tf_op jit(solution)/shard_map/ppermute | solution.py:339
  69.8 11.7 %collective-permute-start.21 = (bf16[256,128]{1,0:T(8,128)(2,1)S(1)}, bf16[256,128]{1,0:T(8,128)(2,1)S(1)}, u32[]{:S(2)}, u32[]{:S(2)}) collective-permute-start(bf16[256,128]{1,0:T(8,128)(2,1)S(1)} %get-tuple-element.41.refs_0_), channel_id=1, source_target_pairs={{0,1},{1,0},{2,3},{3,2},{4,5},{5,4},{6,7},{7,6},{8,9},{9,8},{10,11... | collective-permute-start | bytes 196616 | tf_op jit(solution)/shard_map/ppermute | solution.py:435
  77.0 4.5 %collective-permute-start.22 = (bf16[256,128]{1,0:T(8,128)(2,1)S(1)}, bf16[256,128]{1,0:T(8,128)(2,1)S(1)}, u32[]{:S(2)}, u32[]{:S(2)}) collective-permute-start(bf16[256,128]{1,0:T(8,128)(2,1)S(1)} %collective-permute-done.18.refs_1_), channel_id=1, source_target_pairs={{0,1},{1,0},{2,3},{3,2},{4,5},{5,4},{6,7},{7,6},{8,9},{9,8},{10,11... | collective-permute-start | bytes 196616 | tf_op jit(solution)/shard_map/ppermute | solution.py:435
  77.0 4.5 %collective-permute-start.23 = (bf16[256,128]{1,0:T(8,128)(2,1)S(1)}, bf16[256,128]{1,0:T(8,128)(2,1)S(1)}, u32[]{:S(2)}, u32[]{:S(2)}) collective-permute-start(bf16[256,128]{1,0:T(8,128)(2,1)S(1)} %collective-permute-done.19.refs_2_), channel_id=1, source_target_pairs={{0,1},{1,0},{2,3},{3,2},{4,5},{5,4},{6,7},{7,6},{8,9},{9,8},{10,11... | collective-permute-start | bytes 196616 | tf_op jit(solution)/shard_map/ppermute | solution.py:435
  77.9 4.5 %collective-permute-start.24 = (bf16[256,128]{1,0:T(8,128)(2,1)S(1)}, bf16[256,128]{1,0:T(8,128)(2,1)S(1)}, u32[]{:S(2)}, u32[]{:S(2)}) collective-permute-start(bf16[256,128]{1,0:T(8,128)(2,1)S(1)} %collective-permute-done.20.refs_3_), channel_id=1, source_target_pairs={{0,1},{1,0},{2,3},{3,2},{4,5},{5,4},{6,7},{7,6},{8,9},{9,8},{10,11... | collective-permute-start | bytes 196616 | tf_op jit(solution)/shard_map/ppermute | solution.py:435

commit v5 on v4

--- a/solution.py
+++ b/solution.py
@@ -16,7 +16,8 @@
 most_sum = 2.0**100
 lanes = 128
 key_pieces = 4
-start_queries = 0
+riding = None
+apart = (0, 1, 2, 3)
 
 
 def cost(flops, moved):
@@ -46,13 +47,6 @@
     return tiles
 
 
-def fetch_later(arrays, buffers, sems, row):
-    return [
-        pltpu.make_async_copy(array, buffer, sems.at[row, number])
-        for number, (array, buffer) in enumerate(zip(arrays, buffers))
-    ]
-
-
 def turned_into(stage, head, at, tile):
     turned = tile.T.astype(jnp.bfloat16)
     for part in range(tile.shape[0] // lanes):
@@ -60,53 +54,43 @@
         stage[head, begin : begin + lanes, :] = turned[:, part * lanes : (part + 1) * lanes]
 
 
-def key_value_kernel(heads, place, *refs):
+def project_kernel(heads, place, *refs):
     arrays, outs = refs[:6], refs[6 : 6 + heads]
-    hidden, query_one, query_two = refs[6 + heads : 9 + heads]
-    key_one, key_two, value_proj, stage, sems = refs[9 + heads :]
-    rows, model = hidden.shape
-    pieces = sems.shape[0] - 1
+    query_outs, refs = refs[6 + heads : 6 + heads + len(apart)], refs[6 + heads + len(apart) :]
+    buffers, stage, query_stage, sems = refs[:6], refs[6], refs[7], refs[8]
+    rows, model = buffers[0].shape
+    pieces = sems.shape[0]
     deep = model // pieces
     copies = []
     for piece in range(pieces):
         cut = slice(piece * deep, (piece + 1) * deep)
-        pairs = [(arrays[0].at[:, cut], hidden.at[:, cut])]
-        for array, buffer in zip(arrays[1:4], (key_one, key_two, value_proj)):
-            pairs.append((array.at[cut, :], buffer.at[cut, :]))
-        for number, (source, target) in enumerate(pairs):
+        for number, (array, buffer) in enumerate(zip(arrays, buffers)):
+            source = array.at[cut, :] if number else array.at[:, cut]
+            target = buffer.at[cut, :] if number else buffer.at[:, cut]
             copies.append(pltpu.make_async_copy(source, target, sems.at[piece, number]))
             copies[-1].start()
-    later = fetch_later(arrays[4:], (query_one, query_two), sems, pieces)
-    sums = [0.0, 0.0, 0.0]
+    sums = [0.0] * 5
     for piece in range(pieces):
-        for copy in copies[4 * piece : 4 * piece + 4]:
+        for copy in copies[6 * piece : 6 * piece + 6]:
             copy.wait()
-        if piece == start_queries:
-            for copy in later:
-                copy.start()
         cut = slice(piece * deep, (piece + 1) * deep)
-        tokens = hidden[:, cut]
-        for number, buffer in enumerate((key_one, key_two, value_proj)):
+        tokens = buffers[0][:, cut]
+        for number, buffer in enumerate(buffers[1:]):
             sums[number] += jnp.dot(tokens, buffer[cut, :], preferred_element_type=jnp.float32)
-    first, second, values = sums
-    for head, tile in enumerate(pair_up(first, second, heads)):
+    for head, tile in enumerate(pair_up(sums[0], sums[1], heads)):
         stage[head, :rows, :] = tile.astype(jnp.bfloat16)
     for head in range(heads):
-        turned_into(stage, head, rows, values[:, head * lanes : (head + 1) * lanes])
+        turned_into(stage, head, rows, sums[2][:, head * lanes : (head + 1) * lanes])
+    for head, tile in enumerate(pair_up(sums[3], sums[4], heads)):
+        turned_into(query_stage, head, 0, tile)
+    taken = stage.shape[1]
     for turn in range(heads):
-        outs[turn][...] = stage[place[0] ^ turn]
-    for copy in later:
-        copy.wait()
-
-
-def query_kernel(heads, place, hidden, query_one, query_two, *refs):
-    outs, stage = refs[:heads], refs[heads]
-    first = jnp.dot(hidden[...], query_one[...], preferred_element_type=jnp.float32)
-    second = jnp.dot(hidden[...], query_two[...], preferred_element_type=jnp.float32)
-    for head, tile in enumerate(pair_up(first, second, heads)):
-        turned_into(stage, head, 0, tile)
-    for turn in range(heads):
-        outs[turn][...] = stage[place[0] ^ turn]
+        if turn == riding:
+            outs[turn][:taken, :] = stage[place[0] ^ turn]
+            outs[turn][taken:, :] = query_stage[place[0] ^ turn]
+        else:
+            outs[turn][...] = stage[place[0] ^ turn]
+            query_outs[apart.index(turn)][...] = query_stage[place[0] ^ turn]
 
 
 def two_maps_of(turned):
@@ -161,14 +145,17 @@
     parts = down * across
     last = heads // 2
     early = [turn for turn in range(heads) if turn != last]
-    query_in, refs = refs[:heads], refs[heads:]
+    query_in, refs = refs[: len(apart)], refs[len(apart) :]
     block_in, refs = refs[: len(early) * parts], refs[len(early) * parts :]
     queries, keys, values, accum, sums = refs
     rows = queries.shape[1]
     span = parts * rows
 
     for turn in range(heads):
-        queries[z ^ turn] = query_in[turn][...]
+        if turn == riding:
+            queries[z ^ turn] = block_in[early.index(turn)][2 * rows :, :]
+        else:
+            queries[z ^ turn] = query_in[apart.index(turn)][...]
     for below in range(down):
         for aside in range(across):
             for number, turn in enumerate(early):
@@ -289,17 +276,18 @@
     out_mine, out_other, result, joined, staged, sems = refs[2 * heads :]
     z = place[0]
     for turn in range(heads):
-        at = pl.multiple_of((z ^ turn) * lanes, lanes)
-        joined[0, :, pl.ds(at, lanes)] = mine[turn][...]
-        joined[1, :, pl.ds(at, lanes)] = other[turn][...]
+        joined[0, z ^ turn] = mine[turn][...]
+        joined[1, z ^ turn] = other[turn][...]
+    first = jnp.concatenate([joined[0, head] for head in range(heads)], axis=1)
+    second = jnp.concatenate([joined[1, head] for head in range(heads)], axis=1)
     copies = []
     pieces = sems.shape[0]
     wide = result.shape[1] // pieces
     for piece in range(pieces):
         columns = slice(piece * wide, (piece + 1) * wide)
-        total = jnp.dot(joined[0], out_mine[:, columns], preferred_element_type=jnp.float32)
+        total = jnp.dot(first, out_mine[:, columns], preferred_element_type=jnp.float32)
         total = total + jnp.dot(
-            joined[1], out_other[:, columns], preferred_element_type=jnp.float32
+            second, out_other[:, columns], preferred_element_type=jnp.float32
         )
         staged[:, columns] = total.astype(jnp.bfloat16)
         copies.append(
@@ -344,45 +332,39 @@
     block_rows = 2 * rows
     block = jax.ShapeDtypeStruct((block_rows, lanes), bf16)
     stripe = jax.ShapeDtypeStruct((rows, lanes), bf16)
-    fetched = (hidden_in, query_one, query_two)
+    merged = jax.ShapeDtypeStruct((block_rows + rows, lanes), bf16)
     made = pl.pallas_call(
-        functools.partial(key_value_kernel, heads),
-        out_shape=[block] * heads + [jax.ShapeDtypeStruct(a.shape, bf16) for a in fetched],
+        functools.partial(project_kernel, heads),
+        out_shape=[merged if turn == riding else block for turn in turns] + [stripe] * len(apart),
         in_specs=[in_smem()] + [in_hbm()] * 6,
-        out_specs=[in_vmem()] * (heads + 3),
+        out_specs=[in_vmem()] * (heads + len(apart)),
         scratch_shapes=[
+            pltpu.VMEM((rows, model), bf16),
             pltpu.VMEM((model, width), bf16),
             pltpu.VMEM((model, width), bf16),
             pltpu.VMEM((model, heads * lanes), bf16),
+            pltpu.VMEM((model, width), bf16),
+            pltpu.VMEM((model, width), bf16),
             pltpu.VMEM((heads, block_rows, lanes), bf16),
-            pltpu.SemaphoreType.DMA((key_pieces + 1, 4)),
+            pltpu.VMEM((heads, rows, lanes), bf16),
+            pltpu.SemaphoreType.DMA((key_pieces, 6)),
         ],
         compiler_params=pltpu.CompilerParams(vmem_limit_bytes=20 << 20),
-        cost_estimate=cost(2 * rows * model * 4 * width, 7 << 20),
-        name="project_keys",
+        cost_estimate=cost(2 * rows * model * 6 * width, 7 << 20),
+        name="project",
     )(place, *from_hbm(hidden_in, key_one, key_two, value_proj, query_one, query_two))
-    kv, held = made[:heads], made[heads:]
-    own = [kv[0]] + [exchange(kv[turn], turn * parts) for turn in turns[1:]]
-
-    queries = pl.pallas_call(
-        functools.partial(query_kernel, heads),
-        out_shape=[stripe] * heads,
-        in_specs=[in_smem()] + [in_vmem()] * 3,
-        out_specs=[in_vmem()] * heads,
-        scratch_shapes=[pltpu.VMEM((heads, rows, lanes), bf16)],
-        compiler_params=pltpu.CompilerParams(vmem_limit_bytes=16 << 20),
-        cost_estimate=cost(2 * rows * model * 2 * width, 4 << 20),
-        name="project_queries",
-    )(place, *held)
+    kv, queries = made[:heads], made[heads:]
+    sent = [kv[0]] + [exchange(kv[turn], turn * parts) for turn in turns[1:]]
+    own = [array[:block_rows] if turn == riding else array for turn, array in enumerate(sent)]
     own_queries = [queries[0]]
-    for turn in turns[1:]:
-        own_queries.append(exchange(queries[turn], turn * parts))
+    for turn, array in zip(apart[1:], queries[1:]):
+        own_queries.append(exchange(array, turn * parts))
 
     out_other = lax.ppermute(out_proj, "tp", swap_core)
     aside = [exchange(own[turn], 1) for turn in turns]
     below = [exchange(own[turn], across) for turn in turns]
     corner = [exchange(own[turn], 1 + across) for turn in turns]
-    sides = (own, aside, below, corner)
+    sides = (sent, aside, below, corner)
     last = heads // 2
     tokens = heads * rows
     early_blocks = [side[turn] for side in sides for turn in turns if turn != last]
@@ -396,7 +378,7 @@
     state = pl.pallas_call(
         functools.partial(early_kernel, scale, heads, down, across),
         out_shape=state,
-        in_specs=[in_smem()] + [in_vmem()] * (heads + len(early_blocks)),
+        in_specs=[in_smem()] + [in_vmem()] * (len(apart) + len(early_blocks)),
         out_specs=[in_vmem()] * 5,
         compiler_params=pltpu.CompilerParams(vmem_limit_bytes=28 << 20),
         cost_estimate=cost(3 * tokens * tokens * parts * lanes, 3 << 20),
@@ -439,7 +421,7 @@
         in_specs=[in_smem()] + [in_vmem()] * (2 * heads + 2),
         out_specs=in_hbm(),
         scratch_shapes=[
-            pltpu.VMEM((groups, rows, heads * lanes), bf16),
+            pltpu.VMEM((groups, heads, rows, lanes), bf16),
             pltpu.VMEM((rows, model), bf16),
             pltpu.SemaphoreType.DMA((4,)),
         ],

time: 85.3 us -> 84.6 us (level)
    pallas_call x2 -> x1, Pallas kernels: 5.5 us -> 4.85 us  [exchanged(): pl.pallas_call(functools.partial(project_kernel, heads), out_shape=[merge...]
where the time goes in v5:
time: 84.6 us; the launch traced here: 84.5 us
  Pallas kernels  36 us (43%)
  starting transfers between devices  34.3 us (41%)
  waiting for transfers between devices  13.8 us (16%)
    pallas_call x1, Pallas kernels, exchanged(): pl.pallas_call(functools.partial(late_kernel, scale, heads, down, across)...  23.4 us
    ppermute x21, starting transfers between devices, exchange(): return lax.ppermute(array, 'sp', pairs)  22 us
    ppermute x21, waiting for transfers between devices, exchange(): return lax.ppermute(array, 'sp', pairs)  12.9 us
    ppermute x4, starting transfers between devices, exchanged(): back_other = [lax.ppermute(back[turn], 'tp', swap_core) for turn in turns]  11.7 us
    pallas_call x1, Pallas kernels, exchanged(): pl.pallas_call(functools.partial(early_kernel, scale, heads, down, across...  5.18 us
    pallas_call x1, Pallas kernels, exchanged(): pl.pallas_call(functools.partial(project_kernel, heads), out_shape=[merge...  4.85 us
    pallas_call x1, Pallas kernels, exchanged(): pl.pallas_call(functools.partial(project_out_kernel, heads), out_shape=ja...  2.59 us
  transfers between devices with their start and end apart: 26, of which 10 were waited for; matrix products, arithmetic and copies ran while one was open for 0% of the time, Pallas kernels for 40%

profile of v5, /device:TPU:7, one launch (start us, length us, event | category | flops | bytes accessed | tf_op | source)
XLA Modules:
  0.0 84.5 jit_solution(9235311776458604241)
XLA Ops:
  0.0 0.7 collective-permute-start.25
  0.8 4.9 %project.1 = (bf16[512,128]{1,0:T(8,128)(2,1)S(1)}, bf16[512,128]{1,0:T(8,128)(2,1)S(1)}, bf16[512,128]{1,0:T(8,128)(2,1)S(1)}, bf16[512,128]{1,0:T(8,128)(2,1)S...) custom-call(s32[3]{0:T(128)S(1)} %pad_add_fusion.place, ...), custom_call_target="tpu_custom_call" | custom-call | flops 1610612736 | bytes 7340032 | tf_op jit(solution)/shard_map/project/pallas_call | solution.py:336
  5.6 1.4 %collective-permute-start.4 = (bf16[256,128]{1,0:T(8,128)(2,1)S(1)}, bf16[256,128]{1,0:T(8,128)(2,1)S(1)}, u32[]{:S(2)}, u32[]{:S(2)}) collective-permute-start(bf16[256,128]{1,0:T(8,128)(2,1)S(1)} %get-tuple-element.24), channel_id=1, source_target_pairs={{0,8},{2,10},{4,12},{6,14},{8,0},{10,2},{12,4},{14,6},{16,24},{18,... | collective-permute-start | bytes 196616 | tf_op jit(solution)/shard_map/ppermute | solution.py:327
  7.0 2.3 %collective-permute-start.5 = (bf16[256,128]{1,0:T(8,128)(2,1)S(1)}, bf16[256,128]{1,0:T(8,128)(2,1)S(1)}, u32[]{:S(2)}, u32[]{:S(2)}) collective-permute-start(bf16[256,128]{1,0:T(8,128)(2,1)S(1)} %get-tuple-element.25), channel_id=1, source_target_pairs={{0,16},{2,18},{4,20},{6,22},{8,24},{10,26},{12,28},{14,30},{16,0},... | collective-permute-start | bytes 196616 | tf_op jit(solution)/shard_map/ppermute | solution.py:327
  9.3 0.3 collective-permute-start.7
  9.6 3.0 %collective-permute-start.8 = (bf16[512,128]{1,0:T(8,128)(2,1)S(1)}, bf16[512,128]{1,0:T(8,128)(2,1)S(1)}, u32[]{:S(2)}, u32[]{:S(2)}) collective-permute-start(bf16[512,128]{1,0:T(8,128)(2,1)S(1)} %get-tuple-element.29), channel_id=1, source_target_pairs={{0,24},{2,26},{4,28},{6,30},{8,16},{10,18},{12,20},{14,22},{16,8},... | collective-permute-start | bytes 393224 | tf_op jit(solution)/shard_map/ppermute | solution.py:327
  12.9 1.5 %collective-permute-done.6.refs_3_ = bf16[256,128]{1,0:T(8,128)(2,1)S(1)} collective-permute-done((bf16[256,128]{1,0:T(8,128)(2,1)S(1)}, bf16[256,128]{1,0:T(8,128)(2,1)S(1)}, u32[]{:S(2)}, u32[]{:S(2)}) %collective-permute-start.6) | collective-permute-done | bytes 65568 | tf_op jit(solution)/shard_map/ppermute | solution.py:327
  14.8 1.0 %collective-permute-start.9 = (bf16[512,128]{1,0:T(8,128)(2,1)S(1)}, bf16[512,128]{1,0:T(8,128)(2,1)S(1)}, u32[]{:S(2)}, u32[]{:S(2)}) collective-permute-start(bf16[512,128]{1,0:T(8,128)(2,1)S(1)} %get-tuple-element.27.refs_4_), channel_id=1, source_target_pairs={{0,2},{2,0},{4,6},{6,4},{8,10},{10,8},{12,14},{14,12},{16,18},{18,... | collective-permute-start | bytes 393224 | tf_op jit(solution)/shard_map/ppermute | solution.py:327
  15.7 4.1 %collective-permute-done.8.refs_6_ = bf16[512,128]{1,0:T(8,128)(2,1)S(1)} collective-permute-done((bf16[512,128]{1,0:T(8,128)(2,1)S(1)}, bf16[512,128]{1,0:T(8,128)(2,1)S(1)}, u32[]{:S(2)}, u32[]{:S(2)}) %collective-permute-start.8) | collective-permute-done | bytes 131104 | tf_op jit(solution)/shard_map/ppermute | solution.py:327
  19.8 2.6 %collective-permute-start = (bf16[512,128]{1,0:T(8,128)(2,1)S(1)}, bf16[512,128]{1,0:T(8,128)(2,1)S(1)}, u32[]{:S(2)}, u32[]{:S(2)}) collective-permute-start(bf16[512,128]{1,0:T(8,128)(2,1)S(1)} %get-tuple-element.22), channel_id=1, source_target_pairs={{0,16},{2,18},{4,20},{6,22},{8,24},{10,26},{12,28},{14,30},{16,0},... | collective-permute-start | bytes 393224 | tf_op jit(solution)/shard_map/ppermute | solution.py:327
  22.4 0.3 collective-permute-start.10
  22.6 1.2 %collective-permute-start.11 = (bf16[512,128]{1,0:T(8,128)(2,1)S(1)}, bf16[512,128]{1,0:T(8,128)(2,1)S(1)}, u32[]{:S(2)}, u32[]{:S(2)}) collective-permute-start(bf16[512,128]{1,0:T(8,128)(2,1)S(1)} %collective-permute-done.8.refs_6_), channel_id=1, source_target_pairs={{0,2},{2,0},{4,6},{6,4},{8,10},{10,8},{12,14},{14,12},{16,18},{18,... | collective-permute-start | bytes 393224 | tf_op jit(solution)/shard_map/ppermute | solution.py:327
  24.1 0.7 collective-permute-done.refs_0_
  24.7 0.6 collective-permute-start.14
  25.3 1.2 %collective-permute-done.10.refs_8_ = bf16[512,128]{1,0:T(8,128)(2,1)S(1)} collective-permute-done((bf16[512,128]{1,0:T(8,128)(2,1)S(1)}, bf16[512,128]{1,0:T(8,128)(2,1)S(1)}, u32[]{:S(2)}, u32[]{:S(2)}) %collective-permute-start.10) | collective-permute-done | bytes 131104 | tf_op jit(solution)/shard_map/ppermute | solution.py:327
  26.7 2.1 %collective-permute-done.11.refs_9_ = bf16[512,128]{1,0:T(8,128)(2,1)S(1)} collective-permute-done((bf16[512,128]{1,0:T(8,128)(2,1)S(1)}, bf16[512,128]{1,0:T(8,128)(2,1)S(1)}, u32[]{:S(2)}, u32[]{:S(2)}) %collective-permute-start.11) | collective-permute-done | bytes 131104 | tf_op jit(solution)/shard_map/ppermute | solution.py:327
  29.0 1.2 %collective-permute-start.1 = (bf16[512,128]{1,0:T(8,128)(2,1)S(1)}, bf16[512,128]{1,0:T(8,128)(2,1)S(1)}, u32[]{:S(2)}, u32[]{:S(2)}) collective-permute-start(bf16[512,128]{1,0:T(8,128)(2,1)S(1)} %collective-permute-done.refs_0_), channel_id=1, source_target_pairs={{0,2},{2,0},{4,6},{6,4},{8,10},{10,8},{12,14},{14,12},{16,18},{18,... | collective-permute-start | bytes 393224 | tf_op jit(solution)/shard_map/ppermute | solution.py:327
  30.2 1.2 %collective-permute-start.2 = (bf16[512,128]{1,0:T(8,128)(2,1)S(1)}, bf16[512,128]{1,0:T(8,128)(2,1)S(1)}, u32[]{:S(2)}, u32[]{:S(2)}) collective-permute-start(bf16[512,128]{1,0:T(8,128)(2,1)S(1)} %collective-permute-done.refs_0_), channel_id=1, source_target_pairs={{0,4},{2,6},{4,0},{6,2},{8,12},{10,14},{12,8},{14,10},{16,20},{18,... | collective-permute-start | bytes 393224 | tf_op jit(solution)/shard_map/ppermute | solution.py:327
  31.5 0.4 collective-permute-done.16.refs_14_
  31.9 1.0 %collective-permute-start.3 = (bf16[512,128]{1,0:T(8,128)(2,1)S(1)}, bf16[512,128]{1,0:T(8,128)(2,1)S(1)}, u32[]{:S(2)}, u32[]{:S(2)}) collective-permute-start(bf16[512,128]{1,0:T(8,128)(2,1)S(1)} %collective-permute-done.refs_0_), channel_id=1, source_target_pairs={{0,6},{2,4},{4,2},{6,0},{8,14},{10,12},{12,10},{14,8},{16,22},{18,... | collective-permute-start | bytes 393224 | tf_op jit(solution)/shard_map/ppermute | solution.py:327
  32.8 0.7 collective-permute-done.17.refs_15_
  33.5 5.2 %attend_early.1 = (bf16[4,256,128]{2,1,0:T(8,128)(2,1)S(1)}, bf16[4096,128]{1,0:T(8,128)(2,1)S(1)}, bf16[128,4096]{1,0:T(8,128)(2,1)S(1)}, f32[4,128,512]{2,1,0:T(8,128)S(1)}, f32[4,8,512]{2,1,0:T(8,128)S(1)}) custom-call(s32[3]{0:T(128)S(1)} %pad_add_fusion.place, bf16[256,128]{1,0:T(8,128)(2,1)S(1)} %get-tuple-element.23.refs_0_, ...), custom_call_target="tpu_custom_call" | custom-call | flops 1610612736 | bytes 3145728 | tf_op jit(solution)/shard_map/attend_early/pallas_call | solution.py:378
  38.8 2.1 %collective-permute-done.2.refs_2_ = bf16[512,128]{1,0:T(8,128)(2,1)S(1)} collective-permute-done((bf16[512,128]{1,0:T(8,128)(2,1)S(1)}, bf16[512,128]{1,0:T(8,128)(2,1)S(1)}, u32[]{:S(2)}, u32[]{:S(2)}) %collective-permute-start.2) | collective-permute-done | bytes 131104 | tf_op jit(solution)/shard_map/ppermute | solution.py:327
  40.9 23.4 %attend_late.1 = (bf16[256,128]{1,0:T(8,128)(2,1)S(1)}, bf16[256,128]{1,0:T(8,128)(2,1)S(1)}, bf16[256,128]{1,0:T(8,128)(2,1)S(1)}, bf16[256,128]{1,0:T(8,128)(2,1)S(1)}) custom-call(s32[3]{0:T(128)S(1)} %pad_add_fusion.place, f32[4]{0:T(128)S(1)} %copy-done.1, f32[1,128]{1,0:T(1,128)S(1)} %bitcast.4, bf16[512,128]{1,0:T(8,128)(2,1)S(1)} %collective-permute-done.refs_0_, ...), custom_call_target="tpu_custom_call" | custom-call | flops 536870912 | bytes 3145728 | tf_op jit(solution)/shard_map/attend_late/pallas_call | solution.py:387
  64.2 2.7 %collective-permute-start.18 = (bf16[256,128]{1,0:T(8,128)(2,1)S(1)}, bf16[256,128]{1,0:T(8,128)(2,1)S(1)}, u32[]{:S(2)}, u32[]{:S(2)}) collective-permute-start(bf16[256,128]{1,0:T(8,128)(2,1)S(1)} %get-tuple-element.36), channel_id=1, source_target_pairs={{0,8},{2,10},{4,12},{6,14},{8,0},{10,2},{12,4},{14,6},{16,24},{18,... | collective-permute-start | bytes 196616 | tf_op jit(solution)/shard_map/ppermute | solution.py:327
  67.0 0.8 collective-permute-start.19
  67.8 1.3 %collective-permute-start.20 = (bf16[256,128]{1,0:T(8,128)(2,1)S(1)}, bf16[256,128]{1,0:T(8,128)(2,1)S(1)}, u32[]{:S(2)}, u32[]{:S(2)}) collective-permute-start(bf16[256,128]{1,0:T(8,128)(2,1)S(1)} %get-tuple-element.38), channel_id=1, source_target_pairs={{0,24},{2,26},{4,28},{6,30},{8,16},{10,18},{12,20},{14,22},{16,8},... | collective-permute-start | bytes 196616 | tf_op jit(solution)/shard_map/ppermute | solution.py:327
  69.1 7.2 %collective-permute-start.21 = (bf16[256,128]{1,0:T(8,128)(2,1)S(1)}, bf16[256,128]{1,0:T(8,128)(2,1)S(1)}, u32[]{:S(2)}, u32[]{:S(2)}) collective-permute-start(bf16[256,128]{1,0:T(8,128)(2,1)S(1)} %get-tuple-element.35.refs_0_), channel_id=1, source_target_pairs={{0,1},{1,0},{2,3},{3,2},{4,5},{5,4},{6,7},{7,6},{8,9},{9,8},{10,11... | collective-permute-start | bytes 196616 | tf_op jit(solution)/shard_map/ppermute | solution.py:417
  76.3 0.8 collective-permute-start.23
  77.2 3.6 %collective-permute-start.24 = (bf16[256,128]{1,0:T(8,128)(2,1)S(1)}, bf16[256,128]{1,0:T(8,128)(2,1)S(1)}, u32[]{:S(2)}, u32[]{:S(2)}) collective-permute-start(bf16[256,128]{1,0:T(8,128)(2,1)S(1)} %collective-permute-done.20.refs_3_), channel_id=1, source_target_pairs={{0,1},{1,0},{2,3},{3,2},{4,5},{5,4},{6,7},{7,6},{8,9},{9,8},{10,11... | collective-permute-start | bytes 196616 | tf_op jit(solution)/shard_map/ppermute | solution.py:417
  80.8 0.9 %collective-permute-done.24.refs_7_ = bf16[256,128]{1,0:T(8,128)(2,1)S(1)} collective-permute-done((bf16[256,128]{1,0:T(8,128)(2,1)S(1)}, bf16[256,128]{1,0:T(8,128)(2,1)S(1)}, u32[]{:S(2)}, u32[]{:S(2)}) %collective-permute-start.24) | collective-permute-done | bytes 65568 | tf_op jit(solution)/shard_map/ppermute | solution.py:417
  81.7 2.6 %project_out.1 = bf16[256,2048]{1,0:T(8,128)(2,1)} custom-call(s32[3]{0:T(128)S(1)} %pad_add_fusion.place, bf16[256,128]{1,0:T(8,128)(2,1)S(1)} %get-tuple-element.35.refs_0_, bf16[256,128]{1,0:T(8,128)(2,1)S(1)} %collective-permute-done.18.refs_1_, bf16[256,128]{1,0:T(8,128)(2,1)S(1)} %collective-permute-done.19.refs_2_, ...), custom_call_target="tpu_custom_call" | custom-call | flops 1073741824 | bytes 6291456 | tf_op jit(solution)/shard_map/project_out/pallas_call | solution.py:418
  (31 shorter events, 1.4 us)
Async XLA Ops:
  0.0 81.7 %collective-permute-start.25 = (bf16[512,2048]{1,0:T(8,128)(2,1)}, bf16[512,2048]{1,0:T(8,128)(2,1)S(1)}, u32[]{:S(2)}, u32[]{:S(2)}) collective-permute-start(bf16[512,2048]{1,0:T(8,128)(2,1)} %refs_8_.1), channel_id=1, source_target_pairs={{0,1},{1,0},{2,3},{3,2},{4,5},{5,4},{6,7},{7,6},{8,9},{9,8},{10,11... | collective-permute-start | bytes 6291464 | tf_op jit(solution)/shard_map/ppermute | solution.py:363
  5.6 4.0 %collective-permute-start.4 = (bf16[256,128]{1,0:T(8,128)(2,1)S(1)}, bf16[256,128]{1,0:T(8,128)(2,1)S(1)}, u32[]{:S(2)}, u32[]{:S(2)}) collective-permute-start(bf16[256,128]{1,0:T(8,128)(2,1)S(1)} %get-tuple-element.24), channel_id=1, source_target_pairs={{0,8},{2,10},{4,12},{6,14},{8,0},{10,2},{12,4},{14,6},{16,24},{18,... | collective-permute-start | bytes 196616 | tf_op jit(solution)/shard_map/ppermute | solution.py:327
  7.0 5.7 %collective-permute-start.5 = (bf16[256,128]{1,0:T(8,128)(2,1)S(1)}, bf16[256,128]{1,0:T(8,128)(2,1)S(1)}, u32[]{:S(2)}, u32[]{:S(2)}) collective-permute-start(bf16[256,128]{1,0:T(8,128)(2,1)S(1)} %get-tuple-element.25), channel_id=1, source_target_pairs={{0,16},{2,18},{4,20},{6,22},{8,24},{10,26},{12,28},{14,30},{16,0},... | collective-permute-start | bytes 196616 | tf_op jit(solution)/shard_map/ppermute | solution.py:327
  9.3 5.0 %collective-permute-start.6 = (bf16[256,128]{1,0:T(8,128)(2,1)S(1)}, bf16[256,128]{1,0:T(8,128)(2,1)S(1)}, u32[]{:S(2)}, u32[]{:S(2)}) collective-permute-start(bf16[256,128]{1,0:T(8,128)(2,1)S(1)} %get-tuple-element.26), channel_id=1, source_target_pairs={{0,24},{2,26},{4,28},{6,30},{8,16},{10,18},{12,20},{14,22},{16,8},... | collective-permute-start | bytes 196616 | tf_op jit(solution)/shard_map/ppermute | solution.py:327
  9.3 5.5 %collective-permute-start.7 = (bf16[512,128]{1,0:T(8,128)(2,1)S(1)}, bf16[512,128]{1,0:T(8,128)(2,1)S(1)}, u32[]{:S(2)}, u32[]{:S(2)}) collective-permute-start(bf16[512,128]{1,0:T(8,128)(2,1)S(1)} %get-tuple-element.28), channel_id=1, source_target_pairs={{0,8},{2,10},{4,12},{6,14},{8,0},{10,2},{12,4},{14,6},{16,24},{18,... | collective-permute-start | bytes 393224 | tf_op jit(solution)/shard_map/ppermute | solution.py:327
  9.6 10.2 %collective-permute-start.8 = (bf16[512,128]{1,0:T(8,128)(2,1)S(1)}, bf16[512,128]{1,0:T(8,128)(2,1)S(1)}, u32[]{:S(2)}, u32[]{:S(2)}) collective-permute-start(bf16[512,128]{1,0:T(8,128)(2,1)S(1)} %get-tuple-element.29), channel_id=1, source_target_pairs={{0,24},{2,26},{4,28},{6,30},{8,16},{10,18},{12,20},{14,22},{16,8},... | collective-permute-start | bytes 393224 | tf_op jit(solution)/shard_map/ppermute | solution.py:327
  12.7 9.7 %collective-permute-start.12 = (bf16[512,128]{1,0:T(8,128)(2,1)S(1)}, bf16[512,128]{1,0:T(8,128)(2,1)S(1)}, u32[]{:S(2)}, u32[]{:S(2)}) collective-permute-start(bf16[512,128]{1,0:T(8,128)(2,1)S(1)} %get-tuple-element.27.refs_4_), channel_id=1, source_target_pairs={{0,4},{2,6},{4,0},{6,2},{8,12},{10,14},{12,8},{14,10},{16,20},{18,... | collective-permute-start | bytes 393224 | tf_op jit(solution)/shard_map/ppermute | solution.py:327
  14.3 8.3 %collective-permute-start.15 = (bf16[512,128]{1,0:T(8,128)(2,1)S(1)}, bf16[512,128]{1,0:T(8,128)(2,1)S(1)}, u32[]{:S(2)}, u32[]{:S(2)}) collective-permute-start(bf16[512,128]{1,0:T(8,128)(2,1)S(1)} %get-tuple-element.27.refs_4_), channel_id=1, source_target_pairs={{0,6},{2,4},{4,2},{6,0},{8,14},{10,12},{12,10},{14,8},{16,22},{18,... | collective-permute-start | bytes 393224 | tf_op jit(solution)/shard_map/ppermute | solution.py:327
  14.8 9.1 %collective-permute-start.9 = (bf16[512,128]{1,0:T(8,128)(2,1)S(1)}, bf16[512,128]{1,0:T(8,128)(2,1)S(1)}, u32[]{:S(2)}, u32[]{:S(2)}) collective-permute-start(bf16[512,128]{1,0:T(8,128)(2,1)S(1)} %get-tuple-element.27.refs_4_), channel_id=1, source_target_pairs={{0,2},{2,0},{4,6},{6,4},{8,10},{10,8},{12,14},{14,12},{16,18},{18,... | collective-permute-start | bytes 393224 | tf_op jit(solution)/shard_map/ppermute | solution.py:327
  19.8 4.9 %collective-permute-start = (bf16[512,128]{1,0:T(8,128)(2,1)S(1)}, bf16[512,128]{1,0:T(8,128)(2,1)S(1)}, u32[]{:S(2)}, u32[]{:S(2)}) collective-permute-start(bf16[512,128]{1,0:T(8,128)(2,1)S(1)} %get-tuple-element.22), channel_id=1, source_target_pairs={{0,16},{2,18},{4,20},{6,22},{8,24},{10,26},{12,28},{14,30},{16,0},... | collective-permute-start | bytes 393224 | tf_op jit(solution)/shard_map/ppermute | solution.py:327
  22.4 4.1 %collective-permute-start.10 = (bf16[512,128]{1,0:T(8,128)(2,1)S(1)}, bf16[512,128]{1,0:T(8,128)(2,1)S(1)}, u32[]{:S(2)}, u32[]{:S(2)}) collective-permute-start(bf16[512,128]{1,0:T(8,128)(2,1)S(1)} %collective-permute-done.7.refs_5_), channel_id=1, source_target_pairs={{0,2},{2,0},{4,6},{6,4},{8,10},{10,8},{12,14},{14,12},{16,18},{18,... | collective-permute-start | bytes 393224 | tf_op jit(solution)/shard_map/ppermute | solution.py:327
  22.6 6.2 %collective-permute-start.11 = (bf16[512,128]{1,0:T(8,128)(2,1)S(1)}, bf16[512,128]{1,0:T(8,128)(2,1)S(1)}, u32[]{:S(2)}, u32[]{:S(2)}) collective-permute-start(bf16[512,128]{1,0:T(8,128)(2,1)S(1)} %collective-permute-done.8.refs_6_), channel_id=1, source_target_pairs={{0,2},{2,0},{4,6},{6,4},{8,10},{10,8},{12,14},{14,12},{16,18},{18,... | collective-permute-start | bytes 393224 | tf_op jit(solution)/shard_map/ppermute | solution.py:327
  23.9 5.2 %collective-permute-start.13 = (bf16[512,128]{1,0:T(8,128)(2,1)S(1)}, bf16[512,128]{1,0:T(8,128)(2,1)S(1)}, u32[]{:S(2)}, u32[]{:S(2)}) collective-permute-start(bf16[512,128]{1,0:T(8,128)(2,1)S(1)} %collective-permute-done.7.refs_5_), channel_id=1, source_target_pairs={{0,4},{2,6},{4,0},{6,2},{8,12},{10,14},{12,8},{14,10},{16,20},{18,... | collective-permute-start | bytes 393224 | tf_op jit(solution)/shard_map/ppermute | solution.py:327
  24.7 5.5 %collective-permute-start.14 = (bf16[512,128]{1,0:T(8,128)(2,1)S(1)}, bf16[512,128]{1,0:T(8,128)(2,1)S(1)}, u32[]{:S(2)}, u32[]{:S(2)}) collective-permute-start(bf16[512,128]{1,0:T(8,128)(2,1)S(1)} %collective-permute-done.8.refs_6_), channel_id=1, source_target_pairs={{0,4},{2,6},{4,0},{6,2},{8,12},{10,14},{12,8},{14,10},{16,20},{18,... | collective-permute-start | bytes 393224 | tf_op jit(solution)/shard_map/ppermute | solution.py:327
  26.5 5.4 %collective-permute-start.16 = (bf16[512,128]{1,0:T(8,128)(2,1)S(1)}, bf16[512,128]{1,0:T(8,128)(2,1)S(1)}, u32[]{:S(2)}, u32[]{:S(2)}) collective-permute-start(bf16[512,128]{1,0:T(8,128)(2,1)S(1)} %collective-permute-done.7.refs_5_), channel_id=1, source_target_pairs={{0,6},{2,4},{4,2},{6,0},{8,14},{10,12},{12,10},{14,8},{16,22},{18,... | collective-permute-start | bytes 393224 | tf_op jit(solution)/shard_map/ppermute | solution.py:327
  28.8 4.7 %collective-permute-start.17 = (bf16[512,128]{1,0:T(8,128)(2,1)S(1)}, bf16[512,128]{1,0:T(8,128)(2,1)S(1)}, u32[]{:S(2)}, u32[]{:S(2)}) collective-permute-start(bf16[512,128]{1,0:T(8,128)(2,1)S(1)} %collective-permute-done.8.refs_6_), channel_id=1, source_target_pairs={{0,6},{2,4},{4,2},{6,0},{8,14},{10,12},{12,10},{14,8},{16,22},{18,... | collective-permute-start | bytes 393224 | tf_op jit(solution)/shard_map/ppermute | solution.py:327
  29.0 9.7 %collective-permute-start.1 = (bf16[512,128]{1,0:T(8,128)(2,1)S(1)}, bf16[512,128]{1,0:T(8,128)(2,1)S(1)}, u32[]{:S(2)}, u32[]{:S(2)}) collective-permute-start(bf16[512,128]{1,0:T(8,128)(2,1)S(1)} %collective-permute-done.refs_0_), channel_id=1, source_target_pairs={{0,2},{2,0},{4,6},{6,4},{8,10},{10,8},{12,14},{14,12},{16,18},{18,... | collective-permute-start | bytes 393224 | tf_op jit(solution)/shard_map/ppermute | solution.py:327
  30.2 10.6 %collective-permute-start.2 = (bf16[512,128]{1,0:T(8,128)(2,1)S(1)}, bf16[512,128]{1,0:T(8,128)(2,1)S(1)}, u32[]{:S(2)}, u32[]{:S(2)}) collective-permute-start(bf16[512,128]{1,0:T(8,128)(2,1)S(1)} %collective-permute-done.refs_0_), channel_id=1, source_target_pairs={{0,4},{2,6},{4,0},{6,2},{8,12},{10,14},{12,8},{14,10},{16,20},{18,... | collective-permute-start | bytes 393224 | tf_op jit(solution)/shard_map/ppermute | solution.py:327
  31.9 9.0 %collective-permute-start.3 = (bf16[512,128]{1,0:T(8,128)(2,1)S(1)}, bf16[512,128]{1,0:T(8,128)(2,1)S(1)}, u32[]{:S(2)}, u32[]{:S(2)}) collective-permute-start(bf16[512,128]{1,0:T(8,128)(2,1)S(1)} %collective-permute-done.refs_0_), channel_id=1, source_target_pairs={{0,6},{2,4},{4,2},{6,0},{8,14},{10,12},{12,10},{14,8},{16,22},{18,... | collective-permute-start | bytes 393224 | tf_op jit(solution)/shard_map/ppermute | solution.py:327
  33.5 7.3 %copy-start.1 = (f32[4]{0:T(128)S(1)}, f32[4]{0:T(128)}, u32[]{:S(2)}) copy-start(f32[4]{0:T(128)} %lambdas.1) | copy-start | bytes 52
  33.5 7.3 %copy-start.2 = (f32[128]{0:T(128)S(1)}, f32[128]{0:T(128)}, u32[]{:S(2)}) copy-start(f32[128]{0:T(128)} %param.16) | copy-start | bytes 1540
  38.7 43.0 %copy-start = (bf16[512,2048]{1,0:T(8,128)(2,1)S(1)}, bf16[512,2048]{1,0:T(8,128)(2,1)}, u32[]{:S(2)}) copy-start(bf16[512,2048]{1,0:T(8,128)(2,1)} %refs_8_.1) | copy-start | bytes 6291460
  64.2 12.1 %collective-permute-start.18 = (bf16[256,128]{1,0:T(8,128)(2,1)S(1)}, bf16[256,128]{1,0:T(8,128)(2,1)S(1)}, u32[]{:S(2)}, u32[]{:S(2)}) collective-permute-start(bf16[256,128]{1,0:T(8,128)(2,1)S(1)} %get-tuple-element.36), channel_id=1, source_target_pairs={{0,8},{2,10},{4,12},{6,14},{8,0},{10,2},{12,4},{14,6},{16,24},{18,... | collective-permute-start | bytes 196616 | tf_op jit(solution)/shard_map/ppermute | solution.py:327
  67.0 9.4 %collective-permute-start.19 = (bf16[256,128]{1,0:T(8,128)(2,1)S(1)}, bf16[256,128]{1,0:T(8,128)(2,1)S(1)}, u32[]{:S(2)}, u32[]{:S(2)}) collective-permute-start(bf16[256,128]{1,0:T(8,128)(2,1)S(1)} %get-tuple-element.37), channel_id=1, source_target_pairs={{0,16},{2,18},{4,20},{6,22},{8,24},{10,26},{12,28},{14,30},{16,0},... | collective-permute-start | bytes 196616 | tf_op jit(solution)/shard_map/ppermute | solution.py:327
  67.8 9.4 %collective-permute-start.20 = (bf16[256,128]{1,0:T(8,128)(2,1)S(1)}, bf16[256,128]{1,0:T(8,128)(2,1)S(1)}, u32[]{:S(2)}, u32[]{:S(2)}) collective-permute-start(bf16[256,128]{1,0:T(8,128)(2,1)S(1)} %get-tuple-element.38), channel_id=1, source_target_pairs={{0,24},{2,26},{4,28},{6,30},{8,16},{10,18},{12,20},{14,22},{16,8},... | collective-permute-start | bytes 196616 | tf_op jit(solution)/shard_map/ppermute | solution.py:327
  69.1 11.7 %collective-permute-start.21 = (bf16[256,128]{1,0:T(8,128)(2,1)S(1)}, bf16[256,128]{1,0:T(8,128)(2,1)S(1)}, u32[]{:S(2)}, u32[]{:S(2)}) collective-permute-start(bf16[256,128]{1,0:T(8,128)(2,1)S(1)} %get-tuple-element.35.refs_0_), channel_id=1, source_target_pairs={{0,1},{1,0},{2,3},{3,2},{4,5},{5,4},{6,7},{7,6},{8,9},{9,8},{10,11... | collective-permute-start | bytes 196616 | tf_op jit(solution)/shard_map/ppermute | solution.py:417
  76.3 4.5 %collective-permute-start.22 = (bf16[256,128]{1,0:T(8,128)(2,1)S(1)}, bf16[256,128]{1,0:T(8,128)(2,1)S(1)}, u32[]{:S(2)}, u32[]{:S(2)}) collective-permute-start(bf16[256,128]{1,0:T(8,128)(2,1)S(1)} %collective-permute-done.18.refs_1_), channel_id=1, source_target_pairs={{0,1},{1,0},{2,3},{3,2},{4,5},{5,4},{6,7},{7,6},{8,9},{9,8},{10,11... | collective-permute-start | bytes 196616 | tf_op jit(solution)/shard_map/ppermute | solution.py:417
  76.3 4.5 %collective-permute-start.23 = (bf16[256,128]{1,0:T(8,128)(2,1)S(1)}, bf16[256,128]{1,0:T(8,128)(2,1)S(1)}, u32[]{:S(2)}, u32[]{:S(2)}) collective-permute-start(bf16[256,128]{1,0:T(8,128)(2,1)S(1)} %collective-permute-done.19.refs_2_), channel_id=1, source_target_pairs={{0,1},{1,0},{2,3},{3,2},{4,5},{5,4},{6,7},{7,6},{8,9},{9,8},{10,11... | collective-permute-start | bytes 196616 | tf_op jit(solution)/shard_map/ppermute | solution.py:417
  77.2 4.5 %collective-permute-start.24 = (bf16[256,128]{1,0:T(8,128)(2,1)S(1)}, bf16[256,128]{1,0:T(8,128)(2,1)S(1)}, u32[]{:S(2)}, u32[]{:S(2)}) collective-permute-start(bf16[256,128]{1,0:T(8,128)(2,1)S(1)} %collective-permute-done.20.refs_3_), channel_id=1, source_target_pairs={{0,1},{1,0},{2,3},{3,2},{4,5},{5,4},{6,7},{7,6},{8,9},{9,8},{10,11... | collective-permute-start | bytes 196616 | tf_op jit(solution)/shard_map/ppermute | solution.py:417
